TPU v7x, 512 devices: a whole 4x8x8 slice. The times are simulated.
512 devices in a mesh: sp: 32 (over z, x), tp: 16 (over y, core).
Axes of the slice: x: 4, y: 8, z: 8, core: 2. Of those that a mesh axis runs over, the one named last changes fastest.
Arguments:
- residual: bfloat16 [8192, 2048], P('sp', 'tp'), may hold values from -26 to 26
- queries: bfloat16 [2048, 8192], P('tp', 'sp'), may hold values from -6 to 6
- keys: bfloat16 [2048, 8192], P('tp', 'sp'), may hold values from -6 to 6
- values: bfloat16 [2048, 8192], P('tp', 'sp'), may hold values from -12 to 12
- forget_cache: float32 [32, 8192], P('tp', 'sp'), as said below
- out_weight: bfloat16 [2048, 2048], P('tp'), may hold values from -0.125 to 0.125
- norm_gain: float32 [2048], replicated, may hold values from 0.1 to 1.9
- routes: int32 [8192, 2], P('sp'), may hold values from 0 to 31, all different within a row; in each aligned block of 256 rows (0 to 255, 256 to 511, ...) at most 20 rows name the same one
- route_weight: float32 [8192, 2], P('sp'), may hold values from 0.2 to 1
- gate_weight: bfloat16 [32, 2048, 4096], P('sp', None, 'tp'), may hold values from -0.125 to 0.125
- up_weight: bfloat16 [32, 2048, 4096], P('sp', None, 'tp'), may hold values from -0.125 to 0.125
- down_weight: bfloat16 [32, 4096, 2048], P('sp', 'tp'), may hold values from -0.09375 to 0.09375
Outputs:
- updated: bfloat16 [8192, 2048], P('sp', 'tp')
Inputs may be any that keep to these rules, and one draw needn't show every extreme that they name: `routes`: each row names 2 different experts; within the 256 rows of one index of sp no expert is named by more than 20 rows, and in the rows of some index some expert is named by exactly 20. `forget_cache`: each head's row never rises from one position to the next.
All inputs are finite; a program needn't handle non-finite values.
Results may differ from a plain program's by a relative error of at most 0.013.
Values may be sent and summed in bfloat16 or wider, within the bound.
No kernel may reach another device: no remote copies, remote signals or barrier semaphores. Data moves between devices by JAX's collectives and lax.ppermute only.
A program may use at most 64 MiB of HBM per device.

v0:
```python
import jax
import jax.numpy as jnp
from jax import lax
from jax.sharding import Mesh
from jax.sharding import PartitionSpec as P

SP = ("sp_0", "sp_1")


norm_eps = 1e-06
masked_score = -1e30
key_span = 1024


def gathered_by_axis(shard, axes, dim):
    out = shard
    for number in range(len(axes) - 1, -1, -1):
        out = lax.all_gather(out, axes[number], axis=dim, tiled=True)
    return out


def cut_along(shard, dim, peers):
    before, after = (shard.shape[:dim], shard.shape[dim + 1 :])
    return jnp.moveaxis(shard.reshape(*before, peers, -1, *after), dim, 0)


def sum_at_owner(shard, axis, dim):
    peers = lax.axis_size(axis)
    pieces = lax.all_to_all(cut_along(shard, dim, peers), axis, 0, 0, tiled=True)
    return jnp.sum(pieces.astype(jnp.float32), axis=0)


def sent_to_all(shard, axis):
    copies = jnp.broadcast_to(shard, (lax.axis_size(axis), *shard.shape))
    return lax.all_to_all(copies, axis, split_axis=0, concat_axis=0, tiled=True)


def taken_together(shard, axis):
    return sent_to_all(shard, axis).sum(axis=0)


def shards(
    residual,
    queries,
    keys,
    values,
    forget_cache,
    out_weight,
    norm_gain,
    routes,
    route_weight,
    gate_weight,
    up_weight,
    down_weight,
):
    sp_count = lax.axis_size(SP)
    token_count, local_width = residual.shape
    model_width = norm_gain.shape[0]
    head_count = forget_cache.shape[0]
    head_width = queries.shape[0] // head_count
    first_token = lax.axis_index(SP) * token_count
    last_token = first_token + token_count - 1
    query_heads = queries.reshape(head_count, head_width, token_count)
    query_place = first_token + jnp.arange(token_count, dtype=jnp.int32)
    score_scale = head_width ** (-0.5)

    def attend_block(state_now, key_block, value_block, cache_block, key_first):
        running_peak, running_total, running_sum = state_now
        block_length = key_block.shape[1]
        key_heads = key_block.reshape(head_count, head_width, block_length)
        value_heads = value_block.reshape(head_count, head_width, block_length)
        scores = (
            jnp.einsum("hdq,hdk->hqk", query_heads, key_heads, preferred_element_type=jnp.float32)
            * score_scale
        )
        scores = scores + forget_cache[:, :, None] - cache_block[:, None, :]
        key_place = key_first + jnp.arange(block_length, dtype=jnp.int32)
        allowed = key_place[None, :] <= query_place[:, None]
        scores = jnp.where(allowed[None], scores, masked_score)
        new_peak = jnp.maximum(running_peak, jnp.max(scores, axis=2))
        weights = jnp.exp(scores - new_peak[:, :, None])
        shrink = jnp.exp(running_peak - new_peak)
        new_total = running_total * shrink + jnp.sum(weights, axis=2)
        new_sum = running_sum * shrink[:, None, :] + jnp.einsum(
            "hdk,hqk->hdq",
            value_heads,
            weights.astype(jnp.bfloat16),
            preferred_element_type=jnp.float32,
        )
        return (new_peak, new_total, new_sum)

    initial = (
        jnp.full((head_count, token_count), masked_score, jnp.float32),
        jnp.zeros((head_count, token_count), jnp.float32),
        jnp.zeros((head_count, head_width, token_count), jnp.float32),
    )
    key_part = gathered_by_axis(keys.astype(jnp.float32), SP, 1).astype(jnp.bfloat16)
    value_part = gathered_by_axis(values.astype(jnp.float32), SP, 1).astype(jnp.bfloat16)
    cache_part = gathered_by_axis(forget_cache, SP, 1)
    part_length = key_part.shape[1]
    block_length = key_span

    def one_block(block_index, state_in):
        start_column = block_index * block_length
        key_block = lax.dynamic_slice_in_dim(key_part, start_column, block_length, 1)
        value_block = lax.dynamic_slice_in_dim(value_part, start_column, block_length, 1)
        cache_block = lax.dynamic_slice_in_dim(cache_part, start_column, block_length, 1)
        return lax.cond(
            start_column <= last_token,
            lambda inner: attend_block(inner, key_block, value_block, cache_block, start_column),
            lambda inner: inner,
            state_in,
        )

    final_peak, final_total, final_sum = lax.fori_loop(
        0, part_length // block_length, one_block, initial
    )
    attended = (
        (final_sum / final_total[:, None, :])
        .astype(jnp.bfloat16)
        .reshape(head_count * head_width, token_count)
    )
    projected = lax.dot_general(
        attended, out_weight, (((0,), (0,)), ((), ())), preferred_element_type=jnp.float32
    )
    head_sum = sum_at_owner(projected.astype(jnp.bfloat16), "tp", 1)
    stream = (residual.astype(jnp.float32) + head_sum).astype(jnp.bfloat16)
    top_count = routes.shape[1]
    item_count = token_count * top_count
    capacity = max(2, token_count * top_count * 5 // (4 * sp_count))
    expert_of = routes.reshape(item_count)
    onehot = (expert_of[:, None] == jnp.arange(sp_count, dtype=jnp.int32)[None, :]).astype(
        jnp.int32
    )
    earlier = jnp.cumsum(onehot, axis=0) - onehot
    target = expert_of * capacity + jnp.sum(earlier * onehot, axis=1)
    matches = target[None, :] == jnp.arange(sp_count * capacity, dtype=jnp.int32)[:, None]
    filled = jnp.any(matches, axis=1)
    source_row = (
        jnp.sum(jnp.where(matches, jnp.arange(item_count, dtype=jnp.int32)[None, :], 0), axis=1)
        // top_count
    )
    local_rows = stream.astype(jnp.float32)
    squares = taken_together(jnp.sum(local_rows * local_rows, axis=1), "tp")
    row_scale = lax.rsqrt(squares / model_width + norm_eps)
    local_gain = lax.dynamic_slice_in_dim(
        norm_gain, lax.axis_index("tp") * local_width, local_width
    )
    normed = (local_rows * row_scale[:, None] * local_gain[None, :]).astype(jnp.bfloat16)
    taken_rows = jnp.take(normed, source_row, axis=0)
    taken_rows = jnp.where(filled[:, None], taken_rows, jnp.zeros((), normed.dtype))
    arrived = lax.all_gather(
        lax.all_to_all(
            taken_rows.reshape(sp_count, capacity, normed.shape[1]),
            SP,
            split_axis=0,
            concat_axis=0,
            tiled=True,
        ),
        "tp",
        axis=2,
        tiled=True,
    )
    source_count = arrived.shape[0]
    slot_count = arrived.shape[1]
    flat_rows = arrived.reshape(source_count * slot_count, model_width)
    gate_value = jnp.dot(flat_rows, gate_weight[0], preferred_element_type=jnp.float32)
    up_value = jnp.dot(flat_rows, up_weight[0], preferred_element_type=jnp.float32)
    hidden = (jax.nn.silu(gate_value) * up_value).astype(jnp.bfloat16)
    down_value = jnp.dot(hidden, down_weight[0], preferred_element_type=jnp.float32)
    summed = sum_at_owner(
        down_value.reshape(source_count, slot_count, model_width).astype(jnp.bfloat16), "tp", 2
    )
    expert_back = lax.all_to_all(
        summed.astype(jnp.bfloat16), SP, split_axis=0, concat_axis=0, tiled=True
    )
    back_rows = expert_back.reshape(sp_count * capacity, local_width)
    picked = (
        jnp.take(back_rows, target, axis=0).astype(jnp.float32)
        * route_weight.reshape(item_count)[:, None]
    )
    mixture = jnp.sum(picked.reshape(token_count, top_count, local_width), axis=1)
    return (stream.astype(jnp.float32) + mixture).astype(jnp.bfloat16)


def solution(mesh):
    finer = Mesh(mesh.devices.reshape(8, 4, mesh.shape["tp"]), ("sp_0", "sp_1", "tp"))
    in_specs = (
        P(SP, "tp"),
        P("tp", SP),
        P("tp", SP),
        P("tp", SP),
        P("tp", SP),
        P("tp", None),
        P(),
        P(SP, None),
        P(SP, None),
        P(SP, None, "tp"),
        P(SP, None, "tp"),
        P(SP, "tp", None),
    )
    out_specs = P(SP, "tp")
    return jax.shard_map(
        shards, mesh=finer, in_specs=in_specs, out_specs=out_specs, check_vma=False
    )
```

profile of v0, /device:TPU:1, one launch (start us, length us, event | category | flops | bytes accessed | tf_op | source)
XLA Modules:
  0.0 360.3 jit_solution(1007863958048043251)
XLA Ops:
  6.5 12.8 %all_gather.21 = bf16[128,1024]{1,0:T(8,128)(2,1)} all-gather(bf16[128,256]{1,0:T(8,128)(2,1)} %param.18), channel_id=1, replica_groups=mesh['sp_0'=8,'sp_1'=4,'tp'=16] {'sp_1'}, dimensions={1}, use_global_device_ids=true | all-gather | bytes 327680 | tf_op jit(solution)/shard_map/all_gather | solution.py:18
  19.4 10.3 %all_gather.25 = bf16[128,1024]{1,0:T(8,128)(2,1)} all-gather(bf16[128,256]{1,0:T(8,128)(2,1)} %param.19), channel_id=1, replica_groups=mesh['sp_0'=8,'sp_1'=4,'tp'=16] {'sp_1'}, dimensions={1}, use_global_device_ids=true | all-gather | bytes 327680 | tf_op jit(solution)/shard_map/all_gather | solution.py:18
  29.8 8.7 %all_gather.23 = f32[2,1024]{1,0:T(2,128)S(1)} all-gather(f32[2,256]{1,0:T(2,128)} %param.20), channel_id=1, replica_groups=mesh['sp_0'=8,'sp_1'=4,'tp'=16] {'sp_1'}, dimensions={1}, use_global_device_ids=true | all-gather | bytes 10240 | tf_op jit(solution)/shard_map/all_gather | solution.py:18
  38.5 26.0 %all_gather.24 = f32[2,8192]{1,0:T(2,128)S(1)} all-gather(f32[2,1024]{1,0:T(2,128)S(1)} %all_gather.23), channel_id=1, replica_groups=mesh['sp_0'=8,'sp_1'=4,'tp'=16] {'sp_0'}, dimensions={1}, use_global_device_ids=true | all-gather | bytes 73728 | tf_op jit(solution)/shard_map/all_gather | solution.py:18
  64.5 0.6 all-gather.4.cloned.1.call-done
  65.1 44.3 %all-gather.6.cloned.1.call-done = bf16[128,8192]{1,0:T(8,128)(2,1)} async-done(((bf16[128,1024]{1,0:T(8,128)(2,1)}), bf16[128,8192]{1,0:T(8,128)(2,1)}) %all-gather.6.cloned.1.call-update) | async-done | bytes 2097168 | tf_op jit(solution)/shard_map/all_gather | solution.py:18
  109.4 4.2 %while.18 = (s32[]{:T(128)}, f32[2,256]{1,0:T(2,128)S(1)}, f32[2,256]{1,0:T(2,128)S(1)}, f32[2,64,256]{2,1,0:T(8,128)S(1)}, s32[]{:T(128)}, /*index=5*/bf16[128,...) while((s32[]{:T(128)}, f32[2,256]{1,0:T(2,128)S(1)}, ...), condition=%wide.region_5.6_spmd.clone, body=%wide.region_0.5_spmd.clone.sunk | while | flops 139266304 | bytes 8788313 | solution.py:115
  109.4 3.8 %conditional.3 = ((f32[2,256]{1,0:T(2,128)S(1)}, f32[2,256]{1,0:T(2,128)S(1)}, f32[2,64,256]{2,1,0:T(8,128)S(1)})) conditional(s32[]{:T(128)} %convert_element_type.119, (f32[2,256]{1,0:T(2,128)S(1)}, f32[2,256]{1,0:T(2,128)S(1)}, f32[2,64,256]{2,1,0:T(8,128)S(1)}) %tuple.55, (s32[]{:T(128)}, s32[]{:T(128)}, bf16[128,8192]{1,0:T(8,128)(2,1)}, ...), branch_computations={%region_1.0_spmd, %region_2.4_spmd} | conditional | flops 139266304 | bytes 8787026 | solution.py:108
  109.5 1.1 constant_dynamic-slice_fusion
  110.6 0.2 broadcast_compare_fusion
  110.8 1.6 fusion.26
  112.4 0.3 fusion.3
  112.8 0.5 convolution_add_fusion
  113.6 0.5 fusion.7
  114.1 1.3 copy.95
  115.4 11.7 %all-to-all-start = ((bf16[16,256,128]{2,1,0:T(8,128)(2,1)}), bf16[16,256,128]{2,1,0:T(8,128)(2,1)S(1)}, u32[]{:S(2)}, u32[]{:S(2)}) async-start(bf16[16,256,128]{2,1,0:T(8,128)(2,1)} %bitcast.60), calls=%async_computation | async-start | bytes 2097152 | tf_op jit(solution)/shard_map/all_to_all | solution.py:29
  127.2 0.1 eq.39
  127.4 0.1 reshape.233
  127.5 1.2 reduce-window.6
  128.7 0.2 slice_reduce_fusion
  129.1 0.2 select_reduce_fusion
  129.4 0.2 fusion.8
  129.7 25.4 %all-to-all-done = bf16[16,256,128]{2,1,0:T(8,128)(2,1)S(1)} async-done(((bf16[16,256,128]{2,1,0:T(8,128)(2,1)}), bf16[16,256,128]{2,1,0:T(8,128)(2,1)S(1)}, u32[]{:S(2)}, u32[]{:S(2)}) %all-to-all-start) | async-done | bytes 1048608 | tf_op jit(solution)/shard_map/all_to_all | solution.py:29
  155.1 0.1 convert_reduce_fusion
  155.3 0.6 broadcast_in_dim.101
  156.0 3.4 all-to-all-start.1
  159.6 0.8 dynamic_slice.42
  160.3 6.4 %all-to-all-done.1 = f32[16,1,256]{2,1,0:T(1,128)S(1)} async-done(((f32[16,1,256]{2,1,0:T(1,128)}), f32[16,1,256]{2,1,0:T(1,128)S(1)}, u32[]{:S(2)}, u32[]{:S(2)}) %all-to-all-start.1) | async-done | bytes 16416 | tf_op jit(solution)/shard_map/all_to_all | solution.py:35
  166.9 2.0 gather_fusion
  168.9 0.3 select_select_fusion
  169.2 42.5 %all_to_all.26 = bf16[32,20,128]{2,1,0:T(8,128)(2,1)} all-to-all(bf16[32,20,128]{2,1,0:T(8,128)(2,1)S(1)} %select_select_fusion), channel_id=1, replica_groups=mesh['sp_0'=8,'sp_1'=4,'tp'=16] {'sp_0','sp_1'}, dimensions={0} | all-to-all | bytes 327680 | tf_op jit(solution)/shard_map/all_to_all | solution.py:153
  211.8 39.8 %all-gather.8.cloned.1.call-done = bf16[32,20,2048]{2,1,0:T(8,128)(2,1)} async-done(((bf16[32,20,128]{2,1,0:T(8,128)(2,1)}), bf16[32,20,2048]{2,1,0:T(8,128)(2,1)}) %all-gather.8.cloned.1.call-update) | async-done | bytes 2621456 | tf_op jit(solution)/shard_map/all_gather | solution.py:152
  251.6 5.2 %reshape.235 = bf16[640,2048]{1,0:T(8,128)(2,1)} reshape(bf16[32,20,2048]{2,1,0:T(8,128)(2,1)} %all-gather.8.cloned.1.call-done) | data formatting | bytes 5242880 | tf_op jit(solution)/shard_map/reshape | solution.py:166
  256.7 2.7 fusion.12
  259.5 0.8 fusion.9
  260.5 0.8 fusion.6
  261.3 2.2 copy.94
  263.5 4.6 %all-to-all-start.3 = ((bf16[16,32,20,128]{3,1,2,0:T(8,128)(2,1)}), bf16[16,32,20,128]{3,1,2,0:T(8,128)(2,1)}, u32[]{:S(2)}, u32[]{:S(2)}) async-start(bf16[16,32,20,128]{3,1,2,0:T(8,128)(2,1)} %bitcast.62), calls=%async_computation.3 | async-start | bytes 5242880 | tf_op jit(solution)/shard_map/all_to_all | solution.py:29
  268.4 0.1 mul.123
  268.7 0.2 copy.75
  269.0 58.9 %all-to-all-done.3 = bf16[16,32,20,128]{3,1,2,0:T(8,128)(2,1)} async-done(((bf16[16,32,20,128]{3,1,2,0:T(8,128)(2,1)}), bf16[16,32,20,128]{3,1,2,0:T(8,128)(2,1)}, u32[]{:S(2)}, u32[]{:S(2)}) %all-to-all-start.3) | async-done | bytes 2621472 | tf_op jit(solution)/shard_map/all_to_all | solution.py:29
  327.9 2.1 reduce_sum.94
  330.0 0.7 copy.80
  330.7 9.6 %all-to-all-start.4 = ((bf16[32,20,128]{2,1,0:T(8,128)(2,1)}), bf16[32,20,128]{2,1,0:T(8,128)(2,1)S(1)}, u32[]{:S(2)}, u32[]{:S(2)}) async-start(bf16[32,20,128]{2,1,0:T(8,128)(2,1)} %copy.80), calls=%async_computation.4 | async-start | bytes 393216 | tf_op jit(solution)/shard_map/all_to_all | solution.py:174
  340.4 9.8 %all-to-all-done.4 = bf16[32,20,128]{2,1,0:T(8,128)(2,1)S(1)} async-done(((bf16[32,20,128]{2,1,0:T(8,128)(2,1)}), bf16[32,20,128]{2,1,0:T(8,128)(2,1)S(1)}, u32[]{:S(2)}, u32[]{:S(2)}) %all-to-all-start.4) | async-done | bytes 163872 | tf_op jit(solution)/shard_map/all_to_all | solution.py:174
  350.3 1.3 gather_fusion.1
  351.6 1.5 multiply_reduce_fusion
  353.1 0.7 fusion.18
  (73 shorter events, 1.9 us)
Async XLA Ops:
  6.5 253.9 %copy-start = (bf16[1,256,2048]{2,1,0:T(8,128)(2,1)S(1)}, bf16[1,256,2048]{2,1,0:T(8,128)(2,1)}, u32[]{:S(2)}) copy-start(bf16[1,256,2048]{2,1,0:T(8,128)(2,1)} %param.27) | copy-start | bytes 3145732
  6.5 58.5 %all-gather.4.cloned.1.call-start = ((), (), s32[]{:S(2)}) async-start(), calls=%async_computation.5 | async-start | bytes 2359296 | tf_op jit(solution)/shard_map/all_gather | solution.py:18
  19.4 90.0 %all-gather.6.cloned.1.call-start = ((), (), s32[]{:S(2)}) async-start(), calls=%async_computation.6 | async-start | bytes 2359296 | tf_op jit(solution)/shard_map/all_gather | solution.py:18
  109.4 4.2 %copy-start.2 = (bf16[128,2048]{1,0:T(8,128)(2,1)S(1)}, bf16[128,2048]{1,0:T(8,128)(2,1)}, u32[]{:S(2)}) copy-start(bf16[128,2048]{1,0:T(8,128)(2,1)} %param.21) | copy-start | bytes 1572868
  114.1 13.0 %copy-start.4 = (s32[256,2]{0,1:T(2,128)S(1)}, s32[256,2]{0,1:T(2,128)}, u32[]{:S(2)}) copy-start(s32[256,2]{0,1:T(2,128)} %param.23) | copy-start | bytes 6148
  115.4 39.8 %copy-start.3 = (bf16[256,128]{1,0:T(8,128)(2,1)S(1)}, bf16[256,128]{1,0:T(8,128)(2,1)}, u32[]{:S(2)}) copy-start(bf16[256,128]{1,0:T(8,128)(2,1)} %param.16) | copy-start | bytes 196612
  115.4 39.7 %all-to-all-start = ((bf16[16,256,128]{2,1,0:T(8,128)(2,1)}), bf16[16,256,128]{2,1,0:T(8,128)(2,1)S(1)}, u32[]{:S(2)}, u32[]{:S(2)}) async-start(bf16[16,256,128]{2,1,0:T(8,128)(2,1)} %bitcast.60), calls=%async_computation | async-start | bytes 2097152 | tf_op jit(solution)/shard_map/all_to_all | solution.py:29
  156.0 10.8 %all-to-all-start.1 = ((f32[16,1,256]{2,1,0:T(1,128)}), f32[16,1,256]{2,1,0:T(1,128)S(1)}, u32[]{:S(2)}, u32[]{:S(2)}) async-start(f32[16,1,256]{2,1,0:T(1,128)} %broadcast_in_dim.101), calls=%async_computation.1 | async-start | bytes 32768 | tf_op jit(solution)/shard_map/all_to_all | solution.py:35
  159.4 92.2 %all-gather.8.cloned.1.call-start = ((), (), s32[]{:S(2)}) async-start(), calls=%async_computation.7 | async-start | bytes 3342336 | tf_op jit(solution)/shard_map/all_gather | solution.py:152
  211.8 45.0 %copy-start.6 = (bf16[1,2048,256]{2,1,0:T(8,128)(2,1)S(1)}, bf16[1,2048,256]{2,1,0:T(8,128)(2,1)}, u32[]{:S(2)}) copy-start(bf16[1,2048,256]{2,1,0:T(8,128)(2,1)} %param.25) | copy-start | bytes 3145732
  256.7 2.8 copy-start.1
  256.7 2.8 copy-start.7
  263.5 5.3 %copy-start.5 = (f32[256,2]{0,1:T(2,128)S(1)}, f32[256,2]{0,1:T(2,128)}, u32[]{:S(2)}) copy-start(f32[256,2]{0,1:T(2,128)} %param.24) | copy-start | bytes 6148
  263.5 64.3 %all-to-all-start.3 = ((bf16[16,32,20,128]{3,1,2,0:T(8,128)(2,1)}), bf16[16,32,20,128]{3,1,2,0:T(8,128)(2,1)}, u32[]{:S(2)}, u32[]{:S(2)}) async-start(bf16[16,32,20,128]{3,1,2,0:T(8,128)(2,1)} %bitcast.62), calls=%async_computation.3 | async-start | bytes 5242880 | tf_op jit(solution)/shard_map/all_to_all | solution.py:29
  330.7 19.5 %all-to-all-start.4 = ((bf16[32,20,128]{2,1,0:T(8,128)(2,1)}), bf16[32,20,128]{2,1,0:T(8,128)(2,1)S(1)}, u32[]{:S(2)}, u32[]{:S(2)}) async-start(bf16[32,20,128]{2,1,0:T(8,128)(2,1)} %copy.80), calls=%async_computation.4 | async-start | bytes 393216 | tf_op jit(solution)/shard_map/all_to_all | solution.py:174
Sparse Core Ops, SparseCore 0:
  19.5 45.5 all-gather.3
  67.2 42.1 all-gather.5
  211.9 39.6 all-gather.7
where the time goes:
time: 363 us; the launch traced here: 360 us
  waiting for transfers between devices  185 us (51%)
  blocking collectives  100 us (28%)
  starting transfers between devices  29.4 us (8%)
  local copies, waits for them, and re-layouts  17.1 us (5%)
  between operations  13.4 us (4%)
  other arithmetic  7.3 us (2%)
  matrix products  6.94 us (2%)
    all_to_all x2, waiting for transfers between devices, sum_at_owner(): lax.all_to_all(cut_along(shard, dim, peers), axis, 0, 0, tiled=True)  84.3 us
    all_gather x4, blocking collectives, gathered_by_axis(): out = lax.all_gather(out, axes[number], axis=dim, tiled=True)  57.9 us
    all_gather x2, waiting for transfers between devices, gathered_by_axis(): out = lax.all_gather(out, axes[number], axis=dim, tiled=True)  44.9 us
    all_to_all x1, blocking collectives, shards(): lax.all_to_all(taken_rows.reshape(sp_count, capacity, normed.shape[1]), S...  42.5 us
    all_gather x1, waiting for transfers between devices, shards(): lax.all_gather(lax.all_to_all(taken_rows.reshape(sp_count, capacity, norm...  39.8 us
    all_to_all x2, starting transfers between devices, sum_at_owner(): lax.all_to_all(cut_along(shard, dim, peers), axis, 0, 0, tiled=True)  16.3 us
    all_to_all x1, waiting for transfers between devices, shards(): lax.all_to_all(summed.astype(jnp.bfloat16), SP, split_axis=0, concat_axis...  9.85 us
    all_to_all x1, starting transfers between devices, shards(): lax.all_to_all(summed.astype(jnp.bfloat16), SP, split_axis=0, concat_axis...  9.62 us
  transfers between devices with their start and end apart: 7, of which 7 were waited for; matrix products, arithmetic and copies ran while one was open for 1% of the time, Pallas kernels for 0%

commit v1 on v0

v1 whole, which is shorter than its diff:
```python
import functools

import jax
import jax.numpy as jnp
from jax import lax
from jax.experimental import pallas as pl
from jax.experimental.pallas import tpu as pltpu
from jax.sharding import Mesh
from jax.sharding import PartitionSpec as P

SP = ("z", "x")
TP = ("y", "c")
INTERPRET = False

norm_eps = 1e-06
masked_score = -1e30
extra_rows = 16
lane = 128


def split_three(full):
    first = lax.reduce_precision(full, 8, 7)
    second = lax.reduce_precision(full - first, 8, 7)
    third = lax.reduce_precision(full - first - second, 8, 7)
    return [part.astype(jnp.bfloat16) for part in (first, second, third)]


def sent_to_all(shard, axis):
    copies = jnp.broadcast_to(shard, (lax.axis_size(axis), *shard.shape))
    return lax.all_to_all(copies, axis, split_axis=0, concat_axis=0, tiled=True)


def swapped(shard):
    return lax.ppermute(shard, "c", [(0, 1), (1, 0)])


def attend_kernel(head_count, head_width, place_ref, kv_ref, *refs):
    x_count = len(refs) - 4
    query_refs = refs[:x_count]
    out_ref, query_scratch, sum_scratch, peak_scratch = refs[x_count:]
    tokens = kv_ref.shape[2]
    deep = head_width + extra_rows
    z_place, x_place = place_ref[0], place_ref[1]
    row = lax.broadcasted_iota(jnp.int32, (extra_rows, tokens), 0)
    minus = jnp.where(row < 3, -1.0, 0.0).astype(jnp.bfloat16)
    ones = jnp.ones((extra_rows, tokens), jnp.bfloat16)
    for head in range(head_count):
        for shift in range(x_count):
            chain = head * x_count + shift
            query_scratch[chain, :head_width] = query_refs[shift][
                head * head_width : (head + 1) * head_width
            ]
            query_scratch[chain, head_width:] = minus
            sum_scratch[chain] = jnp.zeros((deep, tokens), jnp.float32)
            peak_scratch[chain] = jnp.full((8, tokens), masked_score, jnp.float32)

    def one(chain, key_rows, value_rows, masked):
        scores = lax.dot_general(
            key_rows,
            query_scratch[chain],
            (((0,), (0,)), ((), ())),
            preferred_element_type=jnp.float32,
        )
        if masked:
            key_place = lax.broadcasted_iota(jnp.int32, scores.shape, 0)
            query_place = lax.broadcasted_iota(jnp.int32, scores.shape, 1)
            scores = jnp.where(key_place <= query_place, scores, masked_score)
        old_peak = peak_scratch[chain, :1]
        new_peak = jnp.maximum(old_peak, jnp.max(scores, axis=0, keepdims=True))
        weights = jnp.exp(scores - new_peak).astype(jnp.bfloat16)
        shrink = jnp.exp(old_peak - new_peak)
        sum_scratch[chain] = sum_scratch[chain] * shrink + jnp.dot(
            value_rows, weights, preferred_element_type=jnp.float32
        )
        peak_scratch[chain] = jnp.broadcast_to(new_peak, (8, tokens))

    def loaded(z_key, head):
        key_rows = kv_ref[z_key, head * deep : (head + 1) * deep]
        value_first = head_count * deep + head * head_width
        value_rows = kv_ref[z_key, value_first : value_first + head_width]
        return key_rows, jnp.concatenate([value_rows, ones], axis=0)

    def earlier(z_key, carry):
        for head in range(head_count):
            key_rows, value_rows = loaded(z_key, head)
            for shift in range(x_count):
                one(head * x_count + shift, key_rows, value_rows, False)
        return carry

    lax.fori_loop(0, z_place, earlier, 0)
    for head in range(head_count):
        key_rows, value_rows = loaded(z_place, head)
        one(head * x_count, key_rows, value_rows, True)
    for shift in range(1, x_count):

        @pl.when(x_place < shift)
        def _():
            for head in range(head_count):
                key_rows, value_rows = loaded(z_place, head)
                one(head * x_count + shift, key_rows, value_rows, False)

    for shift in range(x_count):
        target = lax.rem(x_place + x_count - shift, x_count)
        stats = jnp.zeros((extra_rows, tokens), jnp.float32)
        for head in range(head_count):
            chain = head * x_count + shift
            out_ref[target, head * head_width : (head + 1) * head_width] = sum_scratch[
                chain, :head_width
            ].astype(jnp.bfloat16)
            place = head * 6
            for full in (peak_scratch[chain, :1], sum_scratch[chain, head_width : head_width + 1]):
                for _ in range(3):
                    part = full.astype(jnp.bfloat16).astype(jnp.float32)
                    full = full - part
                    stats = jnp.where(row == place, part, stats)
                    place += 1
        out_ref[target, head_count * head_width :] = stats.astype(jnp.bfloat16)


def project_kernel(head_count, head_width, place_ref, parts_ref, weight_ref, mine_ref, other_ref, full_ref):
    x_count = parts_ref.shape[0]
    tp_half = mine_ref.shape[0]
    width = head_count * head_width
    core = place_ref[2]
    rows = []
    for head in range(head_count):
        peaks, totals = [], []
        for part in range(x_count):
            stats = parts_ref[part, width : width + extra_rows].astype(jnp.float32)
            base = head * 6
            peaks.append(stats[base : base + 1] + stats[base + 1 : base + 2] + stats[base + 2 : base + 3])
            totals.append(
                stats[base + 3 : base + 4] + stats[base + 4 : base + 5] + stats[base + 5 : base + 6]
            )
        top = functools.reduce(jnp.maximum, peaks)
        factors = [jnp.exp(peak - top) for peak in peaks]
        total = sum(factor * amount for factor, amount in zip(factors, totals))
        summed = sum(
            parts_ref[part, head * head_width : (head + 1) * head_width].astype(jnp.float32)
            * factors[part]
            for part in range(x_count)
        )
        rows.append((summed / total).astype(jnp.bfloat16))
    attended = jnp.concatenate(rows, axis=0)
    full_ref[...] = lax.dot_general(
        attended, weight_ref[...], (((0,), (0,)), ((), ())), preferred_element_type=jnp.float32
    ).astype(jnp.bfloat16)
    for block in range(tp_half):
        own = pl.multiple_of((block * 2 + core) * lane, lane)
        far = pl.multiple_of((block * 2 + 1 - core) * lane, lane)
        mine_ref[block] = full_ref[:, pl.ds(own, lane)]
        other_ref[block] = full_ref[:, pl.ds(far, lane)]


def expert_kernel(place_ref, own_ref, far_ref, gain_ref, gate_ref, up_ref, down_ref, mine_ref, other_ref, rows_ref, full_ref):
    core = place_ref[2]
    blocks = own_ref.shape[0]
    width = rows_ref.shape[1]
    squares = jnp.zeros(own_ref.shape[1:], jnp.float32)
    for block in range(blocks):
        for source in (own_ref, far_ref):
            values = source[block].astype(jnp.float32)
            squares = squares + values * values
    scale = lax.rsqrt(jnp.sum(squares, axis=1, keepdims=True) / width + norm_eps)
    for block in range(blocks):
        for source, side in ((own_ref, core), (far_ref, 1 - core)):
            index = block * 2 + side
            values = source[block].astype(jnp.float32) * scale * gain_ref[index]
            rows_ref[:, pl.ds(pl.multiple_of(index * lane, lane), lane)] = values.astype(jnp.bfloat16)
    gate = jnp.dot(rows_ref[...], gate_ref[...], preferred_element_type=jnp.float32)
    up = jnp.dot(rows_ref[...], up_ref[...], preferred_element_type=jnp.float32)
    hidden = (gate / (1.0 + jnp.exp(-gate)) * up).astype(jnp.bfloat16)
    full_ref[...] = jnp.dot(hidden, down_ref[...], preferred_element_type=jnp.float32).astype(
        jnp.bfloat16
    )
    for block in range(blocks):
        own = pl.multiple_of((block * 2 + core) * lane, lane)
        far = pl.multiple_of((block * 2 + 1 - core) * lane, lane)
        mine_ref[block] = full_ref[:, pl.ds(own, lane)]
        other_ref[block] = full_ref[:, pl.ds(far, lane)]


def shards(
    residual,
    queries,
    keys,
    values,
    forget_cache,
    out_weight,
    norm_gain,
    routes,
    route_weight,
    gate_weight,
    up_weight,
    down_weight,
):
    z_count, x_count, y_count = (lax.axis_size(axis) for axis in ("z", "x", "y"))
    sp_count = z_count * x_count
    token_count, local_width = residual.shape
    model_width = norm_gain.shape[0]
    head_count = forget_cache.shape[0]
    head_width = queries.shape[0] // head_count
    top_count = routes.shape[1]
    capacity = max(2, token_count * top_count * 5 // (4 * sp_count))
    slot_total = sp_count * capacity
    bf16, f32 = jnp.bfloat16, jnp.float32
    place = jnp.stack(
        [lax.axis_index("z"), lax.axis_index("x"), lax.axis_index("c"), lax.axis_index("y")]
    ).astype(jnp.int32)
    smem = pl.BlockSpec(memory_space=pltpu.SMEM)
    vmem = pl.BlockSpec(memory_space=pltpu.VMEM)

    gates = jnp.stack(split_three(forget_cache), axis=1)
    gates = jnp.pad(gates, ((0, 0), (0, extra_rows - 3), (0, 0)))
    key_rows = jnp.concatenate([keys.reshape(head_count, head_width, token_count), gates], axis=1)
    message = jnp.concatenate([key_rows.reshape(-1, token_count), values], axis=0)
    gathered = sent_to_all(message, "z")
    scaled = queries * jnp.asarray(head_width ** (-0.5), bf16)
    query_list = [scaled] + [
        lax.ppermute(scaled, "x", [(i, (i + shift) % x_count) for i in range(x_count)])
        for shift in range(1, x_count)
    ]
    chains = head_count * x_count
    deep = head_width + extra_rows
    part_rows = head_count * head_width + extra_rows
    parts = pl.pallas_call(
        functools.partial(attend_kernel, head_count, head_width),
        out_shape=jax.ShapeDtypeStruct((x_count, part_rows, token_count), bf16),
        in_specs=[smem] + [vmem] * (1 + x_count),
        out_specs=vmem,
        scratch_shapes=[
            pltpu.VMEM((chains, deep, token_count), bf16),
            pltpu.VMEM((chains, deep, token_count), f32),
            pltpu.VMEM((chains, 8, token_count), f32),
        ],
        name="attend",
        interpret=INTERPRET,
    )(place, gathered, *query_list)

    expert_ids = jnp.arange(sp_count, dtype=jnp.int32)
    chosen = routes[:, :, None] == expert_ids
    named = jnp.any(chosen, axis=1)
    token_ids = jnp.arange(token_count, dtype=jnp.int32)
    before = (token_ids[None, :] < token_ids[:, None]).astype(bf16)
    rank = jnp.dot(before, named.astype(bf16), preferred_element_type=f32).astype(jnp.int32)
    slot_ids = jnp.arange(capacity, dtype=jnp.int32)
    taken = (named.T[:, None, :] & (rank.T[:, None, :] == slot_ids[:, None])).astype(bf16)
    taken = taken.reshape(slot_total, token_count)
    share = jnp.sum(jnp.where(chosen, route_weight[:, :, None], 0.0), axis=1)
    share_first = lax.reduce_precision(share, 8, 7)
    share_rest = (share - share_first).astype(bf16)

    def spread(weights):
        return jnp.where(
            rank[:, :, None] == slot_ids, weights.astype(bf16)[:, :, None], jnp.zeros((), bf16)
        ).reshape(token_count, slot_total)

    give_first, give_rest = spread(share_first), spread(share_rest)

    received = lax.all_to_all(parts, "x", split_axis=0, concat_axis=0, tiled=True)
    half = jax.ShapeDtypeStruct((y_count, token_count, local_width), bf16)
    mine, other = pl.pallas_call(
        functools.partial(project_kernel, head_count, head_width),
        out_shape=(half, half),
        in_specs=[smem, vmem, vmem],
        out_specs=(vmem, vmem),
        scratch_shapes=[pltpu.VMEM((token_count, model_width), bf16)],
        name="project",
        interpret=INTERPRET,
    )(place, received, out_weight)
    paired = (mine.astype(f32) + swapped(other).astype(f32)).astype(bf16)
    pieces = lax.all_to_all(paired, "y", split_axis=0, concat_axis=0, tiled=True)
    head_sum = jnp.sum(pieces.astype(f32), axis=0)
    stream = (residual.astype(f32) + head_sum).astype(bf16)

    sent = jnp.dot(taken, stream, preferred_element_type=f32).astype(bf16)
    arrived = lax.all_to_all(
        sent.reshape(sp_count, capacity, local_width), SP, split_axis=0, concat_axis=0, tiled=True
    ).reshape(slot_total, local_width)
    own = sent_to_all(arrived, "y")
    far = swapped(own)
    row_steps = 2 if slot_total % 32 == 0 else 1
    row_block = slot_total // row_steps
    hidden_units = gate_weight.shape[2]
    row_spec = pl.BlockSpec((y_count, row_block, local_width), lambda i: (0, i, 0))
    half = jax.ShapeDtypeStruct((y_count, slot_total, local_width), bf16)
    mine, other = pl.pallas_call(
        expert_kernel,
        grid=(row_steps,),
        out_shape=(half, half),
        in_specs=[
            smem,
            row_spec,
            row_spec,
            pl.BlockSpec((2 * y_count, 1, lane), lambda i: (0, 0, 0)),
            pl.BlockSpec((model_width, hidden_units), lambda i: (0, 0)),
            pl.BlockSpec((model_width, hidden_units), lambda i: (0, 0)),
            pl.BlockSpec((hidden_units, model_width), lambda i: (0, 0)),
        ],
        out_specs=(row_spec, row_spec),
        scratch_shapes=[
            pltpu.VMEM((row_block, model_width), bf16),
            pltpu.VMEM((row_block, model_width), bf16),
        ],
        name="expert",
        interpret=INTERPRET,
    )(
        place,
        own,
        far,
        norm_gain.reshape(2 * y_count, 1, lane),
        gate_weight[0],
        up_weight[0],
        down_weight[0],
    )
    paired = (mine.astype(f32) + swapped(other).astype(f32)).astype(bf16)
    pieces = lax.all_to_all(paired, "y", split_axis=0, concat_axis=0, tiled=True)
    expert_out = jnp.sum(pieces.astype(f32), axis=0).astype(bf16)
    back = lax.all_to_all(
        expert_out.reshape(sp_count, capacity, local_width), SP, split_axis=0, concat_axis=0, tiled=True
    ).reshape(slot_total, local_width)
    mixture = jnp.dot(give_first, back, preferred_element_type=f32) + jnp.dot(
        give_rest, back, preferred_element_type=f32
    )
    return (stream.astype(f32) + mixture).astype(bf16)


def solution(mesh):
    sp_count, tp_count = mesh.shape["sp"], mesh.shape["tp"]
    x_count = 4 if sp_count % 8 == 0 else 2
    finer = Mesh(
        mesh.devices.reshape(sp_count // x_count, x_count, tp_count // 2, 2), ("z", "x", "y", "c")
    )
    in_specs = (
        P(SP, TP),
        P(TP, SP),
        P(TP, SP),
        P(TP, SP),
        P(TP, SP),
        P(TP, None),
        P(),
        P(SP, None),
        P(SP, None),
        P(SP, None, TP),
        P(SP, None, TP),
        P(SP, TP, None),
    )
    return jax.shard_map(
        shards, mesh=finer, in_specs=in_specs, out_specs=P(SP, TP), check_vma=False
    )
```

time: 363 us -> 238 us (0.66)
  waiting for transfers between devices: 185 us -> 55.8 us
  Pallas kernels: 0 us -> 16.1 us
  starting transfers between devices: 29.4 us -> 43.7 us
  between operations: 13.4 us -> 0.27 us
  local copies, waits for them, and re-layouts: 17.1 us -> 4.59 us
  blocking collectives: 100 us -> 108 us
  matrix products: 6.94 us -> 1.72 us
    all_gather x3 -> x0, waiting for transfers between devices: 84.6 us -> none  [the longest x2 44.9 us: gathered_by_axis(): out = lax.all_gather(out, axes[number], axis=dim, tiled=True)]
    all_to_all x3 -> x2, waiting for transfers between devices: 94.1 us -> 27.7 us  [the longest x1 17.3 us: shards(): lax.all_to_all(paired, 'y', split_axis=0, concat_axis=0, tiled=True)]
    all_to_all x1 -> x4, blocking collectives: 42.5 us -> 108 us  [the longest x1 37.2 us: shards(): lax.all_to_all(paired, 'y', split_axis=0, concat_axis=0, tiled=True)]
    all_gather x4 -> x0, blocking collectives: 57.9 us -> none  [gathered_by_axis(): out = lax.all_gather(out, axes[number], axis=dim, tiled=True)]
    ppermute x0 -> x6, starting transfers between devices: none -> 21.7 us  [the longest x3 11.2 us: swapped(): return lax.ppermute(shard, 'c', [(0, 1), (1, 0)])]
    pallas_call x0 -> x3, Pallas kernels: none -> 16.1 us  [the longest x1 8.35 us: shards(): pl.pallas_call(expert_kernel, grid=(row_steps,), out_shape=(half, half),...]
    all_to_all x3 -> x2, starting transfers between devices: 25.9 us -> 11 us  [the longest x1 6.82 us: shards(): lax.all_to_all(paired, 'y', split_axis=0, concat_axis=0, tiled=True)]
    all_to_all x1, waiting for transfers between devices: 6.39 us -> 19.2 us  [sent_to_all(): return lax.all_to_all(copies, axis, split_axis=0, concat_axis=0, tiled=True)]
  transfers between devices with their start and end apart: 7 -> 9, of which waited for: 7 -> 7; matrix products, arithmetic and copies ran while one was open for 1% -> 0% of each run, Pallas kernels for 0% -> 0%
where the time goes in v1:
time: 238 us; the launch traced here: 237 us
  blocking collectives  108 us (45%)
  waiting for transfers between devices  55.8 us (23%)
  starting transfers between devices  43.7 us (18%)
  Pallas kernels  16.1 us (7%)
  other arithmetic  6.92 us (3%)
  local copies, waits for them, and re-layouts  4.59 us (2%)
    all_to_all x1, blocking collectives, shards(): lax.all_to_all(paired, 'y', split_axis=0, concat_axis=0, tiled=True)  37.2 us
    all_to_all x1, blocking collectives, sent_to_all(): return lax.all_to_all(copies, axis, split_axis=0, concat_axis=0, tiled=True)  33.9 us
    all_to_all x1, blocking collectives, shards(): lax.all_to_all(sent.reshape(sp_count, capacity, local_width), SP, split_a...  26 us
    all_to_all x1, waiting for transfers between devices, sent_to_all(): return lax.all_to_all(copies, axis, split_axis=0, concat_axis=0, tiled=True)  19.2 us
    all_to_all x1, waiting for transfers between devices, shards(): lax.all_to_all(paired, 'y', split_axis=0, concat_axis=0, tiled=True)  17.3 us
    ppermute x3, starting transfers between devices, swapped(): return lax.ppermute(shard, 'c', [(0, 1), (1, 0)])  11.2 us
    all_to_all x1, starting transfers between devices, sent_to_all(): return lax.all_to_all(copies, axis, split_axis=0, concat_axis=0, tiled=True)  11 us
    all_to_all x1, blocking collectives, shards(): lax.all_to_all(parts, 'x', split_axis=0, concat_axis=0, tiled=True)  10.8 us
  transfers between devices with their start and end apart: 9, of which 7 were waited for; matrix products, arithmetic and copies ran while one was open for 0% of the time, Pallas kernels for 0%

profile of v1, /device:TPU:1, one launch (start us, length us, event | category | flops | bytes accessed | tf_op | source)
XLA Modules:
  0.0 237.2 jit_solution(471608747635432368)
XLA Ops:
  0.0 0.7 fusion.24
  0.7 0.9 fusion.19
  1.6 0.8 pad_maximum_fusion
  2.4 1.1 broadcast_in_dim.49
  3.5 11.0 %all-to-all-start = ((bf16[8,288,256]{2,1,0:T(8,128)(2,1)}), bf16[8,288,256]{2,1,0:T(8,128)(2,1)S(1)}, u32[]{:S(2)}, u32[]{:S(2)}) async-start(bf16[8,288,256]{2,1,0:T(8,128)(2,1)} %broadcast_in_dim.49), calls=%async_computation | async-start | bytes 2359296 | tf_op jit(solution)/shard_map/all_to_all | solution.py:30
  14.5 0.0 copy-start.3
  14.6 3.1 %collective-permute-start = (bf16[128,256]{1,0:T(8,128)(2,1)S(1)}, bf16[128,256]{1,0:T(8,128)(2,1)S(1)}, u32[]{:S(2)}, u32[]{:S(2)}) collective-permute-start(bf16[128,256]{1,0:T(8,128)(2,1)S(1)} %broadcast_multiply_fusion.refs_0_), channel_id=1, source_target_pairs={{0,16},{16,32},{32,48},{48,0},{1,17},{17,33},{33,49},{49,1},{2,18}... | collective-permute-start | bytes 196616 | tf_op jit(solution)/shard_map/ppermute | solution.py:220
  17.7 4.4 %collective-permute-start.1 = (bf16[128,256]{1,0:T(8,128)(2,1)S(1)}, bf16[128,256]{1,0:T(8,128)(2,1)S(1)}, u32[]{:S(2)}, u32[]{:S(2)}) collective-permute-start(bf16[128,256]{1,0:T(8,128)(2,1)S(1)} %broadcast_multiply_fusion.refs_0_), channel_id=1, source_target_pairs={{0,32},{16,48},{32,0},{48,16},{1,33},{17,49},{33,1},{49,17},{2,34}... | collective-permute-start | bytes 196616 | tf_op jit(solution)/shard_map/ppermute | solution.py:220
  22.0 3.1 %collective-permute-start.2 = (bf16[128,256]{1,0:T(8,128)(2,1)S(1)}, bf16[128,256]{1,0:T(8,128)(2,1)S(1)}, u32[]{:S(2)}, u32[]{:S(2)}) collective-permute-start(bf16[128,256]{1,0:T(8,128)(2,1)S(1)} %broadcast_multiply_fusion.refs_0_), channel_id=1, source_target_pairs={{0,48},{16,0},{32,16},{48,32},{1,49},{17,1},{33,17},{49,33},{2,50}... | collective-permute-start | bytes 196616 | tf_op jit(solution)/shard_map/ppermute | solution.py:220
  25.1 0.6 pad_add_fusion.place_ref
  25.7 0.0 collective-permute-done.1.refs_2_
  25.7 1.6 collective-permute-done.2.refs_3_
  27.4 19.2 %all-to-all-done.kv_ref = bf16[8,288,256]{2,1,0:T(8,128)(2,1)S(1)} async-done(((bf16[8,288,256]{2,1,0:T(8,128)(2,1)}), bf16[8,288,256]{2,1,0:T(8,128)(2,1)S(1)}, u32[]{:S(2)}, u32[]{:S(2)}) %all-to-all-start) | async-done | bytes 1179680 | tf_op jit(solution)/shard_map/all_to_all | solution.py:30
  46.6 1.0 copy-done.1
  47.6 5.0 %attend.1 = bf16[4,144,256]{2,1,0:T(8,128)(2,1)} custom-call(s32[4]{0:T(128)} %pad_add_fusion.place_ref, bf16[8,288,256]{2,1,0:T(8,128)(2,1)} %copy-done.1, bf16[128,256]{1,0:T(8,128)(2,1)} %copy-done.3, bf16[128,256]{1,0:T(8,128)(2,1)} %copy-done.5, bf16[128,256]{1,0:T(8,128)(2,1)} %copy-done.6, bf16[128,256]{1,0:T(8,128)(2,1)} %copy-done.7), custom_call_target="tpu_custom_call" | custom-call | tf_op jit(solution)/shard_map/attend/pallas_call | solution.py:226
  52.6 10.8 %all_to_all.35.parts_ref = bf16[4,144,256]{2,1,0:T(8,128)(2,1)} all-to-all(bf16[4,144,256]{2,1,0:T(8,128)(2,1)} %attend.1), channel_id=1, replica_groups=mesh['z'=8,'x'=4,'y'=8,'c'=2] {'x'}, dimensions={0} | all-to-all | bytes 589824 | tf_op jit(solution)/shard_map/all_to_all | solution.py:260
  63.4 2.8 %project.1 = (bf16[8,256,128]{2,1,0:T(8,128)(2,1)}, bf16[8,256,128]{2,1,0:T(8,128)(2,1)}) custom-call(s32[4]{0:T(128)} %pad_add_fusion.place_ref, bf16[4,144,256]{2,1,0:T(8,128)(2,1)} %all_to_all.35.parts_ref, bf16[128,2048]{1,0:T(8,128)(2,1)} %weight_ref.1), custom_call_target="tpu_custom_call" | custom-call | tf_op jit(solution)/shard_map/project/pallas_call | solution.py:262
  66.2 3.2 %collective-permute-start.3 = (bf16[8,256,128]{2,1,0:T(8,128)(2,1)}, bf16[8,256,128]{2,1,0:T(8,128)(2,1)S(1)}, u32[]{:S(2)}, u32[]{:S(2)}) collective-permute-start(bf16[8,256,128]{2,1,0:T(8,128)(2,1)} %get-tuple-element.10), channel_id=1, source_target_pairs={{0,1},{1,0},{2,3},{3,2},{4,5},{5,4},{6,7},{7,6},{8,9},{9,8},{10,11... | collective-permute-start | bytes 1572872 | tf_op jit(solution)/shard_map/ppermute | solution.py:34
  69.4 1.7 collective-permute-done.3
  71.2 2.0 add_convert_fusion.1
  73.2 6.8 %all-to-all-start.2 = ((bf16[8,256,128]{2,1,0:T(8,128)(2,1)}), bf16[8,256,128]{2,1,0:T(8,128)(2,1)S(1)}, u32[]{:S(2)}, u32[]{:S(2)}) async-start(bf16[8,256,128]{2,1,0:T(8,128)(2,1)} %add_convert_fusion.1), calls=%async_computation.2 | async-start | bytes 1048576 | tf_op jit(solution)/shard_map/all_to_all | solution.py:272
  80.0 0.2 convolution_convert_fusion.1
  80.2 0.1 eq.59
  80.3 0.0 copy-start.4
  80.3 0.1 eq.60
  80.3 0.1 and.15
  80.4 0.1 and.16
  80.5 0.1 eq.62
  80.6 17.3 %all-to-all-done.2 = bf16[8,256,128]{2,1,0:T(8,128)(2,1)S(1)} async-done(((bf16[8,256,128]{2,1,0:T(8,128)(2,1)}), bf16[8,256,128]{2,1,0:T(8,128)(2,1)S(1)}, u32[]{:S(2)}, u32[]{:S(2)}) %all-to-all-start.2) | async-done | bytes 524320 | tf_op jit(solution)/shard_map/all_to_all | solution.py:272
  97.9 0.1 convert_reduce_fusion
  98.0 0.3 convolution_convert_fusion
  98.4 26.0 %all_to_all.36 = bf16[32,20,128]{2,1,0:T(8,128)(2,1)S(1)} all-to-all(bf16[32,20,128]{2,1,0:T(8,128)(2,1)S(1)} %reshape.40), channel_id=1, replica_groups=mesh['z'=8,'x'=4,'y'=8,'c'=2] {'z','x'}, dimensions={0} | all-to-all | bytes 327680 | tf_op jit(solution)/shard_map/all_to_all | solution.py:277
  124.5 0.2 broadcast_in_dim.54
  124.7 33.9 %all_to_all.37.own_ref = bf16[8,640,128]{2,1,0:T(8,128)(2,1)S(1)} all-to-all(bf16[8,640,128]{2,1,0:T(8,128)(2,1)S(1)} %broadcast_in_dim.54), channel_id=1, replica_groups=mesh['z'=8,'x'=4,'y'=8,'c'=2] {'y'}, dimensions={0} | all-to-all | bytes 2621440 | tf_op jit(solution)/shard_map/all_to_all | solution.py:30
  158.6 5.7 %collective-permute-start.4 = (bf16[8,640,128]{2,1,0:T(8,128)(2,1)S(1)}, bf16[8,640,128]{2,1,0:T(8,128)(2,1)S(1)}, u32[]{:S(2)}, u32[]{:S(2)}) collective-permute-start(bf16[8,640,128]{2,1,0:T(8,128)(2,1)S(1)} %all_to_all.37.own_ref), channel_id=1, source_target_pairs={{0,1},{1,0},{2,3},{3,2},{4,5},{5,4},{6,7},{7,6},{8,9},{9,8},{10,11... | collective-permute-start | bytes 3932168 | tf_op jit(solution)/shard_map/ppermute | solution.py:34
  164.3 2.6 %collective-permute-done.4.far_ref = bf16[8,640,128]{2,1,0:T(8,128)(2,1)S(1)} collective-permute-done((bf16[8,640,128]{2,1,0:T(8,128)(2,1)S(1)}, bf16[8,640,128]{2,1,0:T(8,128)(2,1)S(1)}, u32[]{:S(2)}, u32[]{:S(2)}) %collective-permute-start.4) | collective-permute-done | bytes 1310752 | tf_op jit(solution)/shard_map/ppermute | solution.py:34
  166.9 1.1 copy-done.2
  168.0 8.3 %expert.1 = (bf16[8,640,128]{2,1,0:T(8,128)(2,1)}, bf16[8,640,128]{2,1,0:T(8,128)(2,1)}) custom-call(s32[4]{0:T(128)} %pad_add_fusion.place_ref, bf16[8,640,128]{2,1,0:T(8,128)(2,1)} %copy-done, bf16[8,640,128]{2,1,0:T(8,128)(2,1)} %copy-done.2, f32[16,1,128]{2,1,0:T(1,128)} %bitcast.36, bf16[2048,256]{1,0:T(8,128)(2,1)} %bitcast.29, ...), custom_call_target="tpu_custom_call" | custom-call | tf_op jit(solution)/shard_map/expert/pallas_call | solution.py:287
  176.3 2.3 collective-permute-start.5
  178.6 2.9 %collective-permute-done.5 = bf16[8,640,128]{2,1,0:T(8,128)(2,1)S(1)} collective-permute-done((bf16[8,640,128]{2,1,0:T(8,128)(2,1)}, bf16[8,640,128]{2,1,0:T(8,128)(2,1)S(1)}, u32[]{:S(2)}, u32[]{:S(2)}) %collective-permute-start.5) | collective-permute-done | bytes 1310752 | tf_op jit(solution)/shard_map/ppermute | solution.py:34
  181.5 1.7 add_convert_fusion
  183.1 37.2 %all_to_all.38 = bf16[8,640,128]{2,1,0:T(8,128)(2,1)S(1)} all-to-all(bf16[8,640,128]{2,1,0:T(8,128)(2,1)S(1)} %add_convert_fusion), channel_id=1, replica_groups=mesh['z'=8,'x'=4,'y'=8,'c'=2] {'y'}, dimensions={0} | all-to-all | bytes 2621440 | tf_op jit(solution)/shard_map/all_to_all | solution.py:317
  220.4 0.2 reduce_sum.32
  220.6 0.7 reshape.43
  221.3 4.2 %all-to-all-start.6 = ((bf16[32,20,128]{2,1,0:T(8,128)(2,1)}), bf16[32,20,128]{2,1,0:T(8,128)(2,1)S(1)}, u32[]{:S(2)}, u32[]{:S(2)}) async-start(bf16[32,20,128]{2,1,0:T(8,128)(2,1)} %reshape.43), calls=%async_computation.6 | async-start | bytes 393216 | tf_op jit(solution)/shard_map/all_to_all | solution.py:319
  225.5 10.4 %all-to-all-done.6 = bf16[32,20,128]{2,1,0:T(8,128)(2,1)S(1)} async-done(((bf16[32,20,128]{2,1,0:T(8,128)(2,1)}), bf16[32,20,128]{2,1,0:T(8,128)(2,1)S(1)}, u32[]{:S(2)}, u32[]{:S(2)}) %all-to-all-start.6) | async-done | bytes 163872 | tf_op jit(solution)/shard_map/all_to_all | solution.py:319
  235.9 0.3 convolution_bitcast_fusion
  236.2 0.9 fusion.2
  (28 shorter events, 0.2 us)
Async XLA Ops:
  3.5 11.0 %copy-start.8 = (bf16[128,256]{1,0:T(8,128)(2,1)S(1)}, bf16[128,256]{1,0:T(8,128)(2,1)}, u32[]{:S(2)}) copy-start(bf16[128,256]{1,0:T(8,128)(2,1)} %param.13) | copy-start | bytes 196612
  3.5 43.0 %all-to-all-start = ((bf16[8,288,256]{2,1,0:T(8,128)(2,1)}), bf16[8,288,256]{2,1,0:T(8,128)(2,1)S(1)}, u32[]{:S(2)}, u32[]{:S(2)}) async-start(bf16[8,288,256]{2,1,0:T(8,128)(2,1)} %broadcast_in_dim.49), calls=%async_computation | async-start | bytes 2359296 | tf_op jit(solution)/shard_map/all_to_all | solution.py:30
  14.5 32.0 %copy-start.3 = (bf16[128,256]{1,0:T(8,128)(2,1)}, bf16[128,256]{1,0:T(8,128)(2,1)S(1)}, u32[]{:S(2)}) copy-start(bf16[128,256]{1,0:T(8,128)(2,1)S(1)} %broadcast_multiply_fusion.refs_0_) | copy-start | bytes 196612
  14.6 11.1 %collective-permute-start = (bf16[128,256]{1,0:T(8,128)(2,1)S(1)}, bf16[128,256]{1,0:T(8,128)(2,1)S(1)}, u32[]{:S(2)}, u32[]{:S(2)}) collective-permute-start(bf16[128,256]{1,0:T(8,128)(2,1)S(1)} %broadcast_multiply_fusion.refs_0_), channel_id=1, source_target_pairs={{0,16},{16,32},{32,48},{48,0},{1,17},{17,33},{33,49},{49,1},{2,18}... | collective-permute-start | bytes 196616 | tf_op jit(solution)/shard_map/ppermute | solution.py:220
  17.7 8.0 %collective-permute-start.1 = (bf16[128,256]{1,0:T(8,128)(2,1)S(1)}, bf16[128,256]{1,0:T(8,128)(2,1)S(1)}, u32[]{:S(2)}, u32[]{:S(2)}) collective-permute-start(bf16[128,256]{1,0:T(8,128)(2,1)S(1)} %broadcast_multiply_fusion.refs_0_), channel_id=1, source_target_pairs={{0,32},{16,48},{32,0},{48,16},{1,33},{17,49},{33,1},{49,17},{2,34}... | collective-permute-start | bytes 196616 | tf_op jit(solution)/shard_map/ppermute | solution.py:220
  22.0 5.3 %collective-permute-start.2 = (bf16[128,256]{1,0:T(8,128)(2,1)S(1)}, bf16[128,256]{1,0:T(8,128)(2,1)S(1)}, u32[]{:S(2)}, u32[]{:S(2)}) collective-permute-start(bf16[128,256]{1,0:T(8,128)(2,1)S(1)} %broadcast_multiply_fusion.refs_0_), channel_id=1, source_target_pairs={{0,48},{16,0},{32,16},{48,32},{1,49},{17,1},{33,17},{49,33},{2,50}... | collective-permute-start | bytes 196616 | tf_op jit(solution)/shard_map/ppermute | solution.py:220
  25.7 20.9 %copy-start.5 = (bf16[128,256]{1,0:T(8,128)(2,1)}, bf16[128,256]{1,0:T(8,128)(2,1)S(1)}, u32[]{:S(2)}) copy-start(bf16[128,256]{1,0:T(8,128)(2,1)S(1)} %collective-permute-done.refs_1_) | copy-start | bytes 196612
  25.7 20.9 %copy-start.6 = (bf16[128,256]{1,0:T(8,128)(2,1)}, bf16[128,256]{1,0:T(8,128)(2,1)S(1)}, u32[]{:S(2)}) copy-start(bf16[128,256]{1,0:T(8,128)(2,1)S(1)} %collective-permute-done.1.refs_2_) | copy-start | bytes 196612
  27.4 19.2 %copy-start.7 = (bf16[128,256]{1,0:T(8,128)(2,1)}, bf16[128,256]{1,0:T(8,128)(2,1)S(1)}, u32[]{:S(2)}) copy-start(bf16[128,256]{1,0:T(8,128)(2,1)S(1)} %collective-permute-done.2.refs_3_) | copy-start | bytes 196612
  46.6 1.0 copy-start.1
  66.2 5.0 %collective-permute-start.3 = (bf16[8,256,128]{2,1,0:T(8,128)(2,1)}, bf16[8,256,128]{2,1,0:T(8,128)(2,1)S(1)}, u32[]{:S(2)}, u32[]{:S(2)}) collective-permute-start(bf16[8,256,128]{2,1,0:T(8,128)(2,1)} %get-tuple-element.10), channel_id=1, source_target_pairs={{0,1},{1,0},{2,3},{3,2},{4,5},{5,4},{6,7},{7,6},{8,9},{9,8},{10,11... | collective-permute-start | bytes 1572872 | tf_op jit(solution)/shard_map/ppermute | solution.py:34
  71.2 8.8 %copy-start.9 = (s32[256,2]{0,1:T(2,128)S(1)}, s32[256,2]{0,1:T(2,128)}, u32[]{:S(2)}) copy-start(s32[256,2]{0,1:T(2,128)} %param.19) | copy-start | bytes 6148
  73.2 24.8 %all-to-all-start.2 = ((bf16[8,256,128]{2,1,0:T(8,128)(2,1)}), bf16[8,256,128]{2,1,0:T(8,128)(2,1)S(1)}, u32[]{:S(2)}, u32[]{:S(2)}) async-start(bf16[8,256,128]{2,1,0:T(8,128)(2,1)} %add_convert_fusion.1), calls=%async_computation.2 | async-start | bytes 1048576 | tf_op jit(solution)/shard_map/all_to_all | solution.py:272
  80.3 17.8 %copy-start.4 = (bf16[256,128]{1,0:T(8,128)(2,1)S(1)}, bf16[256,128]{1,0:T(8,128)(2,1)}, u32[]{:S(2)}) copy-start(bf16[256,128]{1,0:T(8,128)(2,1)} %param.12) | copy-start | bytes 196612
  158.6 8.3 %copy-start = (bf16[8,640,128]{2,1,0:T(8,128)(2,1)}, bf16[8,640,128]{2,1,0:T(8,128)(2,1)S(1)}, u32[]{:S(2)}) copy-start(bf16[8,640,128]{2,1,0:T(8,128)(2,1)S(1)} %all_to_all.37.own_ref) | copy-start | bytes 3932164
  158.6 8.3 %collective-permute-start.4 = (bf16[8,640,128]{2,1,0:T(8,128)(2,1)S(1)}, bf16[8,640,128]{2,1,0:T(8,128)(2,1)S(1)}, u32[]{:S(2)}, u32[]{:S(2)}) collective-permute-start(bf16[8,640,128]{2,1,0:T(8,128)(2,1)S(1)} %all_to_all.37.own_ref), channel_id=1, source_target_pairs={{0,1},{1,0},{2,3},{3,2},{4,5},{5,4},{6,7},{7,6},{8,9},{9,8},{10,11... | collective-permute-start | bytes 3932168 | tf_op jit(solution)/shard_map/ppermute | solution.py:34
  166.9 1.1 copy-start.2
  176.3 5.1 %collective-permute-start.5 = (bf16[8,640,128]{2,1,0:T(8,128)(2,1)}, bf16[8,640,128]{2,1,0:T(8,128)(2,1)S(1)}, u32[]{:S(2)}, u32[]{:S(2)}) collective-permute-start(bf16[8,640,128]{2,1,0:T(8,128)(2,1)} %get-tuple-element.12), channel_id=1, source_target_pairs={{0,1},{1,0},{2,3},{3,2},{4,5},{5,4},{6,7},{7,6},{8,9},{9,8},{10,11... | collective-permute-start | bytes 3932168 | tf_op jit(solution)/shard_map/ppermute | solution.py:34
  220.4 5.1 %copy-start.10 = (f32[256,2]{0,1:T(2,128)S(1)}, f32[256,2]{0,1:T(2,128)}, u32[]{:S(2)}) copy-start(f32[256,2]{0,1:T(2,128)} %param.20) | copy-start | bytes 6148
  221.3 14.7 %all-to-all-start.6 = ((bf16[32,20,128]{2,1,0:T(8,128)(2,1)}), bf16[32,20,128]{2,1,0:T(8,128)(2,1)S(1)}, u32[]{:S(2)}, u32[]{:S(2)}) async-start(bf16[32,20,128]{2,1,0:T(8,128)(2,1)} %reshape.43), calls=%async_computation.6 | async-start | bytes 393216 | tf_op jit(solution)/shard_map/all_to_all | solution.py:319

commit v2 on v1

--- a/solution.py
+++ b/solution.py
@@ -7,6 +7,7 @@
 from jax.experimental.pallas import tpu as pltpu
 from jax.sharding import Mesh
 from jax.sharding import PartitionSpec as P
+
 
 SP = ("z", "x")
 TP = ("y", "c")
@@ -152,32 +153,46 @@
         other_ref[block] = full_ref[:, pl.ds(far, lane)]
 
 
-def expert_kernel(place_ref, own_ref, far_ref, gain_ref, gate_ref, up_ref, down_ref, mine_ref, other_ref, rows_ref, full_ref):
+def expert_kernel(place_ref, rows_in_ref, gain_ref, *refs):
+    sets = (len(refs) - 8) // 3
+    gate_refs, up_refs, down_refs = refs[:sets], refs[sets : 2 * sets], refs[2 * sets : 3 * sets]
+    out_ref, rows_ref, hidden_ref, full_ref, gates, ups, downs, sems = refs[3 * sets :]
     core = place_ref[2]
-    blocks = own_ref.shape[0]
+    blocks = rows_in_ref.shape[0]
     width = rows_ref.shape[1]
-    squares = jnp.zeros(own_ref.shape[1:], jnp.float32)
+    units = gates.shape[2]
+    copies = []
+    for part in range(sets):
+        for kind, (sources, target) in enumerate(((gate_refs, gates), (up_refs, ups), (down_refs, downs))):
+            copy = pltpu.make_async_copy(sources[part], target.at[part], sems.at[kind, part])
+            copy.start()
+            copies.append(copy)
+    squares = jnp.zeros(rows_in_ref.shape[2:], jnp.float32)
     for block in range(blocks):
-        for source in (own_ref, far_ref):
-            values = source[block].astype(jnp.float32)
+        for side in range(2):
+            values = rows_in_ref[block, side].astype(jnp.float32)
             squares = squares + values * values
     scale = lax.rsqrt(jnp.sum(squares, axis=1, keepdims=True) / width + norm_eps)
     for block in range(blocks):
-        for source, side in ((own_ref, core), (far_ref, 1 - core)):
-            index = block * 2 + side
-            values = source[block].astype(jnp.float32) * scale * gain_ref[index]
+        for side, at in ((0, core), (1, 1 - core)):
+            index = block * 2 + at
+            values = rows_in_ref[block, side].astype(jnp.float32) * scale * gain_ref[index]
             rows_ref[:, pl.ds(pl.multiple_of(index * lane, lane), lane)] = values.astype(jnp.bfloat16)
-    gate = jnp.dot(rows_ref[...], gate_ref[...], preferred_element_type=jnp.float32)
-    up = jnp.dot(rows_ref[...], up_ref[...], preferred_element_type=jnp.float32)
-    hidden = (gate / (1.0 + jnp.exp(-gate)) * up).astype(jnp.bfloat16)
-    full_ref[...] = jnp.dot(hidden, down_ref[...], preferred_element_type=jnp.float32).astype(
-        jnp.bfloat16
-    )
+    for part in range(sets):
+        copies[3 * part].wait()
+        gate = jnp.dot(rows_ref[...], gates[part], preferred_element_type=jnp.float32)
+        copies[3 * part + 1].wait()
+        up = jnp.dot(rows_ref[...], ups[part], preferred_element_type=jnp.float32)
+        hidden_ref[:, part * units : (part + 1) * units] = (
+            gate / (1.0 + jnp.exp(-gate)) * up
+        ).astype(jnp.bfloat16)
+        copies[3 * part + 2].wait()
+    full_ref[...] = jnp.dot(
+        hidden_ref[...], downs[...].reshape(sets * units, width), preferred_element_type=jnp.float32
+    ).astype(jnp.bfloat16)
+    out_width = out_ref.shape[2]
     for block in range(blocks):
-        own = pl.multiple_of((block * 2 + core) * lane, lane)
-        far = pl.multiple_of((block * 2 + 1 - core) * lane, lane)
-        mine_ref[block] = full_ref[:, pl.ds(own, lane)]
-        other_ref[block] = full_ref[:, pl.ds(far, lane)]
+        out_ref[block] = full_ref[:, block * out_width : (block + 1) * out_width]
 
 
 def shards(
@@ -220,10 +235,18 @@
         lax.ppermute(scaled, "x", [(i, (i + shift) % x_count) for i in range(x_count)])
         for shift in range(1, x_count)
     ]
+    slice_moves = []
+    for y_from in range(y_count):
+        slice_moves.append((2 * y_from, 2 * ((y_from - 1) % y_count)))
+        slice_moves.append((2 * y_from + 1, 2 * ((y_from + 1) % y_count) + 1))
+    own_set = (gate_weight[0], up_weight[0], down_weight[0])
+    near_set = tuple(lax.ppermute(weight, TP, slice_moves) for weight in own_set)
+    own_swapped = tuple(swapped(weight) for weight in own_set)
+    near_swapped = tuple(swapped(weight) for weight in near_set)
     chains = head_count * x_count
     deep = head_width + extra_rows
     part_rows = head_count * head_width + extra_rows
-    parts = pl.pallas_call(
+    attend = pl.pallas_call(
         functools.partial(attend_kernel, head_count, head_width),
         out_shape=jax.ShapeDtypeStruct((x_count, part_rows, token_count), bf16),
         in_specs=[smem] + [vmem] * (1 + x_count),
@@ -235,7 +258,8 @@
         ],
         name="attend",
         interpret=INTERPRET,
-    )(place, gathered, *query_list)
+    )
+    parts = attend(place, gathered, *query_list)
 
     expert_ids = jnp.arange(sp_count, dtype=jnp.int32)
     chosen = routes[:, :, None] == expert_ids
@@ -270,6 +294,10 @@
     )(place, received, out_weight)
     paired = (mine.astype(f32) + swapped(other).astype(f32)).astype(bf16)
     pieces = lax.all_to_all(paired, "y", split_axis=0, concat_axis=0, tiled=True)
+    pieces, own_swapped, near_set, near_swapped = lax.optimization_barrier(
+        (pieces, own_swapped, near_set, near_swapped)
+    )
+    weight_sets = [own_set, own_swapped, near_set, near_swapped]
     head_sum = jnp.sum(pieces.astype(f32), axis=0)
     stream = (residual.astype(f32) + head_sum).astype(bf16)
 
@@ -277,45 +305,45 @@
     arrived = lax.all_to_all(
         sent.reshape(sp_count, capacity, local_width), SP, split_axis=0, concat_axis=0, tiled=True
     ).reshape(slot_total, local_width)
-    own = sent_to_all(arrived, "y")
-    far = swapped(own)
-    row_steps = 2 if slot_total % 32 == 0 else 1
-    row_block = slot_total // row_steps
+    quarter = slot_total // 4
+    arrived = arrived.reshape(2, 2, quarter, local_width)
+    core = place[2]
+    mine = lax.dynamic_index_in_dim(arrived, core, 1, keepdims=False)
+    other = lax.dynamic_index_in_dim(arrived, 1 - core, 1, keepdims=False)
+    both = jnp.stack([mine, swapped(other)], axis=1)
+    both = jnp.broadcast_to(both, (y_count // 2, *both.shape))
+    rows = lax.all_to_all(
+        both.reshape(y_count, 2, quarter, local_width), "y", split_axis=0, concat_axis=0, tiled=True
+    )
+    weights = [kind[part] for kind in zip(*weight_sets) for part in range(len(weight_sets))]
+    sets = len(weight_sets)
     hidden_units = gate_weight.shape[2]
-    row_spec = pl.BlockSpec((y_count, row_block, local_width), lambda i: (0, i, 0))
-    half = jax.ShapeDtypeStruct((y_count, slot_total, local_width), bf16)
-    mine, other = pl.pallas_call(
+    any_space = pl.BlockSpec(memory_space=pl.ANY)
+    out_rows = pl.pallas_call(
         expert_kernel,
-        grid=(row_steps,),
-        out_shape=(half, half),
-        in_specs=[
-            smem,
-            row_spec,
-            row_spec,
-            pl.BlockSpec((2 * y_count, 1, lane), lambda i: (0, 0, 0)),
-            pl.BlockSpec((model_width, hidden_units), lambda i: (0, 0)),
-            pl.BlockSpec((model_width, hidden_units), lambda i: (0, 0)),
-            pl.BlockSpec((hidden_units, model_width), lambda i: (0, 0)),
-        ],
-        out_specs=(row_spec, row_spec),
+        out_shape=jax.ShapeDtypeStruct((y_count, quarter, 2 * local_width), bf16),
+        in_specs=[smem, vmem, vmem] + [any_space] * (3 * sets),
+        out_specs=vmem,
         scratch_shapes=[
-            pltpu.VMEM((row_block, model_width), bf16),
-            pltpu.VMEM((row_block, model_width), bf16),
+            pltpu.VMEM((quarter, model_width), bf16),
+            pltpu.VMEM((quarter, sets * hidden_units), bf16),
+            pltpu.VMEM((quarter, model_width), bf16),
+            pltpu.VMEM((sets, model_width, hidden_units), bf16),
+            pltpu.VMEM((sets, model_width, hidden_units), bf16),
+            pltpu.VMEM((sets, hidden_units, model_width), bf16),
+            pltpu.SemaphoreType.DMA((3, sets)),
         ],
         name="expert",
         interpret=INTERPRET,
-    )(
-        place,
-        own,
-        far,
-        norm_gain.reshape(2 * y_count, 1, lane),
-        gate_weight[0],
-        up_weight[0],
-        down_weight[0],
-    )
-    paired = (mine.astype(f32) + swapped(other).astype(f32)).astype(bf16)
-    pieces = lax.all_to_all(paired, "y", split_axis=0, concat_axis=0, tiled=True)
-    expert_out = jnp.sum(pieces.astype(f32), axis=0).astype(bf16)
+    )(place, rows, norm_gain.reshape(2 * y_count, 1, lane), *weights)
+    pieces = lax.all_to_all(out_rows, "y", split_axis=0, concat_axis=0, tiled=True)
+    summed = jnp.sum(
+        pieces.reshape(y_count // 2, 2, quarter, 2, local_width).astype(f32), axis=0
+    ).astype(bf16)
+    mine = lax.dynamic_index_in_dim(summed, core, 2, keepdims=False)
+    got = swapped(lax.dynamic_index_in_dim(summed, 1 - core, 2, keepdims=False))
+    first = core == 0
+    expert_out = jnp.stack([jnp.where(first, mine, got), jnp.where(first, got, mine)], axis=1)
     back = lax.all_to_all(
         expert_out.reshape(sp_count, capacity, local_width), SP, split_axis=0, concat_axis=0, tiled=True
     ).reshape(slot_total, local_width)

time: 238 us -> 223 us (0.937)
  blocking collectives: 108 us -> 57.7 us
  starting transfers between devices: 43.7 us -> 86.6 us
  waiting for transfers between devices: 55.8 us -> 48.8 us
    all_to_all x3 -> x2, blocking collectives: 97.2 us -> 47.8 us  [the longest x1 24 us: shards(): lax.all_to_all(out_rows, 'y', split_axis=0, concat_axis=0, tiled=True)]
    all_to_all x0 -> x1, starting transfers between devices: none -> 21 us  [shards(): lax.all_to_all(sent.reshape(sp_count, capacity, local_width), SP, split_a...]
    all_to_all x1, waiting for transfers between devices: 19.2 us -> 1.05 us  [sent_to_all(): return lax.all_to_all(copies, axis, split_axis=0, concat_axis=0, tiled=True)]
    ppermute x3 -> x9, starting transfers between devices: 11.2 us -> 27.6 us  [swapped(): return lax.ppermute(shard, 'c', [(0, 1), (1, 0)])]
    all_to_all x0 -> x1, waiting for transfers between devices: none -> 10.5 us  [shards(): lax.all_to_all(sent.reshape(sp_count, capacity, local_width), SP, split_a...]
    ppermute x0 -> x3, starting transfers between devices: none -> 9.62 us  [shards(): lax.ppermute(weight, TP, slice_moves)]
    ppermute x3, waiting for transfers between devices: 1.66 us -> 7.8 us  [shards(): lax.ppermute(scaled, 'x', [(i, (i + shift) % x_count) for i in range(x_co...]
    ppermute x3 -> x9, waiting for transfers between devices: 7.21 us -> 1.82 us  [swapped(): return lax.ppermute(shard, 'c', [(0, 1), (1, 0)])]
  transfers between devices with their start and end apart: 9 -> 19, of which waited for: 7 -> 9; matrix products, arithmetic and copies ran while one was open for 0% -> 1% of each run, Pallas kernels for 0% -> 4%
where the time goes in v2:
time: 223 us; the launch traced here: 222 us
  starting transfers between devices  86.6 us (39%)
  blocking collectives  57.7 us (26%)
  waiting for transfers between devices  48.8 us (22%)
  Pallas kernels  15.9 us (7%)
  other arithmetic  6.12 us (3%)
  local copies, waits for them, and re-layouts  4.73 us (2%)
    ppermute x9, starting transfers between devices, swapped(): return lax.ppermute(shard, 'c', [(0, 1), (1, 0)])  27.6 us
    all_to_all x1, blocking collectives, shards(): lax.all_to_all(out_rows, 'y', split_axis=0, concat_axis=0, tiled=True)  24 us
    all_to_all x1, blocking collectives, shards(): lax.all_to_all(both.reshape(y_count, 2, quarter, local_width), 'y', split...  23.8 us
    all_to_all x1, starting transfers between devices, shards(): lax.all_to_all(sent.reshape(sp_count, capacity, local_width), SP, split_a...  21 us
    all_to_all x1, waiting for transfers between devices, shards(): lax.all_to_all(paired, 'y', split_axis=0, concat_axis=0, tiled=True)  17.2 us
    all_to_all x1, starting transfers between devices, sent_to_all(): return lax.all_to_all(copies, axis, split_axis=0, concat_axis=0, tiled=True)  11 us
    all_to_all x1, waiting for transfers between devices, shards(): lax.all_to_all(sent.reshape(sp_count, capacity, local_width), SP, split_a...  10.5 us
    all_to_all x1, waiting for transfers between devices, shards(): lax.all_to_all(expert_out.reshape(sp_count, capacity, local_width), SP, s...  10.4 us
  transfers between devices with their start and end apart: 19, of which 9 were waited for; matrix products, arithmetic and copies ran while one was open for 1% of the time, Pallas kernels for 4%

profile of v2, /device:TPU:1, one launch (start us, length us, event | category | flops | bytes accessed | tf_op | source)
XLA Modules:
  0.0 222.0 jit_solution(5397811078237129908)
XLA Ops:
  0.0 0.7 fusion.26
  0.7 0.9 fusion.19
  1.6 0.8 pad_maximum_fusion.2
  2.4 1.1 broadcast_in_dim.49
  3.6 11.0 %all-to-all-start = ((bf16[8,288,256]{2,1,0:T(8,128)(2,1)}), bf16[8,288,256]{2,1,0:T(8,128)(2,1)S(1)}, u32[]{:S(2)}, u32[]{:S(2)}) async-start(bf16[8,288,256]{2,1,0:T(8,128)(2,1)} %broadcast_in_dim.49), calls=%async_computation | async-start | bytes 2359296 | tf_op jit(solution)/shard_map/all_to_all | solution.py:31
  14.6 2.9 %collective-permute-start.4 = (bf16[2048,256]{1,0:T(8,128)(2,1)S(1)}, bf16[2048,256]{1,0:T(8,128)(2,1)}, u32[]{:S(2)}, u32[]{:S(2)}) collective-permute-start(bf16[2048,256]{1,0:T(8,128)(2,1)S(1)} %bitcast.51), channel_id=1, source_target_pairs={{0,1},{1,0},{2,3},{3,2},{4,5},{5,4},{6,7},{7,6},{8,9},{9,8},{10,11... | collective-permute-start | bytes 3145736 | tf_op jit(solution)/shard_map/ppermute | solution.py:35
  17.4 3.2 %collective-permute-start.7 = (bf16[2048,256]{1,0:T(8,128)(2,1)S(1)}, bf16[2048,256]{1,0:T(8,128)(2,1)}, u32[]{:S(2)}, u32[]{:S(2)}) collective-permute-start(bf16[2048,256]{1,0:T(8,128)(2,1)S(1)} %bitcast.52), channel_id=1, source_target_pairs={{0,14},{1,3},{2,0},{3,5},{4,2},{5,7},{6,4},{7,9},{8,6},{9,11},{10,... | collective-permute-start | bytes 3145736 | tf_op jit(solution)/shard_map/ppermute | solution.py:243
  20.6 3.2 %collective-permute-start.8 = (bf16[2048,256]{1,0:T(8,128)(2,1)S(1)}, bf16[2048,256]{1,0:T(8,128)(2,1)}, u32[]{:S(2)}, u32[]{:S(2)}) collective-permute-start(bf16[2048,256]{1,0:T(8,128)(2,1)S(1)} %bitcast.54), channel_id=1, source_target_pairs={{0,14},{1,3},{2,0},{3,5},{4,2},{5,7},{6,4},{7,9},{8,6},{9,11},{10,... | collective-permute-start | bytes 3145736 | tf_op jit(solution)/shard_map/ppermute | solution.py:243
  23.9 3.2 %collective-permute-start.9 = (bf16[256,2048]{1,0:T(8,128)(2,1)}, bf16[256,2048]{1,0:T(8,128)(2,1)}, u32[]{:S(2)}, u32[]{:S(2)}) collective-permute-start(bf16[256,2048]{1,0:T(8,128)(2,1)} %bitcast.11.refs_8_), channel_id=1, source_target_pairs={{0,14},{1,3},{2,0},{3,5},{4,2},{5,7},{6,4},{7,9},{8,6},{9,11},{10,... | collective-permute-start | bytes 3145736 | tf_op jit(solution)/shard_map/ppermute | solution.py:243
  27.1 3.1 %collective-permute-start = (bf16[128,256]{1,0:T(8,128)(2,1)S(1)}, bf16[128,256]{1,0:T(8,128)(2,1)S(1)}, u32[]{:S(2)}, u32[]{:S(2)}) collective-permute-start(bf16[128,256]{1,0:T(8,128)(2,1)S(1)} %broadcast_multiply_fusion.refs_0_), channel_id=1, source_target_pairs={{0,16},{16,32},{32,48},{48,0},{1,17},{17,33},{33,49},{49,1},{2,18}... | collective-permute-start | bytes 196616 | tf_op jit(solution)/shard_map/ppermute | solution.py:235
  30.2 3.4 %collective-permute-done.refs_1_ = bf16[128,256]{1,0:T(8,128)(2,1)S(1)} collective-permute-done((bf16[128,256]{1,0:T(8,128)(2,1)S(1)}, bf16[128,256]{1,0:T(8,128)(2,1)S(1)}, u32[]{:S(2)}, u32[]{:S(2)}) %collective-permute-start) | collective-permute-done | bytes 65568 | tf_op jit(solution)/shard_map/ppermute | solution.py:235
  33.6 3.5 %collective-permute-start.1 = (bf16[128,256]{1,0:T(8,128)(2,1)S(1)}, bf16[128,256]{1,0:T(8,128)(2,1)S(1)}, u32[]{:S(2)}, u32[]{:S(2)}) collective-permute-start(bf16[128,256]{1,0:T(8,128)(2,1)S(1)} %broadcast_multiply_fusion.refs_0_), channel_id=1, source_target_pairs={{0,32},{16,48},{32,0},{48,16},{1,33},{17,49},{33,1},{49,17},{2,34}... | collective-permute-start | bytes 196616 | tf_op jit(solution)/shard_map/ppermute | solution.py:235
  37.2 3.0 %collective-permute-done.1.refs_2_ = bf16[128,256]{1,0:T(8,128)(2,1)S(1)} collective-permute-done((bf16[128,256]{1,0:T(8,128)(2,1)S(1)}, bf16[128,256]{1,0:T(8,128)(2,1)S(1)}, u32[]{:S(2)}, u32[]{:S(2)}) %collective-permute-start.1) | collective-permute-done | bytes 65568 | tf_op jit(solution)/shard_map/ppermute | solution.py:235
  40.1 3.3 %collective-permute-start.2 = (bf16[128,256]{1,0:T(8,128)(2,1)S(1)}, bf16[128,256]{1,0:T(8,128)(2,1)S(1)}, u32[]{:S(2)}, u32[]{:S(2)}) collective-permute-start(bf16[128,256]{1,0:T(8,128)(2,1)S(1)} %broadcast_multiply_fusion.refs_0_), channel_id=1, source_target_pairs={{0,48},{16,0},{32,16},{48,32},{1,49},{17,1},{33,17},{49,33},{2,50}... | collective-permute-start | bytes 196616 | tf_op jit(solution)/shard_map/ppermute | solution.py:235
  43.4 0.7 pad_add_fusion.place_ref
  44.1 1.5 collective-permute-done.2.refs_3_
  45.5 1.1 all-to-all-done.kv_ref
  46.6 1.0 copy-done
  47.7 5.0 %attend.1 = bf16[4,144,256]{2,1,0:T(8,128)(2,1)} custom-call(s32[4]{0:T(128)} %pad_add_fusion.place_ref, bf16[8,288,256]{2,1,0:T(8,128)(2,1)} %copy-done, bf16[128,256]{1,0:T(8,128)(2,1)} %copy-done.3, bf16[128,256]{1,0:T(8,128)(2,1)} %copy-done.5, bf16[128,256]{1,0:T(8,128)(2,1)} %copy-done.6, bf16[128,256]{1,0:T(8,128)(2,1)} %copy-done.7), custom_call_target="tpu_custom_call" | custom-call | tf_op jit(solution)/shard_map/attend/pallas_call | solution.py:262
  52.7 9.8 %all_to_all.35.parts_ref = bf16[4,144,256]{2,1,0:T(8,128)(2,1)} all-to-all(bf16[4,144,256]{2,1,0:T(8,128)(2,1)} %attend.1), channel_id=1, replica_groups=mesh['z'=8,'x'=4,'y'=8,'c'=2] {'x'}, dimensions={0} | all-to-all | bytes 589824 | tf_op jit(solution)/shard_map/all_to_all | solution.py:284
  62.5 2.8 %project.1 = (bf16[8,256,128]{2,1,0:T(8,128)(2,1)}, bf16[8,256,128]{2,1,0:T(8,128)(2,1)}) custom-call(s32[4]{0:T(128)} %pad_add_fusion.place_ref, bf16[4,144,256]{2,1,0:T(8,128)(2,1)} %all_to_all.35.parts_ref, bf16[128,2048]{1,0:T(8,128)(2,1)} %weight_ref.1), custom_call_target="tpu_custom_call" | custom-call | tf_op jit(solution)/shard_map/project/pallas_call | solution.py:286
  65.4 7.6 %collective-permute-start.3 = (bf16[8,256,128]{2,1,0:T(8,128)(2,1)}, bf16[8,256,128]{2,1,0:T(8,128)(2,1)S(1)}, u32[]{:S(2)}, u32[]{:S(2)}) collective-permute-start(bf16[8,256,128]{2,1,0:T(8,128)(2,1)} %get-tuple-element.18), channel_id=1, source_target_pairs={{0,1},{1,0},{2,3},{3,2},{4,5},{5,4},{6,7},{7,6},{8,9},{9,8},{10,11... | collective-permute-start | bytes 1572872 | tf_op jit(solution)/shard_map/ppermute | solution.py:35
  73.0 1.9 collective-permute-start.5
  75.0 2.4 %collective-permute-start.6 = (bf16[256,2048]{1,0:T(8,128)(2,1)}, bf16[256,2048]{1,0:T(8,128)(2,1)}, u32[]{:S(2)}, u32[]{:S(2)}) collective-permute-start(bf16[256,2048]{1,0:T(8,128)(2,1)} %bitcast.11.refs_8_), channel_id=1, source_target_pairs={{0,1},{1,0},{2,3},{3,2},{4,5},{5,4},{6,7},{7,6},{8,9},{9,8},{10,11... | collective-permute-start | bytes 3145736 | tf_op jit(solution)/shard_map/ppermute | solution.py:35
  77.4 1.9 collective-permute-start.10
  79.3 2.4 %collective-permute-start.11 = (bf16[2048,256]{1,0:T(8,128)(2,1)}, bf16[2048,256]{1,0:T(8,128)(2,1)}, u32[]{:S(2)}, u32[]{:S(2)}) collective-permute-start(bf16[2048,256]{1,0:T(8,128)(2,1)} %collective-permute-done.8.refs_6_), channel_id=1, source_target_pairs={{0,1},{1,0},{2,3},{3,2},{4,5},{5,4},{6,7},{7,6},{8,9},{9,8},{10,11... | collective-permute-start | bytes 3145736 | tf_op jit(solution)/shard_map/ppermute | solution.py:35
  81.8 1.9 collective-permute-start.12
  83.7 2.0 add_convert_fusion
  85.7 3.5 %all-to-all-start.2 = ((bf16[8,256,128]{2,1,0:T(8,128)(2,1)}), bf16[8,256,128]{2,1,0:T(8,128)(2,1)S(1)}, u32[]{:S(2)}, u32[]{:S(2)}) async-start(bf16[8,256,128]{2,1,0:T(8,128)(2,1)} %add_convert_fusion), calls=%async_computation.2 | async-start | bytes 1048576 | tf_op jit(solution)/shard_map/all_to_all | solution.py:296
  89.9 17.2 %all-to-all-done.2 = bf16[8,256,128]{2,1,0:T(8,128)(2,1)S(1)} async-done(((bf16[8,256,128]{2,1,0:T(8,128)(2,1)}), bf16[8,256,128]{2,1,0:T(8,128)(2,1)S(1)}, u32[]{:S(2)}, u32[]{:S(2)}) %all-to-all-start.2) | async-done | bytes 524320 | tf_op jit(solution)/shard_map/all_to_all | solution.py:296
  107.2 0.3 convolution_convert_fusion
  107.5 0.7 reshape.43
  108.2 21.0 %all-to-all-start.3 = ((bf16[32,20,128]{2,1,0:T(8,128)(2,1)}), bf16[32,20,128]{2,1,0:T(8,128)(2,1)S(1)}, u32[]{:S(2)}, u32[]{:S(2)}) async-start(bf16[32,20,128]{2,1,0:T(8,128)(2,1)} %reshape.43), calls=%async_computation.3 | async-start | bytes 393216 | tf_op jit(solution)/shard_map/all_to_all | solution.py:305
  129.2 10.5 %all-to-all-done.3 = bf16[32,20,128]{2,1,0:T(8,128)(2,1)S(1)} async-done(((bf16[32,20,128]{2,1,0:T(8,128)(2,1)}), bf16[32,20,128]{2,1,0:T(8,128)(2,1)S(1)}, u32[]{:S(2)}, u32[]{:S(2)}) %all-to-all-start.3) | async-done | bytes 163872 | tf_op jit(solution)/shard_map/all_to_all | solution.py:305
  139.8 3.9 %collective-permute-start.13 = (bf16[2,160,128]{2,1,0:T(8,128)(2,1)S(1)}, bf16[2,160,128]{2,1,0:T(8,128)(2,1)S(1)}, u32[]{:S(2)}, u32[]{:S(2)}) collective-permute-start(bf16[2,160,128]{2,1,0:T(8,128)(2,1)S(1)} %get-tuple-element.34), channel_id=1, source_target_pairs={{0,1},{1,0},{2,3},{3,2},{4,5},{5,4},{6,7},{7,6},{8,9},{9,8},{10,11... | collective-permute-start | bytes 245768 | tf_op jit(solution)/shard_map/ppermute | solution.py:35
  143.8 0.9 collective-permute-done.13
  144.8 23.8 %all_to_all.36.rows_in_ref = bf16[8,2,160,128]{3,2,1,0:T(8,128)(2,1)} all-to-all(bf16[8,2,160,128]{3,2,1,0:T(8,128)(2,1)S(1)} %bitcast.49), channel_id=1, replica_groups=mesh['z'=8,'x'=4,'y'=8,'c'=2] {'y'}, dimensions={0} | all-to-all | bytes 1310720 | tf_op jit(solution)/shard_map/all_to_all | solution.py:315
  168.6 8.0 %expert.1 = bf16[8,160,256]{2,1,0:T(8,128)(2,1)} custom-call(s32[4]{0:T(128)} %pad_add_fusion.place_ref, bf16[8,2,160,128]{3,2,1,0:T(8,128)(2,1)} %all_to_all.36.rows_in_ref, f32[16,1,128]{2,1,0:T(1,128)} %bitcast.62, bf16[2048,256]{1,0:T(8,128)(2,1)} %bitcast.50, bf16[2048,256]{1,0:T(8,128)(2,1)} %collective-permute-done.4.refs_1_, ...), custom_call_target="tpu_custom_call" | custom-call | tf_op jit(solution)/shard_map/expert/pallas_call | solution.py:322
  176.7 24.0 %all_to_all.37 = bf16[8,160,256]{2,1,0:T(8,128)(2,1)S(1)} all-to-all(bf16[8,160,256]{2,1,0:T(8,128)(2,1)} %expert.1), channel_id=1, replica_groups=mesh['z'=8,'x'=4,'y'=8,'c'=2] {'y'}, dimensions={0} | all-to-all | bytes 1310720 | tf_op jit(solution)/shard_map/all_to_all | solution.py:339
  200.8 0.9 reduce_sum.32
  201.7 0.3 constant_dynamic-slice_fusion.1
  202.1 2.6 %collective-permute-start.14 = (bf16[2,160,128]{2,1,0:T(8,128)(2,1)S(1)}, bf16[2,160,128]{2,1,0:T(8,128)(2,1)S(1)}, u32[]{:S(2)}, u32[]{:S(2)}) collective-permute-start(bf16[2,160,128]{2,1,0:T(8,128)(2,1)S(1)} %bitcast.58), channel_id=1, source_target_pairs={{0,1},{1,0},{2,3},{3,2},{4,5},{5,4},{6,7},{7,6},{8,9},{9,8},{10,11... | collective-permute-start | bytes 245768 | tf_op jit(solution)/shard_map/ppermute | solution.py:35
  204.8 0.9 collective-permute-done.14
  205.7 0.7 reshape.47
  206.4 3.9 %all-to-all-start.6 = ((bf16[32,20,128]{2,1,0:T(8,128)(2,1)}), bf16[32,20,128]{2,1,0:T(8,128)(2,1)S(1)}, u32[]{:S(2)}, u32[]{:S(2)}) async-start(bf16[32,20,128]{2,1,0:T(8,128)(2,1)} %reshape.47), calls=%async_computation.6 | async-start | bytes 393216 | tf_op jit(solution)/shard_map/all_to_all | solution.py:347
  210.4 10.4 %all-to-all-done.6 = bf16[32,20,128]{2,1,0:T(8,128)(2,1)S(1)} async-done(((bf16[32,20,128]{2,1,0:T(8,128)(2,1)}), bf16[32,20,128]{2,1,0:T(8,128)(2,1)S(1)}, u32[]{:S(2)}, u32[]{:S(2)}) %all-to-all-start.6) | async-done | bytes 163872 | tf_op jit(solution)/shard_map/all_to_all | solution.py:347
  220.8 0.3 convolution_bitcast_fusion
  221.1 0.9 fusion.2
  (54 shorter events, 1.1 us)
Async XLA Ops:
  3.6 11.0 %copy-start.1 = (bf16[1,2048,256]{2,1,0:T(8,128)(2,1)S(1)}, bf16[1,2048,256]{2,1,0:T(8,128)(2,1)}, u32[]{:S(2)}) copy-start(bf16[1,2048,256]{2,1,0:T(8,128)(2,1)} %param.21) | copy-start | bytes 3145732
  3.6 17.1 %copy-start.2 = (bf16[1,2048,256]{2,1,0:T(8,128)(2,1)S(1)}, bf16[1,2048,256]{2,1,0:T(8,128)(2,1)}, u32[]{:S(2)}) copy-start(bf16[1,2048,256]{2,1,0:T(8,128)(2,1)} %param.22) | copy-start | bytes 3145732
  3.6 23.5 %copy-start.8 = (bf16[128,256]{1,0:T(8,128)(2,1)S(1)}, bf16[128,256]{1,0:T(8,128)(2,1)}, u32[]{:S(2)}) copy-start(bf16[128,256]{1,0:T(8,128)(2,1)} %param.13) | copy-start | bytes 196612
  3.6 43.0 %all-to-all-start = ((bf16[8,288,256]{2,1,0:T(8,128)(2,1)}), bf16[8,288,256]{2,1,0:T(8,128)(2,1)S(1)}, u32[]{:S(2)}, u32[]{:S(2)}) async-start(bf16[8,288,256]{2,1,0:T(8,128)(2,1)} %broadcast_in_dim.49), calls=%async_computation | async-start | bytes 2359296 | tf_op jit(solution)/shard_map/all_to_all | solution.py:31
  14.6 58.5 %collective-permute-start.4 = (bf16[2048,256]{1,0:T(8,128)(2,1)S(1)}, bf16[2048,256]{1,0:T(8,128)(2,1)}, u32[]{:S(2)}, u32[]{:S(2)}) collective-permute-start(bf16[2048,256]{1,0:T(8,128)(2,1)S(1)} %bitcast.51), channel_id=1, source_target_pairs={{0,1},{1,0},{2,3},{3,2},{4,5},{5,4},{6,7},{7,6},{8,9},{9,8},{10,11... | collective-permute-start | bytes 3145736 | tf_op jit(solution)/shard_map/ppermute | solution.py:35
  17.4 57.5 %collective-permute-start.7 = (bf16[2048,256]{1,0:T(8,128)(2,1)S(1)}, bf16[2048,256]{1,0:T(8,128)(2,1)}, u32[]{:S(2)}, u32[]{:S(2)}) collective-permute-start(bf16[2048,256]{1,0:T(8,128)(2,1)S(1)} %bitcast.52), channel_id=1, source_target_pairs={{0,14},{1,3},{2,0},{3,5},{4,2},{5,7},{6,4},{7,9},{8,6},{9,11},{10,... | collective-permute-start | bytes 3145736 | tf_op jit(solution)/shard_map/ppermute | solution.py:243
  20.6 56.7 %collective-permute-start.8 = (bf16[2048,256]{1,0:T(8,128)(2,1)S(1)}, bf16[2048,256]{1,0:T(8,128)(2,1)}, u32[]{:S(2)}, u32[]{:S(2)}) collective-permute-start(bf16[2048,256]{1,0:T(8,128)(2,1)S(1)} %bitcast.54), channel_id=1, source_target_pairs={{0,14},{1,3},{2,0},{3,5},{4,2},{5,7},{6,4},{7,9},{8,6},{9,11},{10,... | collective-permute-start | bytes 3145736 | tf_op jit(solution)/shard_map/ppermute | solution.py:243
  23.9 55.5 %collective-permute-start.9 = (bf16[256,2048]{1,0:T(8,128)(2,1)}, bf16[256,2048]{1,0:T(8,128)(2,1)}, u32[]{:S(2)}, u32[]{:S(2)}) collective-permute-start(bf16[256,2048]{1,0:T(8,128)(2,1)} %bitcast.11.refs_8_), channel_id=1, source_target_pairs={{0,14},{1,3},{2,0},{3,5},{4,2},{5,7},{6,4},{7,9},{8,6},{9,11},{10,... | collective-permute-start | bytes 3145736 | tf_op jit(solution)/shard_map/ppermute | solution.py:243
  27.1 19.5 %copy-start.3 = (bf16[128,256]{1,0:T(8,128)(2,1)}, bf16[128,256]{1,0:T(8,128)(2,1)S(1)}, u32[]{:S(2)}) copy-start(bf16[128,256]{1,0:T(8,128)(2,1)S(1)} %broadcast_multiply_fusion.refs_0_) | copy-start | bytes 196612
  27.1 6.5 %collective-permute-start = (bf16[128,256]{1,0:T(8,128)(2,1)S(1)}, bf16[128,256]{1,0:T(8,128)(2,1)S(1)}, u32[]{:S(2)}, u32[]{:S(2)}) collective-permute-start(bf16[128,256]{1,0:T(8,128)(2,1)S(1)} %broadcast_multiply_fusion.refs_0_), channel_id=1, source_target_pairs={{0,16},{16,32},{32,48},{48,0},{1,17},{17,33},{33,49},{49,1},{2,18}... | collective-permute-start | bytes 196616 | tf_op jit(solution)/shard_map/ppermute | solution.py:235
  33.6 13.0 %copy-start.5 = (bf16[128,256]{1,0:T(8,128)(2,1)}, bf16[128,256]{1,0:T(8,128)(2,1)S(1)}, u32[]{:S(2)}) copy-start(bf16[128,256]{1,0:T(8,128)(2,1)S(1)} %collective-permute-done.refs_1_) | copy-start | bytes 196612
  33.6 6.5 %collective-permute-start.1 = (bf16[128,256]{1,0:T(8,128)(2,1)S(1)}, bf16[128,256]{1,0:T(8,128)(2,1)S(1)}, u32[]{:S(2)}, u32[]{:S(2)}) collective-permute-start(bf16[128,256]{1,0:T(8,128)(2,1)S(1)} %broadcast_multiply_fusion.refs_0_), channel_id=1, source_target_pairs={{0,32},{16,48},{32,0},{48,16},{1,33},{17,49},{33,1},{49,17},{2,34}... | collective-permute-start | bytes 196616 | tf_op jit(solution)/shard_map/ppermute | solution.py:235
  40.1 6.5 %copy-start.6 = (bf16[128,256]{1,0:T(8,128)(2,1)}, bf16[128,256]{1,0:T(8,128)(2,1)S(1)}, u32[]{:S(2)}) copy-start(bf16[128,256]{1,0:T(8,128)(2,1)S(1)} %collective-permute-done.1.refs_2_) | copy-start | bytes 196612
  40.1 5.4 %collective-permute-start.2 = (bf16[128,256]{1,0:T(8,128)(2,1)S(1)}, bf16[128,256]{1,0:T(8,128)(2,1)S(1)}, u32[]{:S(2)}, u32[]{:S(2)}) collective-permute-start(bf16[128,256]{1,0:T(8,128)(2,1)S(1)} %broadcast_multiply_fusion.refs_0_), channel_id=1, source_target_pairs={{0,48},{16,0},{32,16},{48,32},{1,49},{17,1},{33,17},{49,33},{2,50}... | collective-permute-start | bytes 196616 | tf_op jit(solution)/shard_map/ppermute | solution.py:235
  45.5 1.1 copy-start.7
  46.6 1.0 copy-start
  65.4 16.4 %collective-permute-start.3 = (bf16[8,256,128]{2,1,0:T(8,128)(2,1)}, bf16[8,256,128]{2,1,0:T(8,128)(2,1)S(1)}, u32[]{:S(2)}, u32[]{:S(2)}) collective-permute-start(bf16[8,256,128]{2,1,0:T(8,128)(2,1)} %get-tuple-element.18), channel_id=1, source_target_pairs={{0,1},{1,0},{2,3},{3,2},{4,5},{5,4},{6,7},{7,6},{8,9},{9,8},{10,11... | collective-permute-start | bytes 1572872 | tf_op jit(solution)/shard_map/ppermute | solution.py:35
  73.0 16.8 %collective-permute-start.5 = (bf16[2048,256]{1,0:T(8,128)(2,1)S(1)}, bf16[2048,256]{1,0:T(8,128)(2,1)}, u32[]{:S(2)}, u32[]{:S(2)}) collective-permute-start(bf16[2048,256]{1,0:T(8,128)(2,1)S(1)} %bitcast.55), channel_id=1, source_target_pairs={{0,1},{1,0},{2,3},{3,2},{4,5},{5,4},{6,7},{7,6},{8,9},{9,8},{10,11... | collective-permute-start | bytes 3145736 | tf_op jit(solution)/shard_map/ppermute | solution.py:35
  75.0 14.9 %collective-permute-start.6 = (bf16[256,2048]{1,0:T(8,128)(2,1)}, bf16[256,2048]{1,0:T(8,128)(2,1)}, u32[]{:S(2)}, u32[]{:S(2)}) collective-permute-start(bf16[256,2048]{1,0:T(8,128)(2,1)} %bitcast.11.refs_8_), channel_id=1, source_target_pairs={{0,1},{1,0},{2,3},{3,2},{4,5},{5,4},{6,7},{7,6},{8,9},{9,8},{10,11... | collective-permute-start | bytes 3145736 | tf_op jit(solution)/shard_map/ppermute | solution.py:35
  77.4 12.5 %collective-permute-start.10 = (bf16[2048,256]{1,0:T(8,128)(2,1)}, bf16[2048,256]{1,0:T(8,128)(2,1)}, u32[]{:S(2)}, u32[]{:S(2)}) collective-permute-start(bf16[2048,256]{1,0:T(8,128)(2,1)} %collective-permute-done.7.refs_2_), channel_id=1, source_target_pairs={{0,1},{1,0},{2,3},{3,2},{4,5},{5,4},{6,7},{7,6},{8,9},{9,8},{10,11... | collective-permute-start | bytes 3145736 | tf_op jit(solution)/shard_map/ppermute | solution.py:35
  79.3 10.5 %collective-permute-start.11 = (bf16[2048,256]{1,0:T(8,128)(2,1)}, bf16[2048,256]{1,0:T(8,128)(2,1)}, u32[]{:S(2)}, u32[]{:S(2)}) collective-permute-start(bf16[2048,256]{1,0:T(8,128)(2,1)} %collective-permute-done.8.refs_6_), channel_id=1, source_target_pairs={{0,1},{1,0},{2,3},{3,2},{4,5},{5,4},{6,7},{7,6},{8,9},{9,8},{10,11... | collective-permute-start | bytes 3145736 | tf_op jit(solution)/shard_map/ppermute | solution.py:35
  81.8 8.1 %collective-permute-start.12 = (bf16[256,2048]{1,0:T(8,128)(2,1)}, bf16[256,2048]{1,0:T(8,128)(2,1)}, u32[]{:S(2)}, u32[]{:S(2)}) collective-permute-start(bf16[256,2048]{1,0:T(8,128)(2,1)} %collective-permute-done.9.refs_10_), channel_id=1, source_target_pairs={{0,1},{1,0},{2,3},{3,2},{4,5},{5,4},{6,7},{7,6},{8,9},{9,8},{10,11... | collective-permute-start | bytes 3145736 | tf_op jit(solution)/shard_map/ppermute | solution.py:35
  83.7 5.5 %copy-start.9 = (s32[256,2]{0,1:T(2,128)S(1)}, s32[256,2]{0,1:T(2,128)}, u32[]{:S(2)}) copy-start(s32[256,2]{0,1:T(2,128)} %param.19) | copy-start | bytes 6148
  85.7 21.4 %all-to-all-start.2 = ((bf16[8,256,128]{2,1,0:T(8,128)(2,1)}), bf16[8,256,128]{2,1,0:T(8,128)(2,1)S(1)}, u32[]{:S(2)}, u32[]{:S(2)}) async-start(bf16[8,256,128]{2,1,0:T(8,128)(2,1)} %add_convert_fusion), calls=%async_computation.2 | async-start | bytes 1048576 | tf_op jit(solution)/shard_map/all_to_all | solution.py:296
  89.6 17.5 %copy-start.4 = (bf16[256,128]{1,0:T(8,128)(2,1)S(1)}, bf16[256,128]{1,0:T(8,128)(2,1)}, u32[]{:S(2)}) copy-start(bf16[256,128]{1,0:T(8,128)(2,1)} %param.12) | copy-start | bytes 196612
  108.2 31.5 %all-to-all-start.3 = ((bf16[32,20,128]{2,1,0:T(8,128)(2,1)}), bf16[32,20,128]{2,1,0:T(8,128)(2,1)S(1)}, u32[]{:S(2)}, u32[]{:S(2)}) async-start(bf16[32,20,128]{2,1,0:T(8,128)(2,1)} %reshape.43), calls=%async_computation.3 | async-start | bytes 393216 | tf_op jit(solution)/shard_map/all_to_all | solution.py:305
  139.8 4.8 %collective-permute-start.13 = (bf16[2,160,128]{2,1,0:T(8,128)(2,1)S(1)}, bf16[2,160,128]{2,1,0:T(8,128)(2,1)S(1)}, u32[]{:S(2)}, u32[]{:S(2)}) collective-permute-start(bf16[2,160,128]{2,1,0:T(8,128)(2,1)S(1)} %get-tuple-element.34), channel_id=1, source_target_pairs={{0,1},{1,0},{2,3},{3,2},{4,5},{5,4},{6,7},{7,6},{8,9},{9,8},{10,11... | collective-permute-start | bytes 245768 | tf_op jit(solution)/shard_map/ppermute | solution.py:35
  202.1 8.2 %copy-start.10 = (f32[256,2]{0,1:T(2,128)S(1)}, f32[256,2]{0,1:T(2,128)}, u32[]{:S(2)}) copy-start(f32[256,2]{0,1:T(2,128)} %param.20) | copy-start | bytes 6148
  202.1 3.5 %collective-permute-start.14 = (bf16[2,160,128]{2,1,0:T(8,128)(2,1)S(1)}, bf16[2,160,128]{2,1,0:T(8,128)(2,1)S(1)}, u32[]{:S(2)}, u32[]{:S(2)}) collective-permute-start(bf16[2,160,128]{2,1,0:T(8,128)(2,1)S(1)} %bitcast.58), channel_id=1, source_target_pairs={{0,1},{1,0},{2,3},{3,2},{4,5},{5,4},{6,7},{7,6},{8,9},{9,8},{10,11... | collective-permute-start | bytes 245768 | tf_op jit(solution)/shard_map/ppermute | solution.py:35
  206.4 14.3 %all-to-all-start.6 = ((bf16[32,20,128]{2,1,0:T(8,128)(2,1)}), bf16[32,20,128]{2,1,0:T(8,128)(2,1)S(1)}, u32[]{:S(2)}, u32[]{:S(2)}) async-start(bf16[32,20,128]{2,1,0:T(8,128)(2,1)} %reshape.47), calls=%async_computation.6 | async-start | bytes 393216 | tf_op jit(solution)/shard_map/all_to_all | solution.py:347

commit v3 on v2

--- a/solution.py
+++ b/solution.py
@@ -19,120 +19,100 @@
 lane = 128
 
 
-def split_three(full):
-    first = lax.reduce_precision(full, 8, 7)
-    second = lax.reduce_precision(full - first, 8, 7)
-    third = lax.reduce_precision(full - first - second, 8, 7)
-    return [part.astype(jnp.bfloat16) for part in (first, second, third)]
-
-
-def sent_to_all(shard, axis):
-    copies = jnp.broadcast_to(shard, (lax.axis_size(axis), *shard.shape))
-    return lax.all_to_all(copies, axis, split_axis=0, concat_axis=0, tiled=True)
-
-
 def swapped(shard):
     return lax.ppermute(shard, "c", [(0, 1), (1, 0)])
 
 
+def three_parts(full):
+    parts = []
+    for _ in range(3):
+        part = full.astype(jnp.bfloat16).astype(jnp.float32)
+        full = full - part
+        parts.append(part)
+    return parts
+
+
+def pack_kernel(head_width, keys_ref, values_ref, gates_ref, queries_ref, out_ref, query_ref):
+    tokens = keys_ref.shape[1]
+    head_count = gates_ref.shape[0]
+    row = lax.broadcasted_iota(jnp.int32, (extra_rows, tokens), 0)
+    pieces = []
+    for head in range(head_count):
+        gates = jnp.zeros((extra_rows, tokens), jnp.float32)
+        for place, part in enumerate(three_parts(gates_ref[head : head + 1])):
+            gates = jnp.where(row == place, part, gates)
+        pieces += [keys_ref[head * head_width : (head + 1) * head_width], gates.astype(jnp.bfloat16)]
+    message = jnp.concatenate(pieces + [values_ref[...]], axis=0)
+    for copy in range(out_ref.shape[0]):
+        out_ref[copy] = message
+    query_ref[...] = queries_ref[...] * jnp.asarray(head_width ** (-0.5), jnp.bfloat16)
+
+
 def attend_kernel(head_count, head_width, place_ref, kv_ref, *refs):
-    x_count = len(refs) - 4
-    query_refs = refs[:x_count]
-    out_ref, query_scratch, sum_scratch, peak_scratch = refs[x_count:]
+    out_ref, query_scratch, key_scratch, value_scratch = refs[-4:]
+    query_refs = refs[:-4]
     tokens = kv_ref.shape[2]
+    z_count, x_count = kv_ref.shape[0], len(query_refs)
     deep = head_width + extra_rows
     z_place, x_place = place_ref[0], place_ref[1]
     row = lax.broadcasted_iota(jnp.int32, (extra_rows, tokens), 0)
     minus = jnp.where(row < 3, -1.0, 0.0).astype(jnp.bfloat16)
     ones = jnp.ones((extra_rows, tokens), jnp.bfloat16)
     for head in range(head_count):
+        rows = slice(head * head_width, (head + 1) * head_width)
         for shift in range(x_count):
-            chain = head * x_count + shift
-            query_scratch[chain, :head_width] = query_refs[shift][
-                head * head_width : (head + 1) * head_width
-            ]
-            query_scratch[chain, head_width:] = minus
-            sum_scratch[chain] = jnp.zeros((deep, tokens), jnp.float32)
-            peak_scratch[chain] = jnp.full((8, tokens), masked_score, jnp.float32)
-
-    def one(chain, key_rows, value_rows, masked):
-        scores = lax.dot_general(
-            key_rows,
-            query_scratch[chain],
-            (((0,), (0,)), ((), ())),
-            preferred_element_type=jnp.float32,
-        )
-        if masked:
-            key_place = lax.broadcasted_iota(jnp.int32, scores.shape, 0)
+            target = lax.rem(x_place + x_count - shift, x_count)
+            columns = pl.ds(pl.multiple_of(target * tokens, tokens), tokens)
+            query_scratch[head, :head_width, columns] = query_refs[shift][rows]
+            query_scratch[head, head_width:, columns] = minus
+        for block in range(z_count):
+            columns = slice(block * tokens, (block + 1) * tokens)
+            key_scratch[head, :, columns] = kv_ref[block, head * deep : (head + 1) * deep]
+            first = head_count * deep + head * head_width
+            value_scratch[head, :head_width, columns] = kv_ref[block, first : first + head_width]
+            value_scratch[head, head_width:, columns] = ones
+    wide = 2 * tokens if x_count % 2 == 0 else tokens
+    for head in range(head_count):
+        rows = slice(head * head_width, (head + 1) * head_width)
+        for first in range(0, x_count * tokens, wide):
+            scores = lax.dot_general(
+                key_scratch[head],
+                query_scratch[head, :, first : first + wide],
+                (((0,), (0,)), ((), ())),
+                preferred_element_type=jnp.float32,
+            )
+            key_row = lax.broadcasted_iota(jnp.int32, scores.shape, 0)
+            key_place = key_row // tokens * (x_count * tokens) + key_row % tokens
+            key_place = key_place + x_place * tokens
             query_place = lax.broadcasted_iota(jnp.int32, scores.shape, 1)
-            scores = jnp.where(key_place <= query_place, scores, masked_score)
-        old_peak = peak_scratch[chain, :1]
-        new_peak = jnp.maximum(old_peak, jnp.max(scores, axis=0, keepdims=True))
-        weights = jnp.exp(scores - new_peak).astype(jnp.bfloat16)
-        shrink = jnp.exp(old_peak - new_peak)
-        sum_scratch[chain] = sum_scratch[chain] * shrink + jnp.dot(
-            value_rows, weights, preferred_element_type=jnp.float32
-        )
-        peak_scratch[chain] = jnp.broadcast_to(new_peak, (8, tokens))
-
-    def loaded(z_key, head):
-        key_rows = kv_ref[z_key, head * deep : (head + 1) * deep]
-        value_first = head_count * deep + head * head_width
-        value_rows = kv_ref[z_key, value_first : value_first + head_width]
-        return key_rows, jnp.concatenate([value_rows, ones], axis=0)
-
-    def earlier(z_key, carry):
-        for head in range(head_count):
-            key_rows, value_rows = loaded(z_key, head)
-            for shift in range(x_count):
-                one(head * x_count + shift, key_rows, value_rows, False)
-        return carry
-
-    lax.fori_loop(0, z_place, earlier, 0)
-    for head in range(head_count):
-        key_rows, value_rows = loaded(z_place, head)
-        one(head * x_count, key_rows, value_rows, True)
-    for shift in range(1, x_count):
-
-        @pl.when(x_place < shift)
-        def _():
-            for head in range(head_count):
-                key_rows, value_rows = loaded(z_place, head)
-                one(head * x_count + shift, key_rows, value_rows, False)
-
-    for shift in range(x_count):
-        target = lax.rem(x_place + x_count - shift, x_count)
-        stats = jnp.zeros((extra_rows, tokens), jnp.float32)
-        for head in range(head_count):
-            chain = head * x_count + shift
-            out_ref[target, head * head_width : (head + 1) * head_width] = sum_scratch[
-                chain, :head_width
-            ].astype(jnp.bfloat16)
-            place = head * 6
-            for full in (peak_scratch[chain, :1], sum_scratch[chain, head_width : head_width + 1]):
-                for _ in range(3):
-                    part = full.astype(jnp.bfloat16).astype(jnp.float32)
-                    full = full - part
+            query_place = query_place + (z_place * (x_count * tokens) + first)
+            scores = jnp.where(key_place <= query_place, scores, 2 * masked_score)
+            peak = jnp.maximum(jnp.max(scores, axis=0, keepdims=True), masked_score)
+            weights = jnp.exp(scores - peak).astype(jnp.bfloat16)
+            summed = jnp.dot(value_scratch[head], weights, preferred_element_type=jnp.float32)
+            for block in range(first // tokens, (first + wide) // tokens):
+                columns = slice(block * tokens - first, (block + 1) * tokens - first)
+                out_ref[block, rows] = summed[:head_width, columns].astype(jnp.bfloat16)
+                stats = jnp.zeros((extra_rows, tokens), jnp.float32)
+                total = summed[head_width : head_width + 1, columns]
+                for place, part in enumerate(three_parts(peak[:, columns]) + three_parts(total)):
                     stats = jnp.where(row == place, part, stats)
-                    place += 1
-        out_ref[target, head_count * head_width :] = stats.astype(jnp.bfloat16)
+                base = head_count * head_width + head * extra_rows
+                out_ref[block, base : base + extra_rows] = stats.astype(jnp.bfloat16)
 
 
 def project_kernel(head_count, head_width, place_ref, parts_ref, weight_ref, mine_ref, other_ref, full_ref):
     x_count = parts_ref.shape[0]
     tp_half = mine_ref.shape[0]
-    width = head_count * head_width
     core = place_ref[2]
     rows = []
     for head in range(head_count):
         peaks, totals = [], []
+        base = head_count * head_width + head * extra_rows
         for part in range(x_count):
-            stats = parts_ref[part, width : width + extra_rows].astype(jnp.float32)
-            base = head * 6
-            peaks.append(stats[base : base + 1] + stats[base + 1 : base + 2] + stats[base + 2 : base + 3])
-            totals.append(
-                stats[base + 3 : base + 4] + stats[base + 4 : base + 5] + stats[base + 5 : base + 6]
-            )
+            stats = parts_ref[part, base : base + extra_rows].astype(jnp.float32)
+            peaks.append(stats[0:1] + stats[1:2] + stats[2:3])
+            totals.append(stats[3:4] + stats[4:5] + stats[5:6])
         top = functools.reduce(jnp.maximum, peaks)
         factors = [jnp.exp(peak - top) for peak in peaks]
         total = sum(factor * amount for factor, amount in zip(factors, totals))
@@ -225,12 +205,20 @@
     smem = pl.BlockSpec(memory_space=pltpu.SMEM)
     vmem = pl.BlockSpec(memory_space=pltpu.VMEM)
 
-    gates = jnp.stack(split_three(forget_cache), axis=1)
-    gates = jnp.pad(gates, ((0, 0), (0, extra_rows - 3), (0, 0)))
-    key_rows = jnp.concatenate([keys.reshape(head_count, head_width, token_count), gates], axis=1)
-    message = jnp.concatenate([key_rows.reshape(-1, token_count), values], axis=0)
-    gathered = sent_to_all(message, "z")
-    scaled = queries * jnp.asarray(head_width ** (-0.5), bf16)
+    deep = head_width + extra_rows
+    message_rows = head_count * (deep + head_width)
+    message, scaled = pl.pallas_call(
+        functools.partial(pack_kernel, head_width),
+        out_shape=(
+            jax.ShapeDtypeStruct((z_count, message_rows, token_count), bf16),
+            jax.ShapeDtypeStruct(queries.shape, bf16),
+        ),
+        in_specs=[vmem] * 4,
+        out_specs=(vmem, vmem),
+        name="pack",
+        interpret=INTERPRET,
+    )(keys, values, forget_cache, queries)
+    gathered = lax.all_to_all(message, "z", split_axis=0, concat_axis=0, tiled=True)
     query_list = [scaled] + [
         lax.ppermute(scaled, "x", [(i, (i + shift) % x_count) for i in range(x_count)])
         for shift in range(1, x_count)
@@ -242,24 +230,21 @@
     own_set = (gate_weight[0], up_weight[0], down_weight[0])
     near_set = tuple(lax.ppermute(weight, TP, slice_moves) for weight in own_set)
     own_swapped = tuple(swapped(weight) for weight in own_set)
-    near_swapped = tuple(swapped(weight) for weight in near_set)
-    chains = head_count * x_count
-    deep = head_width + extra_rows
-    part_rows = head_count * head_width + extra_rows
     attend = pl.pallas_call(
         functools.partial(attend_kernel, head_count, head_width),
-        out_shape=jax.ShapeDtypeStruct((x_count, part_rows, token_count), bf16),
+        out_shape=jax.ShapeDtypeStruct((x_count, head_count * deep, token_count), bf16),
         in_specs=[smem] + [vmem] * (1 + x_count),
         out_specs=vmem,
         scratch_shapes=[
-            pltpu.VMEM((chains, deep, token_count), bf16),
-            pltpu.VMEM((chains, deep, token_count), f32),
-            pltpu.VMEM((chains, 8, token_count), f32),
+            pltpu.VMEM((head_count, deep, x_count * token_count), bf16),
+            pltpu.VMEM((head_count, deep, z_count * token_count), bf16),
+            pltpu.VMEM((head_count, deep, z_count * token_count), bf16),
         ],
         name="attend",
         interpret=INTERPRET,
     )
     parts = attend(place, gathered, *query_list)
+    received = lax.all_to_all(parts, "x", split_axis=0, concat_axis=0, tiled=True)
 
     expert_ids = jnp.arange(sp_count, dtype=jnp.int32)
     chosen = routes[:, :, None] == expert_ids
@@ -281,7 +266,6 @@
 
     give_first, give_rest = spread(share_first), spread(share_rest)
 
-    received = lax.all_to_all(parts, "x", split_axis=0, concat_axis=0, tiled=True)
     half = jax.ShapeDtypeStruct((y_count, token_count, local_width), bf16)
     mine, other = pl.pallas_call(
         functools.partial(project_kernel, head_count, head_width),
@@ -294,17 +278,17 @@
     )(place, received, out_weight)
     paired = (mine.astype(f32) + swapped(other).astype(f32)).astype(bf16)
     pieces = lax.all_to_all(paired, "y", split_axis=0, concat_axis=0, tiled=True)
-    pieces, own_swapped, near_set, near_swapped = lax.optimization_barrier(
-        (pieces, own_swapped, near_set, near_swapped)
-    )
-    weight_sets = [own_set, own_swapped, near_set, near_swapped]
+    pieces, own_swapped, near_set = lax.optimization_barrier((pieces, own_swapped, near_set))
+    near_swapped = tuple(swapped(weight) for weight in near_set)
     head_sum = jnp.sum(pieces.astype(f32), axis=0)
     stream = (residual.astype(f32) + head_sum).astype(bf16)
 
     sent = jnp.dot(taken, stream, preferred_element_type=f32).astype(bf16)
     arrived = lax.all_to_all(
         sent.reshape(sp_count, capacity, local_width), SP, split_axis=0, concat_axis=0, tiled=True
-    ).reshape(slot_total, local_width)
+    )
+    arrived, near_swapped = lax.optimization_barrier((arrived, near_swapped))
+    weight_sets = [own_set, own_swapped, near_set, near_swapped]
     quarter = slot_total // 4
     arrived = arrived.reshape(2, 2, quarter, local_width)
     core = place[2]

time: 223 us -> 233 us (1.045)
  waiting for transfers between devices: 48.8 us -> 70.3 us
  starting transfers between devices: 86.6 us -> 71.1 us
  Pallas kernels: 15.9 us -> 22 us
  other arithmetic: 6.12 us -> 3.66 us
    ppermute x3, waiting for transfers between devices: 0.01 us -> 23.2 us  [shards(): lax.ppermute(weight, TP, slice_moves)]
    all_to_all x1, starting transfers between devices: 21 us -> 3.87 us  [shards(): lax.all_to_all(sent.reshape(sp_count, capacity, local_width), SP, split_a...]
    all_to_all x1, waiting for transfers between devices: 1.05 us -> 16.4 us  [shards(): lax.all_to_all(message, 'z', split_axis=0, concat_axis=0, tiled=True)]
    all_to_all x1, waiting for transfers between devices: 17.2 us -> 6.39 us  [shards(): lax.all_to_all(paired, 'y', split_axis=0, concat_axis=0, tiled=True)]
    ppermute x3, waiting for transfers between devices: 7.8 us -> 1.59 us  [shards(): lax.ppermute(scaled, 'x', [(i, (i + shift) % x_count) for i in range(x_co...]
    pallas_call x1, Pallas kernels: 5.02 us -> 9.05 us  [shards(): parts = attend(place, gathered, *query_list)]
  transfers between devices with their start and end apart: 19 -> 19, of which waited for: 9 -> 9; matrix products, arithmetic and copies ran while one was open for 1% -> 2% of each run, Pallas kernels for 4% -> 5%
where the time goes in v3:
time: 233 us; the launch traced here: 231 us
  starting transfers between devices  71.1 us (31%)
  waiting for transfers between devices  70.3 us (30%)
  blocking collectives  58.2 us (25%)
  Pallas kernels  22 us (9%)
  local copies, waits for them, and re-layouts  3.99 us (2%)
  other arithmetic  3.66 us (2%)
    ppermute x9, starting transfers between devices, swapped(): return lax.ppermute(shard, 'c', [(0, 1), (1, 0)])  29 us
    all_to_all x1, blocking collectives, shards(): lax.all_to_all(both.reshape(y_count, 2, quarter, local_width), 'y', split...  25.4 us
    ppermute x3, waiting for transfers between devices, shards(): lax.ppermute(weight, TP, slice_moves)  23.2 us
    all_to_all x1, blocking collectives, shards(): lax.all_to_all(out_rows, 'y', split_axis=0, concat_axis=0, tiled=True)  21.7 us
    all_to_all x1, waiting for transfers between devices, shards(): lax.all_to_all(message, 'z', split_axis=0, concat_axis=0, tiled=True)  16.4 us
    all_to_all x1, blocking collectives, shards(): lax.all_to_all(parts, 'x', split_axis=0, concat_axis=0, tiled=True)  11 us
    all_to_all x1, starting transfers between devices, shards(): lax.all_to_all(message, 'z', split_axis=0, concat_axis=0, tiled=True)  11 us
    ppermute x3, starting transfers between devices, shards(): lax.ppermute(scaled, 'x', [(i, (i + shift) % x_count) for i in range(x_co...  10.5 us
  transfers between devices with their start and end apart: 19, of which 9 were waited for; matrix products, arithmetic and copies ran while one was open for 2% of the time, Pallas kernels for 5%

profile of v3, /device:TPU:1, one launch (start us, length us, event | category | flops | bytes accessed | tf_op | source)
XLA Modules:
  0.0 231.4 jit_solution(13718661347897716648)
XLA Ops:
  0.0 2.1 pack.1
  2.1 11.0 %all-to-all-start = ((bf16[8,288,256]{2,1,0:T(8,128)(2,1)}), bf16[8,288,256]{2,1,0:T(8,128)(2,1)S(1)}, u32[]{:S(2)}, u32[]{:S(2)}) async-start(bf16[8,288,256]{2,1,0:T(8,128)(2,1)} %get-tuple-element.20), calls=%async_computation | async-start | bytes 2359296 | tf_op jit(solution)/shard_map/all_to_all | solution.py:221
  13.1 2.9 %collective-permute-start.4 = (bf16[2048,256]{1,0:T(8,128)(2,1)S(1)}, bf16[2048,256]{1,0:T(8,128)(2,1)S(1)}, u32[]{:S(2)}, u32[]{:S(2)}) collective-permute-start(bf16[2048,256]{1,0:T(8,128)(2,1)S(1)} %bitcast.43), channel_id=1, source_target_pairs={{0,1},{1,0},{2,3},{3,2},{4,5},{5,4},{6,7},{7,6},{8,9},{9,8},{10,11... | collective-permute-start | bytes 3145736 | tf_op jit(solution)/shard_map/ppermute | solution.py:23
  15.9 3.1 %collective-permute-start = (bf16[128,256]{1,0:T(8,128)(2,1)S(1)}, bf16[128,256]{1,0:T(8,128)(2,1)S(1)}, u32[]{:S(2)}, u32[]{:S(2)}) collective-permute-start(bf16[128,256]{1,0:T(8,128)(2,1)S(1)} %copy-done.5), channel_id=1, source_target_pairs={{0,16},{16,32},{32,48},{48,0},{1,17},{17,33},{33,49},{49,1},{2,18}... | collective-permute-start | bytes 196616 | tf_op jit(solution)/shard_map/ppermute | solution.py:223
  19.1 4.4 %collective-permute-start.1 = (bf16[128,256]{1,0:T(8,128)(2,1)S(1)}, bf16[128,256]{1,0:T(8,128)(2,1)S(1)}, u32[]{:S(2)}, u32[]{:S(2)}) collective-permute-start(bf16[128,256]{1,0:T(8,128)(2,1)S(1)} %copy-done.5), channel_id=1, source_target_pairs={{0,32},{16,48},{32,0},{48,16},{1,33},{17,49},{33,1},{49,17},{2,34}... | collective-permute-start | bytes 196616 | tf_op jit(solution)/shard_map/ppermute | solution.py:223
  23.4 3.1 %collective-permute-start.2 = (bf16[128,256]{1,0:T(8,128)(2,1)S(1)}, bf16[128,256]{1,0:T(8,128)(2,1)S(1)}, u32[]{:S(2)}, u32[]{:S(2)}) collective-permute-start(bf16[128,256]{1,0:T(8,128)(2,1)S(1)} %copy-done.5), channel_id=1, source_target_pairs={{0,48},{16,0},{32,16},{48,32},{1,49},{17,1},{33,17},{49,33},{2,50}... | collective-permute-start | bytes 196616 | tf_op jit(solution)/shard_map/ppermute | solution.py:223
  26.5 0.6 pad_add_fusion.place_ref
  27.2 1.6 collective-permute-done.2.refs_3_
  28.8 16.4 %all-to-all-done.kv_ref = bf16[8,288,256]{2,1,0:T(8,128)(2,1)S(1)} async-done(((bf16[8,288,256]{2,1,0:T(8,128)(2,1)}), bf16[8,288,256]{2,1,0:T(8,128)(2,1)S(1)}, u32[]{:S(2)}, u32[]{:S(2)}) %all-to-all-start) | async-done | bytes 1179680 | tf_op jit(solution)/shard_map/all_to_all | solution.py:221
  45.1 1.0 copy-done
  46.2 9.1 %attend.1 = bf16[4,160,256]{2,1,0:T(8,128)(2,1)} custom-call(s32[4]{0:T(128)} %pad_add_fusion.place_ref, bf16[8,288,256]{2,1,0:T(8,128)(2,1)} %copy-done, bf16[128,256]{1,0:T(8,128)(2,1)} %get-tuple-element.21.refs_0_, bf16[128,256]{1,0:T(8,128)(2,1)} %copy-done.6, bf16[128,256]{1,0:T(8,128)(2,1)} %copy-done.7, bf16[128,256]{1,0:T(8,128)(2,1)} %copy-done.8), custom_call_target="tpu_custom_call" | custom-call | tf_op jit(solution)/shard_map/attend/pallas_call | solution.py:246
  55.2 11.0 %all_to_all.35.parts_ref = bf16[4,160,256]{2,1,0:T(8,128)(2,1)} all-to-all(bf16[4,160,256]{2,1,0:T(8,128)(2,1)} %attend.1), channel_id=1, replica_groups=mesh['z'=8,'x'=4,'y'=8,'c'=2] {'x'}, dimensions={0} | all-to-all | bytes 655360 | tf_op jit(solution)/shard_map/all_to_all | solution.py:247
  66.3 2.8 %project.1 = (bf16[8,256,128]{2,1,0:T(8,128)(2,1)}, bf16[8,256,128]{2,1,0:T(8,128)(2,1)}) custom-call(s32[4]{0:T(128)} %pad_add_fusion.place_ref, bf16[4,160,256]{2,1,0:T(8,128)(2,1)} %all_to_all.35.parts_ref, bf16[128,2048]{1,0:T(8,128)(2,1)} %weight_ref.1), custom_call_target="tpu_custom_call" | custom-call | tf_op jit(solution)/shard_map/project/pallas_call | solution.py:270
  69.1 3.5 %collective-permute-start.3 = (bf16[8,256,128]{2,1,0:T(8,128)(2,1)}, bf16[8,256,128]{2,1,0:T(8,128)(2,1)S(1)}, u32[]{:S(2)}, u32[]{:S(2)}) collective-permute-start(bf16[8,256,128]{2,1,0:T(8,128)(2,1)} %get-tuple-element.23), channel_id=1, source_target_pairs={{0,1},{1,0},{2,3},{3,2},{4,5},{5,4},{6,7},{7,6},{8,9},{9,8},{10,11... | collective-permute-start | bytes 1572872 | tf_op jit(solution)/shard_map/ppermute | solution.py:23
  72.6 3.2 %collective-permute-start.7 = (bf16[2048,256]{1,0:T(8,128)(2,1)S(1)}, bf16[2048,256]{1,0:T(8,128)(2,1)}, u32[]{:S(2)}, u32[]{:S(2)}) collective-permute-start(bf16[2048,256]{1,0:T(8,128)(2,1)S(1)} %bitcast.44), channel_id=1, source_target_pairs={{0,14},{1,3},{2,0},{3,5},{4,2},{5,7},{6,4},{7,9},{8,6},{9,11},{10,... | collective-permute-start | bytes 3145736 | tf_op jit(solution)/shard_map/ppermute | solution.py:231
  75.8 4.1 %collective-permute-start.5 = (bf16[2048,256]{1,0:T(8,128)(2,1)S(1)}, bf16[2048,256]{1,0:T(8,128)(2,1)}, u32[]{:S(2)}, u32[]{:S(2)}) collective-permute-start(bf16[2048,256]{1,0:T(8,128)(2,1)S(1)} %bitcast.46), channel_id=1, source_target_pairs={{0,1},{1,0},{2,3},{3,2},{4,5},{5,4},{6,7},{7,6},{8,9},{9,8},{10,11... | collective-permute-start | bytes 3145736 | tf_op jit(solution)/shard_map/ppermute | solution.py:23
  79.9 1.9 collective-permute-start.8
  81.8 3.3 %collective-permute-start.6 = (bf16[256,2048]{1,0:T(8,128)(2,1)}, bf16[256,2048]{1,0:T(8,128)(2,1)}, u32[]{:S(2)}, u32[]{:S(2)}) collective-permute-start(bf16[256,2048]{1,0:T(8,128)(2,1)} %bitcast.6.refs_8_), channel_id=1, source_target_pairs={{0,1},{1,0},{2,3},{3,2},{4,5},{5,4},{6,7},{7,6},{8,9},{9,8},{10,11... | collective-permute-start | bytes 3145736 | tf_op jit(solution)/shard_map/ppermute | solution.py:23
  85.1 2.3 collective-permute-start.9
  87.4 2.0 add_convert_fusion
  89.4 5.3 %all-to-all-start.2 = ((bf16[8,256,128]{2,1,0:T(8,128)(2,1)}), bf16[8,256,128]{2,1,0:T(8,128)(2,1)S(1)}, u32[]{:S(2)}, u32[]{:S(2)}) async-start(bf16[8,256,128]{2,1,0:T(8,128)(2,1)} %add_convert_fusion), calls=%async_computation.2 | async-start | bytes 1048576 | tf_op jit(solution)/shard_map/all_to_all | solution.py:280
  94.8 9.9 %collective-permute-done.8.refs_6_ = bf16[2048,256]{1,0:T(8,128)(2,1)} collective-permute-done((bf16[2048,256]{1,0:T(8,128)(2,1)S(1)}, bf16[2048,256]{1,0:T(8,128)(2,1)}, u32[]{:S(2)}, u32[]{:S(2)}) %collective-permute-start.8) | collective-permute-done | bytes 1048608 | tf_op jit(solution)/shard_map/ppermute | solution.py:231
  104.7 13.3 %collective-permute-done.9.refs_10_ = bf16[256,2048]{1,0:T(8,128)(2,1)} collective-permute-done((bf16[256,2048]{1,0:T(8,128)(2,1)}, bf16[256,2048]{1,0:T(8,128)(2,1)}, u32[]{:S(2)}, u32[]{:S(2)}) %collective-permute-start.9) | collective-permute-done | bytes 1048608 | tf_op jit(solution)/shard_map/ppermute | solution.py:231
  118.0 6.4 %all-to-all-done.2 = bf16[8,256,128]{2,1,0:T(8,128)(2,1)S(1)} async-done(((bf16[8,256,128]{2,1,0:T(8,128)(2,1)}), bf16[8,256,128]{2,1,0:T(8,128)(2,1)S(1)}, u32[]{:S(2)}, u32[]{:S(2)}) %all-to-all-start.2) | async-done | bytes 524320 | tf_op jit(solution)/shard_map/all_to_all | solution.py:280
  124.4 1.9 collective-permute-start.10
  126.3 2.4 %collective-permute-start.11 = (bf16[2048,256]{1,0:T(8,128)(2,1)}, bf16[2048,256]{1,0:T(8,128)(2,1)}, u32[]{:S(2)}, u32[]{:S(2)}) collective-permute-start(bf16[2048,256]{1,0:T(8,128)(2,1)} %collective-permute-done.8.refs_6_), channel_id=1, source_target_pairs={{0,1},{1,0},{2,3},{3,2},{4,5},{5,4},{6,7},{7,6},{8,9},{9,8},{10,11... | collective-permute-start | bytes 3145736 | tf_op jit(solution)/shard_map/ppermute | solution.py:23
  128.8 1.9 collective-permute-start.12
  130.7 0.2 convolution_convert_fusion.1
  131.4 0.4 copy-done.4
  131.8 0.3 convolution_convert_fusion
  132.1 0.7 reshape.38
  132.9 3.9 %all-to-all-start.3 = ((bf16[32,20,128]{2,1,0:T(8,128)(2,1)}), bf16[32,20,128]{2,1,0:T(8,128)(2,1)S(1)}, u32[]{:S(2)}, u32[]{:S(2)}) async-start(bf16[32,20,128]{2,1,0:T(8,128)(2,1)} %reshape.38), calls=%async_computation.3 | async-start | bytes 393216 | tf_op jit(solution)/shard_map/all_to_all | solution.py:287
  136.7 10.5 %all-to-all-done.3 = bf16[32,20,128]{2,1,0:T(8,128)(2,1)S(1)} async-done(((bf16[32,20,128]{2,1,0:T(8,128)(2,1)}), bf16[32,20,128]{2,1,0:T(8,128)(2,1)S(1)}, u32[]{:S(2)}, u32[]{:S(2)}) %all-to-all-start.3) | async-done | bytes 163872 | tf_op jit(solution)/shard_map/all_to_all | solution.py:287
  147.3 4.2 %collective-permute-start.13 = (bf16[2,160,128]{2,1,0:T(8,128)(2,1)S(1)}, bf16[2,160,128]{2,1,0:T(8,128)(2,1)S(1)}, u32[]{:S(2)}, u32[]{:S(2)}) collective-permute-start(bf16[2,160,128]{2,1,0:T(8,128)(2,1)S(1)} %get-tuple-element.40), channel_id=1, source_target_pairs={{0,1},{1,0},{2,3},{3,2},{4,5},{5,4},{6,7},{7,6},{8,9},{9,8},{10,11... | collective-permute-start | bytes 245768 | tf_op jit(solution)/shard_map/ppermute | solution.py:23
  151.5 0.9 collective-permute-done.13
  152.5 25.4 %all_to_all.36.rows_in_ref = bf16[8,2,160,128]{3,2,1,0:T(8,128)(2,1)} all-to-all(bf16[8,2,160,128]{3,2,1,0:T(8,128)(2,1)S(1)} %bitcast.41), channel_id=1, replica_groups=mesh['z'=8,'x'=4,'y'=8,'c'=2] {'y'}, dimensions={0} | all-to-all | bytes 1310720 | tf_op jit(solution)/shard_map/all_to_all | solution.py:299
  177.9 8.1 %expert.1 = bf16[8,160,256]{2,1,0:T(8,128)(2,1)} custom-call(s32[4]{0:T(128)} %pad_add_fusion.place_ref, bf16[8,2,160,128]{3,2,1,0:T(8,128)(2,1)} %all_to_all.36.rows_in_ref, f32[16,1,128]{2,1,0:T(1,128)} %bitcast.52, bf16[2048,256]{1,0:T(8,128)(2,1)} %bitcast.42, bf16[2048,256]{1,0:T(8,128)(2,1)} %copy-done.3, ...), custom_call_target="tpu_custom_call" | custom-call | tf_op jit(solution)/shard_map/expert/pallas_call | solution.py:306
  186.0 21.7 %all_to_all.37 = bf16[8,160,256]{2,1,0:T(8,128)(2,1)S(1)} all-to-all(bf16[8,160,256]{2,1,0:T(8,128)(2,1)} %expert.1), channel_id=1, replica_groups=mesh['z'=8,'x'=4,'y'=8,'c'=2] {'y'}, dimensions={0} | all-to-all | bytes 1310720 | tf_op jit(solution)/shard_map/all_to_all | solution.py:323
  207.7 0.2 reshape.42
  207.9 0.9 reduce_sum.32
  208.8 0.3 constant_dynamic-slice_fusion.1
  209.2 4.9 %collective-permute-start.14 = (bf16[2,160,128]{2,1,0:T(8,128)(2,1)S(1)}, bf16[2,160,128]{2,1,0:T(8,128)(2,1)S(1)}, u32[]{:S(2)}, u32[]{:S(2)}) collective-permute-start(bf16[2,160,128]{2,1,0:T(8,128)(2,1)S(1)} %bitcast.49), channel_id=1, source_target_pairs={{0,1},{1,0},{2,3},{3,2},{4,5},{5,4},{6,7},{7,6},{8,9},{9,8},{10,11... | collective-permute-start | bytes 245768 | tf_op jit(solution)/shard_map/ppermute | solution.py:23
  214.1 0.9 collective-permute-done.14
  215.0 0.7 reshape.43
  215.7 3.9 %all-to-all-start.6 = ((bf16[32,20,128]{2,1,0:T(8,128)(2,1)}), bf16[32,20,128]{2,1,0:T(8,128)(2,1)S(1)}, u32[]{:S(2)}, u32[]{:S(2)}) async-start(bf16[32,20,128]{2,1,0:T(8,128)(2,1)} %reshape.43), calls=%async_computation.6 | async-start | bytes 393216 | tf_op jit(solution)/shard_map/all_to_all | solution.py:331
  219.7 10.4 %all-to-all-done.6 = bf16[32,20,128]{2,1,0:T(8,128)(2,1)S(1)} async-done(((bf16[32,20,128]{2,1,0:T(8,128)(2,1)}), bf16[32,20,128]{2,1,0:T(8,128)(2,1)S(1)}, u32[]{:S(2)}, u32[]{:S(2)}) %all-to-all-start.6) | async-done | bytes 163872 | tf_op jit(solution)/shard_map/all_to_all | solution.py:331
  230.1 0.3 convolution_bitcast_fusion
  230.4 0.9 fusion.2
  (48 shorter events, 0.8 us)
Async XLA Ops:
  2.1 11.0 %copy-start.1 = (bf16[1,2048,256]{2,1,0:T(8,128)(2,1)S(1)}, bf16[1,2048,256]{2,1,0:T(8,128)(2,1)}, u32[]{:S(2)}) copy-start(bf16[1,2048,256]{2,1,0:T(8,128)(2,1)} %param.21) | copy-start | bytes 3145732
  2.1 13.9 %copy-start.5 = (bf16[128,256]{1,0:T(8,128)(2,1)S(1)}, bf16[128,256]{1,0:T(8,128)(2,1)}, u32[]{:S(2)}) copy-start(bf16[128,256]{1,0:T(8,128)(2,1)} %get-tuple-element.21.refs_0_) | copy-start | bytes 196612
  2.1 43.0 %all-to-all-start = ((bf16[8,288,256]{2,1,0:T(8,128)(2,1)}), bf16[8,288,256]{2,1,0:T(8,128)(2,1)S(1)}, u32[]{:S(2)}, u32[]{:S(2)}) async-start(bf16[8,288,256]{2,1,0:T(8,128)(2,1)} %get-tuple-element.20), calls=%async_computation | async-start | bytes 2359296 | tf_op jit(solution)/shard_map/all_to_all | solution.py:221
  13.1 68.8 %collective-permute-start.4 = (bf16[2048,256]{1,0:T(8,128)(2,1)S(1)}, bf16[2048,256]{1,0:T(8,128)(2,1)S(1)}, u32[]{:S(2)}, u32[]{:S(2)}) collective-permute-start(bf16[2048,256]{1,0:T(8,128)(2,1)S(1)} %bitcast.43), channel_id=1, source_target_pairs={{0,1},{1,0},{2,3},{3,2},{4,5},{5,4},{6,7},{7,6},{8,9},{9,8},{10,11... | collective-permute-start | bytes 3145736 | tf_op jit(solution)/shard_map/ppermute | solution.py:23
  15.9 11.2 %collective-permute-start = (bf16[128,256]{1,0:T(8,128)(2,1)S(1)}, bf16[128,256]{1,0:T(8,128)(2,1)S(1)}, u32[]{:S(2)}, u32[]{:S(2)}) collective-permute-start(bf16[128,256]{1,0:T(8,128)(2,1)S(1)} %copy-done.5), channel_id=1, source_target_pairs={{0,16},{16,32},{32,48},{48,0},{1,17},{17,33},{33,49},{49,1},{2,18}... | collective-permute-start | bytes 196616 | tf_op jit(solution)/shard_map/ppermute | solution.py:223
  19.1 8.1 %collective-permute-start.1 = (bf16[128,256]{1,0:T(8,128)(2,1)S(1)}, bf16[128,256]{1,0:T(8,128)(2,1)S(1)}, u32[]{:S(2)}, u32[]{:S(2)}) collective-permute-start(bf16[128,256]{1,0:T(8,128)(2,1)S(1)} %copy-done.5), channel_id=1, source_target_pairs={{0,32},{16,48},{32,0},{48,16},{1,33},{17,49},{33,1},{49,17},{2,34}... | collective-permute-start | bytes 196616 | tf_op jit(solution)/shard_map/ppermute | solution.py:223
  23.4 5.3 %collective-permute-start.2 = (bf16[128,256]{1,0:T(8,128)(2,1)S(1)}, bf16[128,256]{1,0:T(8,128)(2,1)S(1)}, u32[]{:S(2)}, u32[]{:S(2)}) collective-permute-start(bf16[128,256]{1,0:T(8,128)(2,1)S(1)} %copy-done.5), channel_id=1, source_target_pairs={{0,48},{16,0},{32,16},{48,32},{1,49},{17,1},{33,17},{49,33},{2,50}... | collective-permute-start | bytes 196616 | tf_op jit(solution)/shard_map/ppermute | solution.py:223
  27.1 18.0 %copy-start.6 = (bf16[128,256]{1,0:T(8,128)(2,1)}, bf16[128,256]{1,0:T(8,128)(2,1)S(1)}, u32[]{:S(2)}) copy-start(bf16[128,256]{1,0:T(8,128)(2,1)S(1)} %collective-permute-done.refs_1_) | copy-start | bytes 196612
  27.2 18.0 %copy-start.7 = (bf16[128,256]{1,0:T(8,128)(2,1)}, bf16[128,256]{1,0:T(8,128)(2,1)S(1)}, u32[]{:S(2)}) copy-start(bf16[128,256]{1,0:T(8,128)(2,1)S(1)} %collective-permute-done.1.refs_2_) | copy-start | bytes 196612
  28.7 16.4 %copy-start.8 = (bf16[128,256]{1,0:T(8,128)(2,1)}, bf16[128,256]{1,0:T(8,128)(2,1)S(1)}, u32[]{:S(2)}) copy-start(bf16[128,256]{1,0:T(8,128)(2,1)S(1)} %collective-permute-done.2.refs_3_) | copy-start | bytes 196612
  45.1 1.0 copy-start
  55.2 20.6 %copy-start.2 = (bf16[1,2048,256]{2,1,0:T(8,128)(2,1)S(1)}, bf16[1,2048,256]{2,1,0:T(8,128)(2,1)}, u32[]{:S(2)}) copy-start(bf16[1,2048,256]{2,1,0:T(8,128)(2,1)} %param.22) | copy-start | bytes 3145732
  69.1 16.0 %collective-permute-start.3 = (bf16[8,256,128]{2,1,0:T(8,128)(2,1)}, bf16[8,256,128]{2,1,0:T(8,128)(2,1)S(1)}, u32[]{:S(2)}, u32[]{:S(2)}) collective-permute-start(bf16[8,256,128]{2,1,0:T(8,128)(2,1)} %get-tuple-element.23), channel_id=1, source_target_pairs={{0,1},{1,0},{2,3},{3,2},{4,5},{5,4},{6,7},{7,6},{8,9},{9,8},{10,11... | collective-permute-start | bytes 1572872 | tf_op jit(solution)/shard_map/ppermute | solution.py:23
  72.6 22.2 %collective-permute-start.7 = (bf16[2048,256]{1,0:T(8,128)(2,1)S(1)}, bf16[2048,256]{1,0:T(8,128)(2,1)}, u32[]{:S(2)}, u32[]{:S(2)}) collective-permute-start(bf16[2048,256]{1,0:T(8,128)(2,1)S(1)} %bitcast.44), channel_id=1, source_target_pairs={{0,14},{1,3},{2,0},{3,5},{4,2},{5,7},{6,4},{7,9},{8,6},{9,11},{10,... | collective-permute-start | bytes 3145736 | tf_op jit(solution)/shard_map/ppermute | solution.py:231
  75.8 19.0 %collective-permute-start.5 = (bf16[2048,256]{1,0:T(8,128)(2,1)S(1)}, bf16[2048,256]{1,0:T(8,128)(2,1)}, u32[]{:S(2)}, u32[]{:S(2)}) collective-permute-start(bf16[2048,256]{1,0:T(8,128)(2,1)S(1)} %bitcast.46), channel_id=1, source_target_pairs={{0,1},{1,0},{2,3},{3,2},{4,5},{5,4},{6,7},{7,6},{8,9},{9,8},{10,11... | collective-permute-start | bytes 3145736 | tf_op jit(solution)/shard_map/ppermute | solution.py:23
  79.9 24.8 %collective-permute-start.8 = (bf16[2048,256]{1,0:T(8,128)(2,1)S(1)}, bf16[2048,256]{1,0:T(8,128)(2,1)}, u32[]{:S(2)}, u32[]{:S(2)}) collective-permute-start(bf16[2048,256]{1,0:T(8,128)(2,1)S(1)} %bitcast.47), channel_id=1, source_target_pairs={{0,14},{1,3},{2,0},{3,5},{4,2},{5,7},{6,4},{7,9},{8,6},{9,11},{10,... | collective-permute-start | bytes 3145736 | tf_op jit(solution)/shard_map/ppermute | solution.py:231
  81.8 7.6 %copy-start.3 = (bf16[2048,256]{1,0:T(8,128)(2,1)}, bf16[2048,256]{1,0:T(8,128)(2,1)S(1)}, u32[]{:S(2)}) copy-start(bf16[2048,256]{1,0:T(8,128)(2,1)S(1)} %collective-permute-done.4.refs_1_) | copy-start | bytes 3145732
  81.8 12.9 %collective-permute-start.6 = (bf16[256,2048]{1,0:T(8,128)(2,1)}, bf16[256,2048]{1,0:T(8,128)(2,1)}, u32[]{:S(2)}, u32[]{:S(2)}) collective-permute-start(bf16[256,2048]{1,0:T(8,128)(2,1)} %bitcast.6.refs_8_), channel_id=1, source_target_pairs={{0,1},{1,0},{2,3},{3,2},{4,5},{5,4},{6,7},{7,6},{8,9},{9,8},{10,11... | collective-permute-start | bytes 3145736 | tf_op jit(solution)/shard_map/ppermute | solution.py:23
  85.1 32.9 %collective-permute-start.9 = (bf16[256,2048]{1,0:T(8,128)(2,1)}, bf16[256,2048]{1,0:T(8,128)(2,1)}, u32[]{:S(2)}, u32[]{:S(2)}) collective-permute-start(bf16[256,2048]{1,0:T(8,128)(2,1)} %bitcast.6.refs_8_), channel_id=1, source_target_pairs={{0,14},{1,3},{2,0},{3,5},{4,2},{5,7},{6,4},{7,9},{8,6},{9,11},{10,... | collective-permute-start | bytes 3145736 | tf_op jit(solution)/shard_map/ppermute | solution.py:231
  87.4 43.3 %copy-start.9 = (s32[256,2]{0,1:T(2,128)S(1)}, s32[256,2]{0,1:T(2,128)}, u32[]{:S(2)}) copy-start(s32[256,2]{0,1:T(2,128)} %param.19) | copy-start | bytes 6148
  89.4 35.0 %all-to-all-start.2 = ((bf16[8,256,128]{2,1,0:T(8,128)(2,1)}), bf16[8,256,128]{2,1,0:T(8,128)(2,1)S(1)}, u32[]{:S(2)}, u32[]{:S(2)}) async-start(bf16[8,256,128]{2,1,0:T(8,128)(2,1)} %add_convert_fusion), calls=%async_computation.2 | async-start | bytes 1048576 | tf_op jit(solution)/shard_map/all_to_all | solution.py:280
  124.4 22.8 %collective-permute-start.10 = (bf16[2048,256]{1,0:T(8,128)(2,1)}, bf16[2048,256]{1,0:T(8,128)(2,1)}, u32[]{:S(2)}, u32[]{:S(2)}) collective-permute-start(bf16[2048,256]{1,0:T(8,128)(2,1)} %collective-permute-done.7.refs_2_), channel_id=1, source_target_pairs={{0,1},{1,0},{2,3},{3,2},{4,5},{5,4},{6,7},{7,6},{8,9},{9,8},{10,11... | collective-permute-start | bytes 3145736 | tf_op jit(solution)/shard_map/ppermute | solution.py:23
  126.3 20.8 %collective-permute-start.11 = (bf16[2048,256]{1,0:T(8,128)(2,1)}, bf16[2048,256]{1,0:T(8,128)(2,1)}, u32[]{:S(2)}, u32[]{:S(2)}) collective-permute-start(bf16[2048,256]{1,0:T(8,128)(2,1)} %collective-permute-done.8.refs_6_), channel_id=1, source_target_pairs={{0,1},{1,0},{2,3},{3,2},{4,5},{5,4},{6,7},{7,6},{8,9},{9,8},{10,11... | collective-permute-start | bytes 3145736 | tf_op jit(solution)/shard_map/ppermute | solution.py:23
  128.8 18.4 %collective-permute-start.12 = (bf16[256,2048]{1,0:T(8,128)(2,1)}, bf16[256,2048]{1,0:T(8,128)(2,1)}, u32[]{:S(2)}, u32[]{:S(2)}) collective-permute-start(bf16[256,2048]{1,0:T(8,128)(2,1)} %collective-permute-done.9.refs_10_), channel_id=1, source_target_pairs={{0,1},{1,0},{2,3},{3,2},{4,5},{5,4},{6,7},{7,6},{8,9},{9,8},{10,11... | collective-permute-start | bytes 3145736 | tf_op jit(solution)/shard_map/ppermute | solution.py:23
  131.0 0.8 copy-start.4
  132.9 14.3 %all-to-all-start.3 = ((bf16[32,20,128]{2,1,0:T(8,128)(2,1)}), bf16[32,20,128]{2,1,0:T(8,128)(2,1)S(1)}, u32[]{:S(2)}, u32[]{:S(2)}) async-start(bf16[32,20,128]{2,1,0:T(8,128)(2,1)} %reshape.38), calls=%async_computation.3 | async-start | bytes 393216 | tf_op jit(solution)/shard_map/all_to_all | solution.py:287
  147.3 5.1 %collective-permute-start.13 = (bf16[2,160,128]{2,1,0:T(8,128)(2,1)S(1)}, bf16[2,160,128]{2,1,0:T(8,128)(2,1)S(1)}, u32[]{:S(2)}, u32[]{:S(2)}) collective-permute-start(bf16[2,160,128]{2,1,0:T(8,128)(2,1)S(1)} %get-tuple-element.40), channel_id=1, source_target_pairs={{0,1},{1,0},{2,3},{3,2},{4,5},{5,4},{6,7},{7,6},{8,9},{9,8},{10,11... | collective-permute-start | bytes 245768 | tf_op jit(solution)/shard_map/ppermute | solution.py:23
  209.1 10.5 %copy-start.10 = (f32[256,2]{0,1:T(2,128)S(1)}, f32[256,2]{0,1:T(2,128)}, u32[]{:S(2)}) copy-start(f32[256,2]{0,1:T(2,128)} %param.20) | copy-start | bytes 6148
  209.2 5.8 %collective-permute-start.14 = (bf16[2,160,128]{2,1,0:T(8,128)(2,1)S(1)}, bf16[2,160,128]{2,1,0:T(8,128)(2,1)S(1)}, u32[]{:S(2)}, u32[]{:S(2)}) collective-permute-start(bf16[2,160,128]{2,1,0:T(8,128)(2,1)S(1)} %bitcast.49), channel_id=1, source_target_pairs={{0,1},{1,0},{2,3},{3,2},{4,5},{5,4},{6,7},{7,6},{8,9},{9,8},{10,11... | collective-permute-start | bytes 245768 | tf_op jit(solution)/shard_map/ppermute | solution.py:23
  215.7 14.4 %all-to-all-start.6 = ((bf16[32,20,128]{2,1,0:T(8,128)(2,1)}), bf16[32,20,128]{2,1,0:T(8,128)(2,1)S(1)}, u32[]{:S(2)}, u32[]{:S(2)}) async-start(bf16[32,20,128]{2,1,0:T(8,128)(2,1)} %reshape.43), calls=%async_computation.6 | async-start | bytes 393216 | tf_op jit(solution)/shard_map/all_to_all | solution.py:331

commit v4 on v3

--- a/solution.py
+++ b/solution.py
@@ -133,46 +133,72 @@
         other_ref[block] = full_ref[:, pl.ds(far, lane)]
 
 
-def expert_kernel(place_ref, rows_in_ref, gain_ref, *refs):
-    sets = (len(refs) - 8) // 3
-    gate_refs, up_refs, down_refs = refs[:sets], refs[sets : 2 * sets], refs[2 * sets : 3 * sets]
-    out_ref, rows_ref, hidden_ref, full_ref, gates, ups, downs, sems = refs[3 * sets :]
-    core = place_ref[2]
+def pack_weights_kernel(gate_ref, up_ref, down_ref, out_ref, sems):
+    units = gate_ref.shape[1]
+    copies = [
+        pltpu.make_async_copy(gate_ref, out_ref.at[0], sems.at[0]),
+        pltpu.make_async_copy(up_ref, out_ref.at[1], sems.at[1]),
+    ]
+    for block in range(down_ref.shape[1] // units):
+        columns = pl.ds(block * units, units)
+        copies.append(
+            pltpu.make_async_copy(
+                down_ref.at[:, columns], out_ref.at[2, columns, :], sems.at[2 + block]
+            )
+        )
+    for copy in copies:
+        copy.start()
+    for copy in copies:
+        copy.wait()
+
+
+def expert_kernel(rows_in_ref, gain_ref, *refs):
+    sets = len(refs) - 8
+    set_refs = refs[:sets]
+    out_ref, rows_ref, hidden_ref, full_ref, gates, ups, downs, sems = refs[sets:]
     blocks = rows_in_ref.shape[0]
     width = rows_ref.shape[1]
     units = gates.shape[2]
-    copies = []
+    gate_copies, up_copies, down_copies = [], [], []
     for part in range(sets):
-        for kind, (sources, target) in enumerate(((gate_refs, gates), (up_refs, ups), (down_refs, downs))):
-            copy = pltpu.make_async_copy(sources[part], target.at[part], sems.at[kind, part])
-            copy.start()
-            copies.append(copy)
-    squares = jnp.zeros(rows_in_ref.shape[2:], jnp.float32)
+        gate_copies.append(
+            pltpu.make_async_copy(set_refs[part].at[0], gates.at[part], sems.at[part, 0])
+        )
+        up_copies.append(pltpu.make_async_copy(set_refs[part].at[1], ups.at[part], sems.at[part, 1]))
+        gate_copies[part].start()
+        up_copies[part].start()
+    for part in range(sets):
+        for block in range(width // units):
+            columns = pl.ds(block * units, units)
+            down_copies.append(
+                pltpu.make_async_copy(
+                    set_refs[part].at[2, columns, :], downs.at[part, :, columns], sems.at[part, 2 + block]
+                )
+            )
+            down_copies[-1].start()
+    squares = jnp.zeros(rows_in_ref.shape[1:], jnp.float32)
     for block in range(blocks):
-        for side in range(2):
-            values = rows_in_ref[block, side].astype(jnp.float32)
-            squares = squares + values * values
+        values = rows_in_ref[block].astype(jnp.float32)
+        squares = squares + values * values
     scale = lax.rsqrt(jnp.sum(squares, axis=1, keepdims=True) / width + norm_eps)
     for block in range(blocks):
-        for side, at in ((0, core), (1, 1 - core)):
-            index = block * 2 + at
-            values = rows_in_ref[block, side].astype(jnp.float32) * scale * gain_ref[index]
-            rows_ref[:, pl.ds(pl.multiple_of(index * lane, lane), lane)] = values.astype(jnp.bfloat16)
+        values = rows_in_ref[block].astype(jnp.float32) * scale * gain_ref[block]
+        rows_ref[:, block * lane : (block + 1) * lane] = values.astype(jnp.bfloat16)
     for part in range(sets):
-        copies[3 * part].wait()
+        gate_copies[part].wait()
         gate = jnp.dot(rows_ref[...], gates[part], preferred_element_type=jnp.float32)
-        copies[3 * part + 1].wait()
+        up_copies[part].wait()
         up = jnp.dot(rows_ref[...], ups[part], preferred_element_type=jnp.float32)
         hidden_ref[:, part * units : (part + 1) * units] = (
             gate / (1.0 + jnp.exp(-gate)) * up
         ).astype(jnp.bfloat16)
-        copies[3 * part + 2].wait()
+    for copy in down_copies:
+        copy.wait()
     full_ref[...] = jnp.dot(
         hidden_ref[...], downs[...].reshape(sets * units, width), preferred_element_type=jnp.float32
     ).astype(jnp.bfloat16)
-    out_width = out_ref.shape[2]
     for block in range(blocks):
-        out_ref[block] = full_ref[:, block * out_width : (block + 1) * out_width]
+        out_ref[block] = full_ref[:, block * lane : (block + 1) * lane]
 
 
 def shards(
@@ -227,9 +253,21 @@
     for y_from in range(y_count):
         slice_moves.append((2 * y_from, 2 * ((y_from - 1) % y_count)))
         slice_moves.append((2 * y_from + 1, 2 * ((y_from + 1) % y_count) + 1))
-    own_set = (gate_weight[0], up_weight[0], down_weight[0])
-    near_set = tuple(lax.ppermute(weight, TP, slice_moves) for weight in own_set)
-    own_swapped = tuple(swapped(weight) for weight in own_set)
+    hidden_units = gate_weight.shape[2]
+    any_space = pl.BlockSpec(memory_space=pl.ANY)
+    down_blocks = model_width // hidden_units
+    own_set = pl.pallas_call(
+        pack_weights_kernel,
+        out_shape=jax.ShapeDtypeStruct((3, model_width, hidden_units), bf16),
+        in_specs=[any_space] * 3,
+        out_specs=any_space,
+        scratch_shapes=[pltpu.SemaphoreType.DMA((2 + down_blocks,))],
+        name="pack_weights",
+        interpret=INTERPRET,
+    )(gate_weight[0], up_weight[0], down_weight[0])
+    near_set = lax.ppermute(own_set, TP, slice_moves)
+    own_swapped = swapped(own_set)
+    near_swapped = swapped(near_set)
     attend = pl.pallas_call(
         functools.partial(attend_kernel, head_count, head_width),
         out_shape=jax.ShapeDtypeStruct((x_count, head_count * deep, token_count), bf16),
@@ -278,8 +316,10 @@
     )(place, received, out_weight)
     paired = (mine.astype(f32) + swapped(other).astype(f32)).astype(bf16)
     pieces = lax.all_to_all(paired, "y", split_axis=0, concat_axis=0, tiled=True)
-    pieces, own_swapped, near_set = lax.optimization_barrier((pieces, own_swapped, near_set))
-    near_swapped = tuple(swapped(weight) for weight in near_set)
+    pieces, own_swapped, near_set, near_swapped = lax.optimization_barrier(
+        (pieces, own_swapped, near_set, near_swapped)
+    )
+    weight_sets = [own_set, own_swapped, near_set, near_swapped]
     head_sum = jnp.sum(pieces.astype(f32), axis=0)
     stream = (residual.astype(f32) + head_sum).astype(bf16)
 
@@ -287,26 +327,17 @@
     arrived = lax.all_to_all(
         sent.reshape(sp_count, capacity, local_width), SP, split_axis=0, concat_axis=0, tiled=True
     )
-    arrived, near_swapped = lax.optimization_barrier((arrived, near_swapped))
-    weight_sets = [own_set, own_swapped, near_set, near_swapped]
     quarter = slot_total // 4
-    arrived = arrived.reshape(2, 2, quarter, local_width)
-    core = place[2]
-    mine = lax.dynamic_index_in_dim(arrived, core, 1, keepdims=False)
-    other = lax.dynamic_index_in_dim(arrived, 1 - core, 1, keepdims=False)
-    both = jnp.stack([mine, swapped(other)], axis=1)
-    both = jnp.broadcast_to(both, (y_count // 2, *both.shape))
+    arrived = arrived.reshape(4, quarter, local_width)
+    copies = jnp.broadcast_to(arrived, (y_count // 2, *arrived.shape))
     rows = lax.all_to_all(
-        both.reshape(y_count, 2, quarter, local_width), "y", split_axis=0, concat_axis=0, tiled=True
-    )
-    weights = [kind[part] for kind in zip(*weight_sets) for part in range(len(weight_sets))]
+        copies.reshape(2 * y_count, quarter, local_width), TP, split_axis=0, concat_axis=0, tiled=True
+    )
     sets = len(weight_sets)
-    hidden_units = gate_weight.shape[2]
-    any_space = pl.BlockSpec(memory_space=pl.ANY)
     out_rows = pl.pallas_call(
         expert_kernel,
-        out_shape=jax.ShapeDtypeStruct((y_count, quarter, 2 * local_width), bf16),
-        in_specs=[smem, vmem, vmem] + [any_space] * (3 * sets),
+        out_shape=jax.ShapeDtypeStruct((2 * y_count, quarter, local_width), bf16),
+        in_specs=[vmem, vmem] + [any_space] * sets,
         out_specs=vmem,
         scratch_shapes=[
             pltpu.VMEM((quarter, model_width), bf16),
@@ -315,19 +346,15 @@
             pltpu.VMEM((sets, model_width, hidden_units), bf16),
             pltpu.VMEM((sets, model_width, hidden_units), bf16),
             pltpu.VMEM((sets, hidden_units, model_width), bf16),
-            pltpu.SemaphoreType.DMA((3, sets)),
+            pltpu.SemaphoreType.DMA((sets, 2 + down_blocks)),
         ],
         name="expert",
         interpret=INTERPRET,
-    )(place, rows, norm_gain.reshape(2 * y_count, 1, lane), *weights)
-    pieces = lax.all_to_all(out_rows, "y", split_axis=0, concat_axis=0, tiled=True)
-    summed = jnp.sum(
-        pieces.reshape(y_count // 2, 2, quarter, 2, local_width).astype(f32), axis=0
+    )(rows, norm_gain.reshape(2 * y_count, 1, lane), *weight_sets)
+    pieces = lax.all_to_all(out_rows, TP, split_axis=0, concat_axis=0, tiled=True)
+    expert_out = jnp.sum(
+        pieces.reshape(y_count // 2, 4, quarter, local_width).astype(f32), axis=0
     ).astype(bf16)
-    mine = lax.dynamic_index_in_dim(summed, core, 2, keepdims=False)
-    got = swapped(lax.dynamic_index_in_dim(summed, 1 - core, 2, keepdims=False))
-    first = core == 0
-    expert_out = jnp.stack([jnp.where(first, mine, got), jnp.where(first, got, mine)], axis=1)
     back = lax.all_to_all(
         expert_out.reshape(sp_count, capacity, local_width), SP, split_axis=0, concat_axis=0, tiled=True
     ).reshape(slot_total, local_width)

time: 233 us -> 307 us (1.32)
  Pallas kernels: 22 us -> 119 us
  starting transfers between devices: 71.1 us -> 45.7 us
  blocking collectives: 58.2 us -> 80.1 us
  waiting for transfers between devices: 70.3 us -> 53.3 us
    pallas_call x1 -> x2, Pallas kernels: 8.06 us -> 105 us  [the longest x1 96.5 us: shards(): pl.pallas_call(pack_weights_kernel, out_shape=jax.ShapeDtypeStruct((3, mo...]
    all_to_all x2 -> x3, blocking collectives: 47.1 us -> 70.1 us  [the longest x1 25.6 us: shards(): lax.all_to_all(copies.reshape(2 * y_count, quarter, local_width), TP, spl...]
    all_to_all x1, waiting for transfers between devices: 16.4 us -> 0.01 us  [shards(): lax.all_to_all(message, 'z', split_axis=0, concat_axis=0, tiled=True)]
    ppermute x9 -> x3, starting transfers between devices: 29 us -> 17 us  [swapped(): return lax.ppermute(shard, 'c', [(0, 1), (1, 0)])]
    all_to_all x1, waiting for transfers between devices: 6.39 us -> 17.3 us  [shards(): lax.all_to_all(paired, 'y', split_axis=0, concat_axis=0, tiled=True)]
    all_to_all x1 -> x0, waiting for transfers between devices: 10.5 us -> none  [shards(): lax.all_to_all(sent.reshape(sp_count, capacity, local_width), SP, split_a...]
    all_to_all x1 -> x0, starting transfers between devices: 3.87 us -> none  [shards(): lax.all_to_all(sent.reshape(sp_count, capacity, local_width), SP, split_a...]
    ppermute x3 -> x1, waiting for transfers between devices: 23.2 us -> 19.7 us  [shards(): near_set = lax.ppermute(own_set, TP, slice_moves)]
  transfers between devices with their start and end apart: 19 -> 10, of which waited for: 9 -> 6; matrix products, arithmetic and copies ran while one was open for 2% -> 1% of each run, Pallas kernels for 5% -> 5%
where the time goes in v4:
time: 307 us; the launch traced here: 306 us
  Pallas kernels  119 us (39%)
  blocking collectives  80.1 us (26%)
  waiting for transfers between devices  53.3 us (17%)
  starting transfers between devices  45.7 us (15%)
    pallas_call x1, Pallas kernels, shards(): pl.pallas_call(pack_weights_kernel, out_shape=jax.ShapeDtypeStruct((3, mo...  96.5 us
    all_to_all x1, blocking collectives, shards(): lax.all_to_all(copies.reshape(2 * y_count, quarter, local_width), TP, spl...  25.6 us
    all_to_all x1, blocking collectives, shards(): lax.all_to_all(out_rows, TP, split_axis=0, concat_axis=0, tiled=True)  23.2 us
    all_to_all x1, blocking collectives, shards(): lax.all_to_all(sent.reshape(sp_count, capacity, local_width), SP, split_a...  21.3 us
    ppermute x1, waiting for transfers between devices, shards(): near_set = lax.ppermute(own_set, TP, slice_moves)  19.7 us
    all_to_all x1, waiting for transfers between devices, shards(): lax.all_to_all(paired, 'y', split_axis=0, concat_axis=0, tiled=True)  17.3 us
    ppermute x3, starting transfers between devices, swapped(): return lax.ppermute(shard, 'c', [(0, 1), (1, 0)])  17 us
    all_to_all x1, waiting for transfers between devices, shards(): lax.all_to_all(expert_out.reshape(sp_count, capacity, local_width), SP, s...  11 us
  transfers between devices with their start and end apart: 10, of which 6 were waited for; matrix products, arithmetic and copies ran while one was open for 1% of the time, Pallas kernels for 5%

profile of v4, /device:TPU:1, one launch (start us, length us, event | category | flops | bytes accessed | tf_op | source)
XLA Modules:
  0.0 305.8 jit_solution(15164964761424724884)
XLA Ops:
  0.0 96.5 %pack_weights.1.refs_0_ = bf16[3,2048,256]{2,1,0:T(8,128)(2,1)} custom-call(bf16[2048,256]{1,0:T(8,128)(2,1)} %bitcast.25, bf16[2048,256]{1,0:T(8,128)(2,1)} %bitcast.26, bf16[256,2048]{1,0:T(8,128)(2,1)} %bitcast.27), custom_call_target="tpu_custom_call" | custom-call | tf_op jit(solution)/shard_map/pack_weights/pallas_call | solution.py:259
  96.5 4.0 %collective-permute-start.5 = (bf16[3,2048,256]{2,1,0:T(8,128)(2,1)}, bf16[3,2048,256]{2,1,0:T(8,128)(2,1)}, u32[]{:S(2)}, u32[]{:S(2)}) collective-permute-start(bf16[3,2048,256]{2,1,0:T(8,128)(2,1)} %pack_weights.1.refs_0_), channel_id=1, source_target_pairs={{0,14},{1,3},{2,0},{3,5},{4,2},{5,7},{6,4},{7,9},{8,6},{9,11},{10,... | collective-permute-start | bytes 9437192 | tf_op jit(solution)/shard_map/ppermute | solution.py:268
  100.5 2.1 pack.1
  102.6 10.0 %all-to-all-start = ((bf16[8,288,256]{2,1,0:T(8,128)(2,1)}), bf16[8,288,256]{2,1,0:T(8,128)(2,1)S(1)}, u32[]{:S(2)}, u32[]{:S(2)}) async-start(bf16[8,288,256]{2,1,0:T(8,128)(2,1)} %get-tuple-element.13), calls=%async_computation | async-start | bytes 2359296 | tf_op jit(solution)/shard_map/all_to_all | solution.py:247
  112.7 5.0 %collective-permute-start.4 = (bf16[3,2048,256]{2,1,0:T(8,128)(2,1)}, bf16[3,2048,256]{2,1,0:T(8,128)(2,1)}, u32[]{:S(2)}, u32[]{:S(2)}) collective-permute-start(bf16[3,2048,256]{2,1,0:T(8,128)(2,1)} %pack_weights.1.refs_0_), channel_id=1, source_target_pairs={{0,1},{1,0},{2,3},{3,2},{4,5},{5,4},{6,7},{7,6},{8,9},{9,8},{10,11... | collective-permute-start | bytes 9437192 | tf_op jit(solution)/shard_map/ppermute | solution.py:23
  117.7 19.7 %collective-permute-done.5.refs_2_ = bf16[3,2048,256]{2,1,0:T(8,128)(2,1)} collective-permute-done((bf16[3,2048,256]{2,1,0:T(8,128)(2,1)}, bf16[3,2048,256]{2,1,0:T(8,128)(2,1)}, u32[]{:S(2)}, u32[]{:S(2)}) %collective-permute-start.5) | collective-permute-done | bytes 3145760 | tf_op jit(solution)/shard_map/ppermute | solution.py:268
  137.4 7.3 %collective-permute-start.6 = (bf16[3,2048,256]{2,1,0:T(8,128)(2,1)}, bf16[3,2048,256]{2,1,0:T(8,128)(2,1)}, u32[]{:S(2)}, u32[]{:S(2)}) collective-permute-start(bf16[3,2048,256]{2,1,0:T(8,128)(2,1)} %collective-permute-done.5.refs_2_), channel_id=1, source_target_pairs={{0,1},{1,0},{2,3},{3,2},{4,5},{5,4},{6,7},{7,6},{8,9},{9,8},{10,11... | collective-permute-start | bytes 9437192 | tf_op jit(solution)/shard_map/ppermute | solution.py:23
  144.7 1.9 collective-permute-start.2
  146.6 1.9 collective-permute-start.1
  148.6 3.4 %collective-permute-start = (bf16[128,256]{1,0:T(8,128)(2,1)}, bf16[128,256]{1,0:T(8,128)(2,1)S(1)}, u32[]{:S(2)}, u32[]{:S(2)}) collective-permute-start(bf16[128,256]{1,0:T(8,128)(2,1)} %get-tuple-element.14.refs_0_), channel_id=1, source_target_pairs={{0,16},{16,32},{32,48},{48,0},{1,17},{17,33},{33,49},{49,1},{2,18}... | collective-permute-start | bytes 196616 | tf_op jit(solution)/shard_map/ppermute | solution.py:249
  151.9 0.6 pad_add_fusion.place_ref
  152.6 0.0 collective-permute-done.2.refs_3_
  152.6 1.3 collective-permute-done.1.refs_2_
  153.9 2.3 collective-permute-done.refs_1_
  156.2 0.0 all-to-all-done.kv_ref
  156.2 0.0 copy-done.2
  156.2 0.6 copy-done.4
  156.8 1.1 copy-done
  157.9 9.1 %attend.1 = bf16[4,160,256]{2,1,0:T(8,128)(2,1)} custom-call(s32[4]{0:T(128)} %pad_add_fusion.place_ref, bf16[8,288,256]{2,1,0:T(8,128)(2,1)} %copy-done, bf16[128,256]{1,0:T(8,128)(2,1)} %get-tuple-element.14.refs_0_, bf16[128,256]{1,0:T(8,128)(2,1)} %copy-done.4, bf16[128,256]{1,0:T(8,128)(2,1)} %copy-done.3, bf16[128,256]{1,0:T(8,128)(2,1)} %copy-done.2), custom_call_target="tpu_custom_call" | custom-call | tf_op jit(solution)/shard_map/attend/pallas_call | solution.py:284
  166.9 10.0 %all_to_all.35.parts_ref = bf16[4,160,256]{2,1,0:T(8,128)(2,1)} all-to-all(bf16[4,160,256]{2,1,0:T(8,128)(2,1)} %attend.1), channel_id=1, replica_groups=mesh['z'=8,'x'=4,'y'=8,'c'=2] {'x'}, dimensions={0} | all-to-all | bytes 655360 | tf_op jit(solution)/shard_map/all_to_all | solution.py:285
  177.0 2.8 project.1
  179.8 4.6 %collective-permute-start.3 = (bf16[8,256,128]{2,1,0:T(8,128)(2,1)}, bf16[8,256,128]{2,1,0:T(8,128)(2,1)S(1)}, u32[]{:S(2)}, u32[]{:S(2)}) collective-permute-start(bf16[8,256,128]{2,1,0:T(8,128)(2,1)} %get-tuple-element.16), channel_id=1, source_target_pairs={{0,1},{1,0},{2,3},{3,2},{4,5},{5,4},{6,7},{7,6},{8,9},{9,8},{10,11... | collective-permute-start | bytes 1572872 | tf_op jit(solution)/shard_map/ppermute | solution.py:23
  184.4 1.7 collective-permute-done.3
  186.2 2.0 add_convert_fusion
  188.1 3.6 %all-to-all-start.2 = ((bf16[8,256,128]{2,1,0:T(8,128)(2,1)}), bf16[8,256,128]{2,1,0:T(8,128)(2,1)S(1)}, u32[]{:S(2)}, u32[]{:S(2)}) async-start(bf16[8,256,128]{2,1,0:T(8,128)(2,1)} %add_convert_fusion), calls=%async_computation.2 | async-start | bytes 1048576 | tf_op jit(solution)/shard_map/all_to_all | solution.py:318
  191.7 0.1 eq.62
  191.8 0.0 copy-done.5
  191.8 0.1 and.15
  191.9 0.1 and.16
  192.0 0.2 convolution_convert_fusion.1
  192.2 0.1 eq.59
  192.2 0.1 eq.60
  192.3 0.0 collective-permute-done.4.refs_1_
  192.3 17.3 %all-to-all-done.2 = bf16[8,256,128]{2,1,0:T(8,128)(2,1)S(1)} async-done(((bf16[8,256,128]{2,1,0:T(8,128)(2,1)}), bf16[8,256,128]{2,1,0:T(8,128)(2,1)S(1)}, u32[]{:S(2)}, u32[]{:S(2)}) %all-to-all-start.2) | async-done | bytes 524320 | tf_op jit(solution)/shard_map/all_to_all | solution.py:318
  209.7 0.0 collective-permute-done.6.refs_3_
  209.7 0.1 convert_reduce_fusion
  209.7 0.3 convolution_convert_fusion
  210.1 21.3 %all_to_all.36 = bf16[32,20,128]{2,1,0:T(8,128)(2,1)S(1)} all-to-all(bf16[32,20,128]{2,1,0:T(8,128)(2,1)S(1)} %reshape.38), channel_id=1, replica_groups=mesh['z'=8,'x'=4,'y'=8,'c'=2] {'z','x'}, dimensions={0} | all-to-all | bytes 327680 | tf_op jit(solution)/shard_map/all_to_all | solution.py:327
  231.5 0.1 broadcast_in_dim.50
  231.6 25.6 %all_to_all.37.rows_in_ref = bf16[16,160,128]{2,1,0:T(8,128)(2,1)} all-to-all(bf16[16,160,128]{2,1,0:T(8,128)(2,1)S(1)} %bitcast.24), channel_id=1, replica_groups=mesh['z'=8,'x'=4,'y'=8,'c'=2] {'y','c'}, dimensions={0} | all-to-all | bytes 1310720 | tf_op jit(solution)/shard_map/all_to_all | solution.py:333
  257.1 8.4 %expert.1 = bf16[16,160,128]{2,1,0:T(8,128)(2,1)} custom-call(bf16[16,160,128]{2,1,0:T(8,128)(2,1)} %all_to_all.37.rows_in_ref, f32[16,1,128]{2,1,0:T(1,128)} %bitcast.30, bf16[3,2048,256]{2,1,0:T(8,128)(2,1)} %pack_weights.1.refs_0_, bf16[3,2048,256]{2,1,0:T(8,128)(2,1)} %collective-permute-done.4.refs_1_, ...), custom_call_target="tpu_custom_call" | custom-call | tf_op jit(solution)/shard_map/expert/pallas_call | solution.py:337
  265.6 23.2 %all_to_all.38 = bf16[16,160,128]{2,1,0:T(8,128)(2,1)S(1)} all-to-all(bf16[16,160,128]{2,1,0:T(8,128)(2,1)} %expert.1), channel_id=1, replica_groups=mesh['z'=8,'x'=4,'y'=8,'c'=2] {'y','c'}, dimensions={0} | all-to-all | bytes 1310720 | tf_op jit(solution)/shard_map/all_to_all | solution.py:354
  288.8 0.1 reduce_sum.32
  288.9 0.7 reshape.43
  289.6 3.9 %all-to-all-start.6 = ((bf16[32,20,128]{2,1,0:T(8,128)(2,1)}), bf16[32,20,128]{2,1,0:T(8,128)(2,1)S(1)}, u32[]{:S(2)}, u32[]{:S(2)}) async-start(bf16[32,20,128]{2,1,0:T(8,128)(2,1)} %reshape.43), calls=%async_computation.6 | async-start | bytes 393216 | tf_op jit(solution)/shard_map/all_to_all | solution.py:358
  293.6 11.0 %all-to-all-done.6 = bf16[32,20,128]{2,1,0:T(8,128)(2,1)S(1)} async-done(((bf16[32,20,128]{2,1,0:T(8,128)(2,1)}), bf16[32,20,128]{2,1,0:T(8,128)(2,1)S(1)}, u32[]{:S(2)}, u32[]{:S(2)}) %all-to-all-start.6) | async-done | bytes 163872 | tf_op jit(solution)/shard_map/all_to_all | solution.py:358
  304.6 0.3 convolution_bitcast_fusion
  304.9 0.9 fusion.2
  (16 shorter events, 0.1 us)
Async XLA Ops:
  96.5 40.9 %collective-permute-start.5 = (bf16[3,2048,256]{2,1,0:T(8,128)(2,1)}, bf16[3,2048,256]{2,1,0:T(8,128)(2,1)}, u32[]{:S(2)}, u32[]{:S(2)}) collective-permute-start(bf16[3,2048,256]{2,1,0:T(8,128)(2,1)} %pack_weights.1.refs_0_), channel_id=1, source_target_pairs={{0,14},{1,3},{2,0},{3,5},{4,2},{5,7},{6,4},{7,9},{8,6},{9,11},{10,... | collective-permute-start | bytes 9437192 | tf_op jit(solution)/shard_map/ppermute | solution.py:268
  102.6 53.6 %all-to-all-start = ((bf16[8,288,256]{2,1,0:T(8,128)(2,1)}), bf16[8,288,256]{2,1,0:T(8,128)(2,1)S(1)}, u32[]{:S(2)}, u32[]{:S(2)}) async-start(bf16[8,288,256]{2,1,0:T(8,128)(2,1)} %get-tuple-element.13), calls=%async_computation | async-start | bytes 2359296 | tf_op jit(solution)/shard_map/all_to_all | solution.py:247
  112.7 79.2 %copy-start.5 = (s32[256,2]{0,1:T(2,128)S(1)}, s32[256,2]{0,1:T(2,128)}, u32[]{:S(2)}) copy-start(s32[256,2]{0,1:T(2,128)} %param.19) | copy-start | bytes 6148
  112.7 79.7 %collective-permute-start.4 = (bf16[3,2048,256]{2,1,0:T(8,128)(2,1)}, bf16[3,2048,256]{2,1,0:T(8,128)(2,1)}, u32[]{:S(2)}, u32[]{:S(2)}) collective-permute-start(bf16[3,2048,256]{2,1,0:T(8,128)(2,1)} %pack_weights.1.refs_0_), channel_id=1, source_target_pairs={{0,1},{1,0},{2,3},{3,2},{4,5},{5,4},{6,7},{7,6},{8,9},{9,8},{10,11... | collective-permute-start | bytes 9437192 | tf_op jit(solution)/shard_map/ppermute | solution.py:23
  137.4 72.3 %collective-permute-start.6 = (bf16[3,2048,256]{2,1,0:T(8,128)(2,1)}, bf16[3,2048,256]{2,1,0:T(8,128)(2,1)}, u32[]{:S(2)}, u32[]{:S(2)}) collective-permute-start(bf16[3,2048,256]{2,1,0:T(8,128)(2,1)} %collective-permute-done.5.refs_2_), channel_id=1, source_target_pairs={{0,1},{1,0},{2,3},{3,2},{4,5},{5,4},{6,7},{7,6},{8,9},{9,8},{10,11... | collective-permute-start | bytes 9437192 | tf_op jit(solution)/shard_map/ppermute | solution.py:23
  144.7 7.9 %collective-permute-start.2 = (bf16[128,256]{1,0:T(8,128)(2,1)}, bf16[128,256]{1,0:T(8,128)(2,1)S(1)}, u32[]{:S(2)}, u32[]{:S(2)}) collective-permute-start(bf16[128,256]{1,0:T(8,128)(2,1)} %get-tuple-element.14.refs_0_), channel_id=1, source_target_pairs={{0,48},{16,0},{32,16},{48,32},{1,49},{17,1},{33,17},{49,33},{2,50}... | collective-permute-start | bytes 196616 | tf_op jit(solution)/shard_map/ppermute | solution.py:249
  146.6 7.2 %collective-permute-start.1 = (bf16[128,256]{1,0:T(8,128)(2,1)}, bf16[128,256]{1,0:T(8,128)(2,1)S(1)}, u32[]{:S(2)}, u32[]{:S(2)}) collective-permute-start(bf16[128,256]{1,0:T(8,128)(2,1)} %get-tuple-element.14.refs_0_), channel_id=1, source_target_pairs={{0,32},{16,48},{32,0},{48,16},{1,33},{17,49},{33,1},{49,17},{2,34}... | collective-permute-start | bytes 196616 | tf_op jit(solution)/shard_map/ppermute | solution.py:249
  148.6 7.6 %collective-permute-start = (bf16[128,256]{1,0:T(8,128)(2,1)}, bf16[128,256]{1,0:T(8,128)(2,1)S(1)}, u32[]{:S(2)}, u32[]{:S(2)}) collective-permute-start(bf16[128,256]{1,0:T(8,128)(2,1)} %get-tuple-element.14.refs_0_), channel_id=1, source_target_pairs={{0,16},{16,32},{32,48},{48,0},{1,17},{17,33},{33,49},{49,1},{2,18}... | collective-permute-start | bytes 196616 | tf_op jit(solution)/shard_map/ppermute | solution.py:249
  152.6 3.6 %copy-start.2 = (bf16[128,256]{1,0:T(8,128)(2,1)}, bf16[128,256]{1,0:T(8,128)(2,1)S(1)}, u32[]{:S(2)}) copy-start(bf16[128,256]{1,0:T(8,128)(2,1)S(1)} %collective-permute-done.2.refs_3_) | copy-start | bytes 196612
  153.9 2.3 copy-start.3
  156.2 0.6 copy-start.4
  156.8 1.1 copy-start
  179.8 29.9 %copy-start.1 = (bf16[256,128]{1,0:T(8,128)(2,1)S(1)}, bf16[256,128]{1,0:T(8,128)(2,1)}, u32[]{:S(2)}) copy-start(bf16[256,128]{1,0:T(8,128)(2,1)} %param.12) | copy-start | bytes 196612
  179.8 6.3 %collective-permute-start.3 = (bf16[8,256,128]{2,1,0:T(8,128)(2,1)}, bf16[8,256,128]{2,1,0:T(8,128)(2,1)S(1)}, u32[]{:S(2)}, u32[]{:S(2)}) collective-permute-start(bf16[8,256,128]{2,1,0:T(8,128)(2,1)} %get-tuple-element.16), channel_id=1, source_target_pairs={{0,1},{1,0},{2,3},{3,2},{4,5},{5,4},{6,7},{7,6},{8,9},{9,8},{10,11... | collective-permute-start | bytes 1572872 | tf_op jit(solution)/shard_map/ppermute | solution.py:23
  188.1 21.5 %all-to-all-start.2 = ((bf16[8,256,128]{2,1,0:T(8,128)(2,1)}), bf16[8,256,128]{2,1,0:T(8,128)(2,1)S(1)}, u32[]{:S(2)}, u32[]{:S(2)}) async-start(bf16[8,256,128]{2,1,0:T(8,128)(2,1)} %add_convert_fusion), calls=%async_computation.2 | async-start | bytes 1048576 | tf_op jit(solution)/shard_map/all_to_all | solution.py:318
  257.1 36.4 %copy-start.6 = (f32[256,2]{0,1:T(2,128)S(1)}, f32[256,2]{0,1:T(2,128)}, u32[]{:S(2)}) copy-start(f32[256,2]{0,1:T(2,128)} %param.20) | copy-start | bytes 6148
  289.6 14.9 %all-to-all-start.6 = ((bf16[32,20,128]{2,1,0:T(8,128)(2,1)}), bf16[32,20,128]{2,1,0:T(8,128)(2,1)S(1)}, u32[]{:S(2)}, u32[]{:S(2)}) async-start(bf16[32,20,128]{2,1,0:T(8,128)(2,1)} %reshape.43), calls=%async_computation.6 | async-start | bytes 393216 | tf_op jit(solution)/shard_map/all_to_all | solution.py:358

commit v5 on v4

--- a/solution.py
+++ b/solution.py
@@ -36,13 +36,13 @@
     tokens = keys_ref.shape[1]
     head_count = gates_ref.shape[0]
     row = lax.broadcasted_iota(jnp.int32, (extra_rows, tokens), 0)
-    pieces = []
+    gates = jnp.zeros((extra_rows, tokens), jnp.float32)
     for head in range(head_count):
-        gates = jnp.zeros((extra_rows, tokens), jnp.float32)
         for place, part in enumerate(three_parts(gates_ref[head : head + 1])):
-            gates = jnp.where(row == place, part, gates)
-        pieces += [keys_ref[head * head_width : (head + 1) * head_width], gates.astype(jnp.bfloat16)]
-    message = jnp.concatenate(pieces + [values_ref[...]], axis=0)
+            gates = jnp.where(row == 3 * head + place, part, gates)
+    message = jnp.concatenate(
+        [keys_ref[...], values_ref[...], gates.astype(jnp.bfloat16)], axis=0
+    )
     for copy in range(out_ref.shape[0]):
         out_ref[copy] = message
     query_ref[...] = queries_ref[...] * jnp.asarray(head_width ** (-0.5), jnp.bfloat16)
@@ -53,12 +53,11 @@
     query_refs = refs[:-4]
     tokens = kv_ref.shape[2]
     z_count, x_count = kv_ref.shape[0], len(query_refs)
-    deep = head_width + extra_rows
     z_place, x_place = place_ref[0], place_ref[1]
     row = lax.broadcasted_iota(jnp.int32, (extra_rows, tokens), 0)
-    minus = jnp.where(row < 3, -1.0, 0.0).astype(jnp.bfloat16)
     ones = jnp.ones((extra_rows, tokens), jnp.bfloat16)
     for head in range(head_count):
+        minus = jnp.where((row >= 3 * head) & (row < 3 * head + 3), -1.0, 0.0).astype(jnp.bfloat16)
         rows = slice(head * head_width, (head + 1) * head_width)
         for shift in range(x_count):
             target = lax.rem(x_place + x_count - shift, x_count)
@@ -67,11 +66,13 @@
             query_scratch[head, head_width:, columns] = minus
         for block in range(z_count):
             columns = slice(block * tokens, (block + 1) * tokens)
-            key_scratch[head, :, columns] = kv_ref[block, head * deep : (head + 1) * deep]
-            first = head_count * deep + head * head_width
+            first = (head_count + head) * head_width
+            key_scratch[head, :head_width, columns] = kv_ref[block, rows]
+            key_scratch[head, head_width:, columns] = kv_ref[block, 2 * head_count * head_width :]
             value_scratch[head, :head_width, columns] = kv_ref[block, first : first + head_width]
             value_scratch[head, head_width:, columns] = ones
     wide = 2 * tokens if x_count % 2 == 0 else tokens
+    stats = [jnp.zeros((extra_rows, tokens), jnp.float32)] * x_count
     for head in range(head_count):
         rows = slice(head * head_width, (head + 1) * head_width)
         for first in range(0, x_count * tokens, wide):
@@ -92,63 +93,82 @@
             summed = jnp.dot(value_scratch[head], weights, preferred_element_type=jnp.float32)
             for block in range(first // tokens, (first + wide) // tokens):
                 columns = slice(block * tokens - first, (block + 1) * tokens - first)
-                out_ref[block, rows] = summed[:head_width, columns].astype(jnp.bfloat16)
-                stats = jnp.zeros((extra_rows, tokens), jnp.float32)
+                part_sum = summed[:head_width, columns].astype(jnp.bfloat16)
                 total = summed[head_width : head_width + 1, columns]
                 for place, part in enumerate(three_parts(peak[:, columns]) + three_parts(total)):
-                    stats = jnp.where(row == place, part, stats)
-                base = head_count * head_width + head * extra_rows
-                out_ref[block, base : base + extra_rows] = stats.astype(jnp.bfloat16)
-
-
-def project_kernel(head_count, head_width, place_ref, parts_ref, weight_ref, mine_ref, other_ref, full_ref):
+                    stats[block] = jnp.where(row == 6 * head + place, part, stats[block])
+                for core in range(2):
+                    out_ref[block, core, rows] = part_sum
+    for block in range(x_count):
+        for core in range(2):
+            out_ref[block, core, head_count * head_width :] = stats[block].astype(jnp.bfloat16)
+
+
+def project_kernel(head_count, head_width, place_ref, parts_ref, weight_ref, far_weight_ref, out_ref, weight_scratch):
     x_count = parts_ref.shape[0]
-    tp_half = mine_ref.shape[0]
+    blocks = out_ref.shape[0]
+    width = head_count * head_width
     core = place_ref[2]
     rows = []
-    for head in range(head_count):
-        peaks, totals = [], []
-        base = head_count * head_width + head * extra_rows
-        for part in range(x_count):
-            stats = parts_ref[part, base : base + extra_rows].astype(jnp.float32)
-            peaks.append(stats[0:1] + stats[1:2] + stats[2:3])
-            totals.append(stats[3:4] + stats[4:5] + stats[5:6])
-        top = functools.reduce(jnp.maximum, peaks)
-        factors = [jnp.exp(peak - top) for peak in peaks]
-        total = sum(factor * amount for factor, amount in zip(factors, totals))
-        summed = sum(
-            parts_ref[part, head * head_width : (head + 1) * head_width].astype(jnp.float32)
-            * factors[part]
-            for part in range(x_count)
-        )
-        rows.append((summed / total).astype(jnp.bfloat16))
+    for side, at in ((0, core), (1, 1 - core)):
+        source = (weight_ref, far_weight_ref)[side]
+        for block in range(blocks):
+            columns = pl.ds(pl.multiple_of((block * 2 + core) * lane, lane), lane)
+            weight_scratch[side * width : (side + 1) * width, block * lane : (block + 1) * lane] = (
+                source[:, columns]
+            )
+        stats = [parts_ref[part, at, width:].astype(jnp.float32) for part in range(x_count)]
+        for head in range(head_count):
+            base = 6 * head
+            peaks = [
+                kept[base : base + 1] + kept[base + 1 : base + 2] + kept[base + 2 : base + 3]
+                for kept in stats
+            ]
+            totals = [
+                kept[base + 3 : base + 4] + kept[base + 4 : base + 5] + kept[base + 5 : base + 6]
+                for kept in stats
+            ]
+            top = functools.reduce(jnp.maximum, peaks)
+            factors = [jnp.exp(peak - top) for peak in peaks]
+            total = sum(factor * amount for factor, amount in zip(factors, totals))
+            summed = sum(
+                parts_ref[part, at, head * head_width : (head + 1) * head_width].astype(jnp.float32)
+                * factors[part]
+                for part in range(x_count)
+            )
+            rows.append((summed / total).astype(jnp.bfloat16))
     attended = jnp.concatenate(rows, axis=0)
-    full_ref[...] = lax.dot_general(
-        attended, weight_ref[...], (((0,), (0,)), ((), ())), preferred_element_type=jnp.float32
+    projected = lax.dot_general(
+        attended, weight_scratch[...], (((0,), (0,)), ((), ())), preferred_element_type=jnp.float32
     ).astype(jnp.bfloat16)
-    for block in range(tp_half):
-        own = pl.multiple_of((block * 2 + core) * lane, lane)
-        far = pl.multiple_of((block * 2 + 1 - core) * lane, lane)
-        mine_ref[block] = full_ref[:, pl.ds(own, lane)]
-        other_ref[block] = full_ref[:, pl.ds(far, lane)]
-
-
-def pack_weights_kernel(gate_ref, up_ref, down_ref, out_ref, sems):
+    for block in range(blocks):
+        out_ref[block] = projected[:, block * lane : (block + 1) * lane]
+
+
+def pack_weights_kernel(gate_ref, up_ref, down_ref, out_ref, held, in_sems, out_sems):
     units = gate_ref.shape[1]
-    copies = [
-        pltpu.make_async_copy(gate_ref, out_ref.at[0], sems.at[0]),
-        pltpu.make_async_copy(up_ref, out_ref.at[1], sems.at[1]),
+    groups = [
+        [pltpu.make_async_copy(gate_ref, held.at[0], in_sems.at[0])],
+        [pltpu.make_async_copy(up_ref, held.at[1], in_sems.at[1])],
+        [],
     ]
     for block in range(down_ref.shape[1] // units):
         columns = pl.ds(block * units, units)
-        copies.append(
+        groups[2].append(
             pltpu.make_async_copy(
-                down_ref.at[:, columns], out_ref.at[2, columns, :], sems.at[2 + block]
+                down_ref.at[:, columns], held.at[2, columns, :], in_sems.at[2 + block]
             )
         )
-    for copy in copies:
-        copy.start()
-    for copy in copies:
+    for group in groups:
+        for copy in group:
+            copy.start()
+    outward = []
+    for kind, group in enumerate(groups):
+        for copy in group:
+            copy.wait()
+        outward.append(pltpu.make_async_copy(held.at[kind], out_ref.at[kind], out_sems.at[kind]))
+        outward[kind].start()
+    for copy in outward:
         copy.wait()
 
 
@@ -232,7 +252,7 @@
     vmem = pl.BlockSpec(memory_space=pltpu.VMEM)
 
     deep = head_width + extra_rows
-    message_rows = head_count * (deep + head_width)
+    message_rows = 2 * head_count * head_width + extra_rows
     message, scaled = pl.pallas_call(
         functools.partial(pack_kernel, head_width),
         out_shape=(
@@ -261,16 +281,23 @@
         out_shape=jax.ShapeDtypeStruct((3, model_width, hidden_units), bf16),
         in_specs=[any_space] * 3,
         out_specs=any_space,
-        scratch_shapes=[pltpu.SemaphoreType.DMA((2 + down_blocks,))],
+        scratch_shapes=[
+            pltpu.VMEM((3, model_width, hidden_units), bf16),
+            pltpu.SemaphoreType.DMA((2 + down_blocks,)),
+            pltpu.SemaphoreType.DMA((3,)),
+        ],
         name="pack_weights",
         interpret=INTERPRET,
     )(gate_weight[0], up_weight[0], down_weight[0])
     near_set = lax.ppermute(own_set, TP, slice_moves)
     own_swapped = swapped(own_set)
+    far_out_weight = swapped(out_weight)
     near_swapped = swapped(near_set)
     attend = pl.pallas_call(
         functools.partial(attend_kernel, head_count, head_width),
-        out_shape=jax.ShapeDtypeStruct((x_count, head_count * deep, token_count), bf16),
+        out_shape=jax.ShapeDtypeStruct(
+            (x_count, 2, head_count * head_width + extra_rows, token_count), bf16
+        ),
         in_specs=[smem] + [vmem] * (1 + x_count),
         out_specs=vmem,
         scratch_shapes=[
@@ -282,7 +309,10 @@
         interpret=INTERPRET,
     )
     parts = attend(place, gathered, *query_list)
-    received = lax.all_to_all(parts, "x", split_axis=0, concat_axis=0, tiled=True)
+    part_shape = parts.shape
+    received = lax.all_to_all(
+        parts.reshape(2 * x_count, *part_shape[2:]), ("x", "c"), split_axis=0, concat_axis=0, tiled=True
+    ).reshape(part_shape)
 
     expert_ids = jnp.arange(sp_count, dtype=jnp.int32)
     chosen = routes[:, :, None] == expert_ids
@@ -304,18 +334,16 @@
 
     give_first, give_rest = spread(share_first), spread(share_rest)
 
-    half = jax.ShapeDtypeStruct((y_count, token_count, local_width), bf16)
-    mine, other = pl.pallas_call(
+    projected = pl.pallas_call(
         functools.partial(project_kernel, head_count, head_width),
-        out_shape=(half, half),
-        in_specs=[smem, vmem, vmem],
-        out_specs=(vmem, vmem),
-        scratch_shapes=[pltpu.VMEM((token_count, model_width), bf16)],
+        out_shape=jax.ShapeDtypeStruct((y_count, token_count, local_width), bf16),
+        in_specs=[smem, vmem, vmem, vmem],
+        out_specs=vmem,
+        scratch_shapes=[pltpu.VMEM((2 * head_count * head_width, y_count * local_width), bf16)],
         name="project",
         interpret=INTERPRET,
-    )(place, received, out_weight)
-    paired = (mine.astype(f32) + swapped(other).astype(f32)).astype(bf16)
-    pieces = lax.all_to_all(paired, "y", split_axis=0, concat_axis=0, tiled=True)
+    )(place, received, out_weight, far_out_weight)
+    pieces = lax.all_to_all(projected, "y", split_axis=0, concat_axis=0, tiled=True)
     pieces, own_swapped, near_set, near_swapped = lax.optimization_barrier(
         (pieces, own_swapped, near_set, near_swapped)
     )

time: 307 us -> 210 us (0.68)
  Pallas kernels: 119 us -> 25.4 us
  blocking collectives: 80.1 us -> 70.6 us
  waiting for transfers between devices: 53.3 us -> 58.2 us
    pallas_call x1, Pallas kernels: 96.5 us -> 3.04 us  [shards(): pl.pallas_call(pack_weights_kernel, out_shape=jax.ShapeDtypeStruct((3, mo...]
    all_to_all x1 -> x0, blocking collectives: 10 us -> none  [shards(): lax.all_to_all(parts, 'x', split_axis=0, concat_axis=0, tiled=True)]
    all_to_all x1 -> x2, waiting for transfers between devices: 17.3 us -> 26.5 us  [the longest x1 16.4 us: shards(): lax.all_to_all(projected, 'y', split_axis=0, concat_axis=0, tiled=True)]
    all_to_all x1 -> x2, starting transfers between devices: 3.56 us -> 8.52 us  [the longest x1 4.88 us: shards(): lax.all_to_all(parts.reshape(2 * x_count, *part_shape[2:]), ('x', 'c'), s...]
  transfers between devices with their start and end apart: 10 -> 11, of which waited for: 6 -> 5; matrix products, arithmetic and copies ran while one was open for 1% -> 1% of each run, Pallas kernels for 5% -> 7%
where the time goes in v5:
time: 210 us; the launch traced here: 209 us
  blocking collectives  70.6 us (34%)
  waiting for transfers between devices  58.2 us (28%)
  starting transfers between devices  48.5 us (23%)
  Pallas kernels  25.4 us (12%)
  local copies, waits for them, and re-layouts  3.8 us (2%)
    all_to_all x1, blocking collectives, shards(): lax.all_to_all(copies.reshape(2 * y_count, quarter, local_width), TP, spl...  26.3 us
    all_to_all x1, blocking collectives, shards(): lax.all_to_all(out_rows, TP, split_axis=0, concat_axis=0, tiled=True)  23.2 us
    all_to_all x1, blocking collectives, shards(): lax.all_to_all(sent.reshape(sp_count, capacity, local_width), SP, split_a...  21.1 us
    ppermute x1, waiting for transfers between devices, shards(): near_set = lax.ppermute(own_set, TP, slice_moves)  19.7 us
    all_to_all x1, waiting for transfers between devices, shards(): lax.all_to_all(projected, 'y', split_axis=0, concat_axis=0, tiled=True)  16.4 us
    ppermute x3, starting transfers between devices, swapped(): return lax.ppermute(shard, 'c', [(0, 1), (1, 0)])  14.8 us
    all_to_all x1, waiting for transfers between devices, shards(): lax.all_to_all(expert_out.reshape(sp_count, capacity, local_width), SP, s...  11 us
    all_to_all x1, waiting for transfers between devices, shards(): lax.all_to_all(parts.reshape(2 * x_count, *part_shape[2:]), ('x', 'c'), s...  10.1 us
  transfers between devices with their start and end apart: 11, of which 5 were waited for; matrix products, arithmetic and copies ran while one was open for 1% of the time, Pallas kernels for 7%

profile of v5, /device:TPU:1, one launch (start us, length us, event | category | flops | bytes accessed | tf_op | source)
XLA Modules:
  0.0 209.4 jit_solution(1587721509453305218)
XLA Ops:
  0.0 3.0 %pack_weights.1.refs_0_ = bf16[3,2048,256]{2,1,0:T(8,128)(2,1)} custom-call(bf16[2048,256]{1,0:T(8,128)(2,1)} %bitcast.29, bf16[2048,256]{1,0:T(8,128)(2,1)} %bitcast.30, bf16[256,2048]{1,0:T(8,128)(2,1)} %bitcast.31), custom_call_target="tpu_custom_call" | custom-call | tf_op jit(solution)/shard_map/pack_weights/pallas_call | solution.py:279
  3.0 4.0 %collective-permute-start.5 = (bf16[3,2048,256]{2,1,0:T(8,128)(2,1)}, bf16[3,2048,256]{2,1,0:T(8,128)(2,1)}, u32[]{:S(2)}, u32[]{:S(2)}) collective-permute-start(bf16[3,2048,256]{2,1,0:T(8,128)(2,1)} %pack_weights.1.refs_0_), channel_id=1, source_target_pairs={{0,14},{1,3},{2,0},{3,5},{4,2},{5,7},{6,4},{7,9},{8,6},{9,11},{10,... | collective-permute-start | bytes 9437192 | tf_op jit(solution)/shard_map/ppermute | solution.py:292
  7.1 2.1 pack.1
  9.1 10.0 %all-to-all-start = ((bf16[8,272,256]{2,1,0:T(8,128)(2,1)}), bf16[8,272,256]{2,1,0:T(8,128)(2,1)S(1)}, u32[]{:S(2)}, u32[]{:S(2)}) async-start(bf16[8,272,256]{2,1,0:T(8,128)(2,1)} %get-tuple-element.11), calls=%async_computation | async-start | bytes 2228224 | tf_op jit(solution)/shard_map/all_to_all | solution.py:267
  19.2 5.0 %collective-permute-start.4 = (bf16[3,2048,256]{2,1,0:T(8,128)(2,1)}, bf16[3,2048,256]{2,1,0:T(8,128)(2,1)}, u32[]{:S(2)}, u32[]{:S(2)}) collective-permute-start(bf16[3,2048,256]{2,1,0:T(8,128)(2,1)} %pack_weights.1.refs_0_), channel_id=1, source_target_pairs={{0,1},{1,0},{2,3},{3,2},{4,5},{5,4},{6,7},{7,6},{8,9},{9,8},{10,11... | collective-permute-start | bytes 9437192 | tf_op jit(solution)/shard_map/ppermute | solution.py:23
  24.2 19.7 %collective-permute-done.5.refs_2_ = bf16[3,2048,256]{2,1,0:T(8,128)(2,1)} collective-permute-done((bf16[3,2048,256]{2,1,0:T(8,128)(2,1)}, bf16[3,2048,256]{2,1,0:T(8,128)(2,1)}, u32[]{:S(2)}, u32[]{:S(2)}) %collective-permute-start.5) | collective-permute-done | bytes 3145760 | tf_op jit(solution)/shard_map/ppermute | solution.py:292
  43.9 7.3 %collective-permute-start.6 = (bf16[3,2048,256]{2,1,0:T(8,128)(2,1)}, bf16[3,2048,256]{2,1,0:T(8,128)(2,1)}, u32[]{:S(2)}, u32[]{:S(2)}) collective-permute-start(bf16[3,2048,256]{2,1,0:T(8,128)(2,1)} %collective-permute-done.5.refs_2_), channel_id=1, source_target_pairs={{0,1},{1,0},{2,3},{3,2},{4,5},{5,4},{6,7},{7,6},{8,9},{9,8},{10,11... | collective-permute-start | bytes 9437192 | tf_op jit(solution)/shard_map/ppermute | solution.py:23
  51.3 1.9 collective-permute-start.2
  53.2 1.9 collective-permute-start.1
  55.1 3.4 %collective-permute-start = (bf16[128,256]{1,0:T(8,128)(2,1)}, bf16[128,256]{1,0:T(8,128)(2,1)S(1)}, u32[]{:S(2)}, u32[]{:S(2)}) collective-permute-start(bf16[128,256]{1,0:T(8,128)(2,1)} %get-tuple-element.12.refs_0_), channel_id=1, source_target_pairs={{0,16},{16,32},{32,48},{48,0},{1,17},{17,33},{33,49},{49,1},{2,18}... | collective-permute-start | bytes 196616 | tf_op jit(solution)/shard_map/ppermute | solution.py:269
  58.5 0.0 collective-permute-done.2.refs_3_
  58.5 2.5 %collective-permute-start.3 = (bf16[128,2048]{1,0:T(8,128)(2,1)S(1)}, bf16[128,2048]{1,0:T(8,128)(2,1)S(1)}, u32[]{:S(2)}, u32[]{:S(2)}) collective-permute-start(bf16[128,2048]{1,0:T(8,128)(2,1)S(1)} %copy-done.2), channel_id=1, source_target_pairs={{0,1},{1,0},{2,3},{3,2},{4,5},{5,4},{6,7},{7,6},{8,9},{9,8},{10,11... | collective-permute-start | bytes 1572872 | tf_op jit(solution)/shard_map/ppermute | solution.py:23
  61.0 0.7 pad_add_fusion.place_ref
  61.7 0.0 collective-permute-done.1.refs_2_
  61.7 1.0 collective-permute-done.refs_1_
  62.7 0.0 all-to-all-done.kv_ref
  62.8 0.6 copy-done.7
  63.4 1.0 copy-done
  64.4 9.2 %attend.1 = bf16[4,2,144,256]{3,2,1,0:T(8,128)(2,1)} custom-call(s32[4]{0:T(128)} %pad_add_fusion.place_ref, bf16[8,272,256]{2,1,0:T(8,128)(2,1)} %copy-done, bf16[128,256]{1,0:T(8,128)(2,1)} %get-tuple-element.12.refs_0_, bf16[128,256]{1,0:T(8,128)(2,1)} %copy-done.7, bf16[128,256]{1,0:T(8,128)(2,1)} %copy-done.6, bf16[128,256]{1,0:T(8,128)(2,1)} %copy-done.5), custom_call_target="tpu_custom_call" | custom-call | tf_op jit(solution)/shard_map/attend/pallas_call | solution.py:311
  73.6 4.9 %all-to-all-start.1 = ((bf16[8,144,256]{2,1,0:T(8,128)(2,1)}), bf16[8,144,256]{2,1,0:T(8,128)(2,1)S(1)}, u32[]{:S(2)}, u32[]{:S(2)}) async-start(bf16[8,144,256]{2,1,0:T(8,128)(2,1)} %bitcast.28), calls=%async_computation.1 | async-start | bytes 1179648 | tf_op jit(solution)/shard_map/all_to_all | solution.py:313
  78.4 0.0 collective-permute-done.3.far_weight_ref
  78.4 10.1 %all-to-all-done.1 = bf16[8,144,256]{2,1,0:T(8,128)(2,1)S(1)} async-done(((bf16[8,144,256]{2,1,0:T(8,128)(2,1)}), bf16[8,144,256]{2,1,0:T(8,128)(2,1)S(1)}, u32[]{:S(2)}, u32[]{:S(2)}) %all-to-all-start.1) | async-done | bytes 589856 | tf_op jit(solution)/shard_map/all_to_all | solution.py:313
  88.5 0.9 copy-done.1
  89.4 2.8 %project.1 = bf16[8,256,128]{2,1,0:T(8,128)(2,1)} custom-call(s32[4]{0:T(128)} %pad_add_fusion.place_ref, bf16[4,2,144,256]{3,2,1,0:T(8,128)(2,1)} %bitcast.27, bf16[128,2048]{1,0:T(8,128)(2,1)} %weight_ref.1, bf16[128,2048]{1,0:T(8,128)(2,1)} %copy-done.3), custom_call_target="tpu_custom_call" | custom-call | tf_op jit(solution)/shard_map/project/pallas_call | solution.py:337
  92.2 3.6 %all-to-all-start.2 = ((bf16[8,256,128]{2,1,0:T(8,128)(2,1)}), bf16[8,256,128]{2,1,0:T(8,128)(2,1)S(1)}, u32[]{:S(2)}, u32[]{:S(2)}) async-start(bf16[8,256,128]{2,1,0:T(8,128)(2,1)} %project.1), calls=%async_computation.2 | async-start | bytes 1048576 | tf_op jit(solution)/shard_map/all_to_all | solution.py:346
  95.8 0.1 eq.62
  95.9 0.1 and.15
  96.0 0.1 and.16
  96.1 0.2 convolution_convert_fusion.1
  96.3 0.1 eq.59
  96.3 0.1 eq.60
  96.4 0.0 collective-permute-done.4.refs_1_
  96.4 16.4 %all-to-all-done.2 = bf16[8,256,128]{2,1,0:T(8,128)(2,1)S(1)} async-done(((bf16[8,256,128]{2,1,0:T(8,128)(2,1)}), bf16[8,256,128]{2,1,0:T(8,128)(2,1)S(1)}, u32[]{:S(2)}, u32[]{:S(2)}) %all-to-all-start.2) | async-done | bytes 524320 | tf_op jit(solution)/shard_map/all_to_all | solution.py:346
  112.8 0.0 collective-permute-done.6.refs_3_
  112.8 0.1 convert_reduce_fusion
  112.9 0.0 copy-done.4
  112.9 0.3 convolution_convert_fusion
  113.3 21.1 %all_to_all.35 = bf16[32,20,128]{2,1,0:T(8,128)(2,1)S(1)} all-to-all(bf16[32,20,128]{2,1,0:T(8,128)(2,1)S(1)} %reshape.46), channel_id=1, replica_groups=mesh['z'=8,'x'=4,'y'=8,'c'=2] {'z','x'}, dimensions={0} | all-to-all | bytes 327680 | tf_op jit(solution)/shard_map/all_to_all | solution.py:355
  134.4 0.1 broadcast_in_dim.50
  134.5 26.3 %all_to_all.36.rows_in_ref = bf16[16,160,128]{2,1,0:T(8,128)(2,1)} all-to-all(bf16[16,160,128]{2,1,0:T(8,128)(2,1)S(1)} %bitcast.26), channel_id=1, replica_groups=mesh['z'=8,'x'=4,'y'=8,'c'=2] {'y','c'}, dimensions={0} | all-to-all | bytes 1310720 | tf_op jit(solution)/shard_map/all_to_all | solution.py:361
  160.8 8.4 %expert.1 = bf16[16,160,128]{2,1,0:T(8,128)(2,1)} custom-call(bf16[16,160,128]{2,1,0:T(8,128)(2,1)} %all_to_all.36.rows_in_ref, f32[16,1,128]{2,1,0:T(1,128)} %bitcast.34, bf16[3,2048,256]{2,1,0:T(8,128)(2,1)} %pack_weights.1.refs_0_, bf16[3,2048,256]{2,1,0:T(8,128)(2,1)} %collective-permute-done.4.refs_1_, ...), custom_call_target="tpu_custom_call" | custom-call | tf_op jit(solution)/shard_map/expert/pallas_call | solution.py:365
  169.2 23.2 %all_to_all.37 = bf16[16,160,128]{2,1,0:T(8,128)(2,1)S(1)} all-to-all(bf16[16,160,128]{2,1,0:T(8,128)(2,1)} %expert.1), channel_id=1, replica_groups=mesh['z'=8,'x'=4,'y'=8,'c'=2] {'y','c'}, dimensions={0} | all-to-all | bytes 1310720 | tf_op jit(solution)/shard_map/all_to_all | solution.py:382
  192.4 0.1 reduce_sum.32
  192.6 0.7 reshape.51
  193.3 3.9 %all-to-all-start.6 = ((bf16[32,20,128]{2,1,0:T(8,128)(2,1)}), bf16[32,20,128]{2,1,0:T(8,128)(2,1)S(1)}, u32[]{:S(2)}, u32[]{:S(2)}) async-start(bf16[32,20,128]{2,1,0:T(8,128)(2,1)} %reshape.51), calls=%async_computation.6 | async-start | bytes 393216 | tf_op jit(solution)/shard_map/all_to_all | solution.py:386
  197.2 11.0 %all-to-all-done.6 = bf16[32,20,128]{2,1,0:T(8,128)(2,1)S(1)} async-done(((bf16[32,20,128]{2,1,0:T(8,128)(2,1)}), bf16[32,20,128]{2,1,0:T(8,128)(2,1)S(1)}, u32[]{:S(2)}, u32[]{:S(2)}) %all-to-all-start.6) | async-done | bytes 163872 | tf_op jit(solution)/shard_map/all_to_all | solution.py:386
  208.2 0.3 convolution_bitcast_fusion
  208.5 0.9 fusion.2
  (22 shorter events, 0.1 us)
Async XLA Ops:
  0.0 58.5 %copy-start.2 = (bf16[128,2048]{1,0:T(8,128)(2,1)S(1)}, bf16[128,2048]{1,0:T(8,128)(2,1)}, u32[]{:S(2)}) copy-start(bf16[128,2048]{1,0:T(8,128)(2,1)} %weight_ref.1) | copy-start | bytes 1572868
  3.0 40.9 %collective-permute-start.5 = (bf16[3,2048,256]{2,1,0:T(8,128)(2,1)}, bf16[3,2048,256]{2,1,0:T(8,128)(2,1)}, u32[]{:S(2)}, u32[]{:S(2)}) collective-permute-start(bf16[3,2048,256]{2,1,0:T(8,128)(2,1)} %pack_weights.1.refs_0_), channel_id=1, source_target_pairs={{0,14},{1,3},{2,0},{3,5},{4,2},{5,7},{6,4},{7,9},{8,6},{9,11},{10,... | collective-permute-start | bytes 9437192 | tf_op jit(solution)/shard_map/ppermute | solution.py:292
  9.1 53.6 %all-to-all-start = ((bf16[8,272,256]{2,1,0:T(8,128)(2,1)}), bf16[8,272,256]{2,1,0:T(8,128)(2,1)S(1)}, u32[]{:S(2)}, u32[]{:S(2)}) async-start(bf16[8,272,256]{2,1,0:T(8,128)(2,1)} %get-tuple-element.11), calls=%async_computation | async-start | bytes 2228224 | tf_op jit(solution)/shard_map/all_to_all | solution.py:267
  19.2 77.2 %collective-permute-start.4 = (bf16[3,2048,256]{2,1,0:T(8,128)(2,1)}, bf16[3,2048,256]{2,1,0:T(8,128)(2,1)}, u32[]{:S(2)}, u32[]{:S(2)}) collective-permute-start(bf16[3,2048,256]{2,1,0:T(8,128)(2,1)} %pack_weights.1.refs_0_), channel_id=1, source_target_pairs={{0,1},{1,0},{2,3},{3,2},{4,5},{5,4},{6,7},{7,6},{8,9},{9,8},{10,11... | collective-permute-start | bytes 9437192 | tf_op jit(solution)/shard_map/ppermute | solution.py:23
  43.9 68.9 %collective-permute-start.6 = (bf16[3,2048,256]{2,1,0:T(8,128)(2,1)}, bf16[3,2048,256]{2,1,0:T(8,128)(2,1)}, u32[]{:S(2)}, u32[]{:S(2)}) collective-permute-start(bf16[3,2048,256]{2,1,0:T(8,128)(2,1)} %collective-permute-done.5.refs_2_), channel_id=1, source_target_pairs={{0,1},{1,0},{2,3},{3,2},{4,5},{5,4},{6,7},{7,6},{8,9},{9,8},{10,11... | collective-permute-start | bytes 9437192 | tf_op jit(solution)/shard_map/ppermute | solution.py:23
  51.3 7.2 %collective-permute-start.2 = (bf16[128,256]{1,0:T(8,128)(2,1)}, bf16[128,256]{1,0:T(8,128)(2,1)S(1)}, u32[]{:S(2)}, u32[]{:S(2)}) collective-permute-start(bf16[128,256]{1,0:T(8,128)(2,1)} %get-tuple-element.12.refs_0_), channel_id=1, source_target_pairs={{0,48},{16,0},{32,16},{48,32},{1,49},{17,1},{33,17},{49,33},{2,50}... | collective-permute-start | bytes 196616 | tf_op jit(solution)/shard_map/ppermute | solution.py:269
  53.2 8.5 %collective-permute-start.1 = (bf16[128,256]{1,0:T(8,128)(2,1)}, bf16[128,256]{1,0:T(8,128)(2,1)S(1)}, u32[]{:S(2)}, u32[]{:S(2)}) collective-permute-start(bf16[128,256]{1,0:T(8,128)(2,1)} %get-tuple-element.12.refs_0_), channel_id=1, source_target_pairs={{0,32},{16,48},{32,0},{48,16},{1,33},{17,49},{33,1},{49,17},{2,34}... | collective-permute-start | bytes 196616 | tf_op jit(solution)/shard_map/ppermute | solution.py:269
  55.1 7.6 %collective-permute-start = (bf16[128,256]{1,0:T(8,128)(2,1)}, bf16[128,256]{1,0:T(8,128)(2,1)S(1)}, u32[]{:S(2)}, u32[]{:S(2)}) collective-permute-start(bf16[128,256]{1,0:T(8,128)(2,1)} %get-tuple-element.12.refs_0_), channel_id=1, source_target_pairs={{0,16},{16,32},{32,48},{48,0},{1,17},{17,33},{33,49},{49,1},{2,18}... | collective-permute-start | bytes 196616 | tf_op jit(solution)/shard_map/ppermute | solution.py:269
  58.5 4.2 %copy-start.5 = (bf16[128,256]{1,0:T(8,128)(2,1)}, bf16[128,256]{1,0:T(8,128)(2,1)S(1)}, u32[]{:S(2)}) copy-start(bf16[128,256]{1,0:T(8,128)(2,1)S(1)} %collective-permute-done.2.refs_3_) | copy-start | bytes 196612
  58.5 19.9 %collective-permute-start.3 = (bf16[128,2048]{1,0:T(8,128)(2,1)S(1)}, bf16[128,2048]{1,0:T(8,128)(2,1)S(1)}, u32[]{:S(2)}, u32[]{:S(2)}) collective-permute-start(bf16[128,2048]{1,0:T(8,128)(2,1)S(1)} %copy-done.2), channel_id=1, source_target_pairs={{0,1},{1,0},{2,3},{3,2},{4,5},{5,4},{6,7},{7,6},{8,9},{9,8},{10,11... | collective-permute-start | bytes 1572872 | tf_op jit(solution)/shard_map/ppermute | solution.py:23
  61.7 34.2 %copy-start.8 = (s32[256,2]{0,1:T(2,128)S(1)}, s32[256,2]{0,1:T(2,128)}, u32[]{:S(2)}) copy-start(s32[256,2]{0,1:T(2,128)} %param.19) | copy-start | bytes 6148
  61.7 1.0 copy-start.6
  62.7 0.6 copy-start.7
  63.4 1.0 copy-start
  73.6 15.0 %all-to-all-start.1 = ((bf16[8,144,256]{2,1,0:T(8,128)(2,1)}), bf16[8,144,256]{2,1,0:T(8,128)(2,1)S(1)}, u32[]{:S(2)}, u32[]{:S(2)}) async-start(bf16[8,144,256]{2,1,0:T(8,128)(2,1)} %bitcast.28), calls=%async_computation.1 | async-start | bytes 1179648 | tf_op jit(solution)/shard_map/all_to_all | solution.py:313
  78.4 10.1 %copy-start.3 = (bf16[128,2048]{1,0:T(8,128)(2,1)}, bf16[128,2048]{1,0:T(8,128)(2,1)S(1)}, u32[]{:S(2)}) copy-start(bf16[128,2048]{1,0:T(8,128)(2,1)S(1)} %collective-permute-done.3.far_weight_ref) | copy-start | bytes 1572868
  88.5 0.9 copy-start.1
  89.4 23.5 %copy-start.4 = (bf16[256,128]{1,0:T(8,128)(2,1)S(1)}, bf16[256,128]{1,0:T(8,128)(2,1)}, u32[]{:S(2)}) copy-start(bf16[256,128]{1,0:T(8,128)(2,1)} %param.12) | copy-start | bytes 196612
  92.2 20.7 %all-to-all-start.2 = ((bf16[8,256,128]{2,1,0:T(8,128)(2,1)}), bf16[8,256,128]{2,1,0:T(8,128)(2,1)S(1)}, u32[]{:S(2)}, u32[]{:S(2)}) async-start(bf16[8,256,128]{2,1,0:T(8,128)(2,1)} %project.1), calls=%async_computation.2 | async-start | bytes 1048576 | tf_op jit(solution)/shard_map/all_to_all | solution.py:346
  160.8 36.3 %copy-start.9 = (f32[256,2]{0,1:T(2,128)S(1)}, f32[256,2]{0,1:T(2,128)}, u32[]{:S(2)}) copy-start(f32[256,2]{0,1:T(2,128)} %param.20) | copy-start | bytes 6148
  193.3 14.9 %all-to-all-start.6 = ((bf16[32,20,128]{2,1,0:T(8,128)(2,1)}), bf16[32,20,128]{2,1,0:T(8,128)(2,1)S(1)}, u32[]{:S(2)}, u32[]{:S(2)}) async-start(bf16[32,20,128]{2,1,0:T(8,128)(2,1)} %reshape.51), calls=%async_computation.6 | async-start | bytes 393216 | tf_op jit(solution)/shard_map/all_to_all | solution.py:386

commit v6 on v5

--- a/solution.py
+++ b/solution.py
@@ -17,6 +17,14 @@
 masked_score = -1e30
 extra_rows = 16
 lane = 128
+
+
+def held(array):
+    return array if INTERPRET else pltpu.with_memory_space_constraint(array, pltpu.VMEM)
+
+
+def kept(shape, dtype):
+    return jax.ShapeDtypeStruct(shape, dtype) if INTERPRET else pltpu.VMEM(shape, dtype)
 
 
 def swapped(shard):
@@ -57,7 +65,8 @@
     row = lax.broadcasted_iota(jnp.int32, (extra_rows, tokens), 0)
     ones = jnp.ones((extra_rows, tokens), jnp.bfloat16)
     for head in range(head_count):
-        minus = jnp.where((row >= 3 * head) & (row < 3 * head + 3), -1.0, 0.0).astype(jnp.bfloat16)
+        counted = ((row >= 3 * head) & (row < 3 * head + 3)) | (row == extra_rows - 1)
+        minus = jnp.where(counted, -1.0, 0.0).astype(jnp.bfloat16)
         rows = slice(head * head_width, (head + 1) * head_width)
         for shift in range(x_count):
             target = lax.rem(x_place + x_count - shift, x_count)
@@ -65,11 +74,16 @@
             query_scratch[head, :head_width, columns] = query_refs[shift][rows]
             query_scratch[head, head_width:, columns] = minus
         for block in range(z_count):
+            source = lax.rem(z_place + block, z_count)
             columns = slice(block * tokens, (block + 1) * tokens)
             first = (head_count + head) * head_width
-            key_scratch[head, :head_width, columns] = kv_ref[block, rows]
-            key_scratch[head, head_width:, columns] = kv_ref[block, 2 * head_count * head_width :]
-            value_scratch[head, :head_width, columns] = kv_ref[block, first : first + head_width]
+            later = jnp.where((block > 0) & (z_place + block < z_count), -2 * masked_score, 0.0)
+            gates = kv_ref[source, 2 * head_count * head_width :]
+            key_scratch[head, :head_width, columns] = kv_ref[source, rows]
+            key_scratch[head, head_width:, columns] = jnp.where(
+                row == extra_rows - 1, later, gates.astype(jnp.float32)
+            ).astype(jnp.bfloat16)
+            value_scratch[head, :head_width, columns] = kv_ref[source, first : first + head_width]
             value_scratch[head, head_width:, columns] = ones
     wide = 2 * tokens if x_count % 2 == 0 else tokens
     stats = [jnp.zeros((extra_rows, tokens), jnp.float32)] * x_count
@@ -82,12 +96,11 @@
                 (((0,), (0,)), ((), ())),
                 preferred_element_type=jnp.float32,
             )
-            key_row = lax.broadcasted_iota(jnp.int32, scores.shape, 0)
-            key_place = key_row // tokens * (x_count * tokens) + key_row % tokens
-            key_place = key_place + x_place * tokens
-            query_place = lax.broadcasted_iota(jnp.int32, scores.shape, 1)
-            query_place = query_place + (z_place * (x_count * tokens) + first)
-            scores = jnp.where(key_place <= query_place, scores, 2 * masked_score)
+            near = scores[:tokens]
+            key_place = lax.broadcasted_iota(jnp.int32, near.shape, 0) + x_place * tokens
+            query_place = lax.broadcasted_iota(jnp.int32, near.shape, 1) + first
+            near = jnp.where(key_place <= query_place, near, 2 * masked_score)
+            scores = jnp.concatenate([near, scores[tokens:]], axis=0)
             peak = jnp.maximum(jnp.max(scores, axis=0, keepdims=True), masked_score)
             weights = jnp.exp(scores - peak).astype(jnp.bfloat16)
             summed = jnp.dot(value_scratch[head], weights, preferred_element_type=jnp.float32)
@@ -173,29 +186,20 @@
 
 
 def expert_kernel(rows_in_ref, gain_ref, *refs):
-    sets = len(refs) - 8
-    set_refs = refs[:sets]
-    out_ref, rows_ref, hidden_ref, full_ref, gates, ups, downs, sems = refs[sets:]
+    sets = len(refs) - 5
+    out_ref, rows_ref, hidden_ref, kinds, sems = refs[sets:]
     blocks = rows_in_ref.shape[0]
     width = rows_ref.shape[1]
-    units = gates.shape[2]
-    gate_copies, up_copies, down_copies = [], [], []
+    units = kinds.shape[3]
+    copies = [
+        [pltpu.make_async_copy(refs[part].at[kind], kinds.at[part, kind], sems.at[part, kind]) for kind in range(3)]
+        for part in range(sets)
+    ]
     for part in range(sets):
-        gate_copies.append(
-            pltpu.make_async_copy(set_refs[part].at[0], gates.at[part], sems.at[part, 0])
-        )
-        up_copies.append(pltpu.make_async_copy(set_refs[part].at[1], ups.at[part], sems.at[part, 1]))
-        gate_copies[part].start()
-        up_copies[part].start()
+        copies[part][0].start()
+        copies[part][1].start()
     for part in range(sets):
-        for block in range(width // units):
-            columns = pl.ds(block * units, units)
-            down_copies.append(
-                pltpu.make_async_copy(
-                    set_refs[part].at[2, columns, :], downs.at[part, :, columns], sems.at[part, 2 + block]
-                )
-            )
-            down_copies[-1].start()
+        copies[part][2].start()
     squares = jnp.zeros(rows_in_ref.shape[1:], jnp.float32)
     for block in range(blocks):
         values = rows_in_ref[block].astype(jnp.float32)
@@ -205,20 +209,21 @@
         values = rows_in_ref[block].astype(jnp.float32) * scale * gain_ref[block]
         rows_ref[:, block * lane : (block + 1) * lane] = values.astype(jnp.bfloat16)
     for part in range(sets):
-        gate_copies[part].wait()
-        gate = jnp.dot(rows_ref[...], gates[part], preferred_element_type=jnp.float32)
-        up_copies[part].wait()
-        up = jnp.dot(rows_ref[...], ups[part], preferred_element_type=jnp.float32)
-        hidden_ref[:, part * units : (part + 1) * units] = (
-            gate / (1.0 + jnp.exp(-gate)) * up
+        copies[part][0].wait()
+        gate = jnp.dot(rows_ref[...], kinds[part, 0], preferred_element_type=jnp.float32)
+        copies[part][1].wait()
+        up = jnp.dot(rows_ref[...], kinds[part, 1], preferred_element_type=jnp.float32)
+        hidden_ref[part] = (gate / (1.0 + jnp.exp(-gate)) * up).astype(jnp.bfloat16)
+    for part in range(sets):
+        copies[part][2].wait()
+    for block in range(width // units):
+        down_rows = slice(block * units, (block + 1) * units)
+        total = sum(
+            jnp.dot(hidden_ref[part], kinds[part, 2, down_rows, :], preferred_element_type=jnp.float32)
+            for part in range(sets)
         ).astype(jnp.bfloat16)
-    for copy in down_copies:
-        copy.wait()
-    full_ref[...] = jnp.dot(
-        hidden_ref[...], downs[...].reshape(sets * units, width), preferred_element_type=jnp.float32
-    ).astype(jnp.bfloat16)
-    for block in range(blocks):
-        out_ref[block] = full_ref[:, block * lane : (block + 1) * lane]
+        for piece in range(units // lane):
+            out_ref[block * (units // lane) + piece] = total[:, piece * lane : (piece + 1) * lane]
 
 
 def shards(
@@ -257,7 +262,7 @@
         functools.partial(pack_kernel, head_width),
         out_shape=(
             jax.ShapeDtypeStruct((z_count, message_rows, token_count), bf16),
-            jax.ShapeDtypeStruct(queries.shape, bf16),
+            kept(queries.shape, bf16),
         ),
         in_specs=[vmem] * 4,
         out_specs=(vmem, vmem),
@@ -308,7 +313,7 @@
         name="attend",
         interpret=INTERPRET,
     )
-    parts = attend(place, gathered, *query_list)
+    parts = attend(place, held(gathered), *map(held, query_list))
     part_shape = parts.shape
     received = lax.all_to_all(
         parts.reshape(2 * x_count, *part_shape[2:]), ("x", "c"), split_axis=0, concat_axis=0, tiled=True
@@ -342,7 +347,7 @@
         scratch_shapes=[pltpu.VMEM((2 * head_count * head_width, y_count * local_width), bf16)],
         name="project",
         interpret=INTERPRET,
-    )(place, received, out_weight, far_out_weight)
+    )(place, held(received), held(out_weight), held(far_out_weight))
     pieces = lax.all_to_all(projected, "y", split_axis=0, concat_axis=0, tiled=True)
     pieces, own_swapped, near_set, near_swapped = lax.optimization_barrier(
         (pieces, own_swapped, near_set, near_swapped)
@@ -364,21 +369,18 @@
     sets = len(weight_sets)
     out_rows = pl.pallas_call(
         expert_kernel,
-        out_shape=jax.ShapeDtypeStruct((2 * y_count, quarter, local_width), bf16),
+        out_shape=kept((2 * y_count, quarter, local_width), bf16),
         in_specs=[vmem, vmem] + [any_space] * sets,
         out_specs=vmem,
         scratch_shapes=[
             pltpu.VMEM((quarter, model_width), bf16),
-            pltpu.VMEM((quarter, sets * hidden_units), bf16),
-            pltpu.VMEM((quarter, model_width), bf16),
-            pltpu.VMEM((sets, model_width, hidden_units), bf16),
-            pltpu.VMEM((sets, model_width, hidden_units), bf16),
-            pltpu.VMEM((sets, hidden_units, model_width), bf16),
-            pltpu.SemaphoreType.DMA((sets, 2 + down_blocks)),
+            pltpu.VMEM((sets, quarter, hidden_units), bf16),
+            pltpu.VMEM((sets, 3, model_width, hidden_units), bf16),
+            pltpu.SemaphoreType.DMA((sets, 3)),
         ],
         name="expert",
         interpret=INTERPRET,
-    )(rows, norm_gain.reshape(2 * y_count, 1, lane), *weight_sets)
+    )(held(rows), norm_gain.reshape(2 * y_count, 1, lane), *weight_sets)
     pieces = lax.all_to_all(out_rows, TP, split_axis=0, concat_axis=0, tiled=True)
     expert_out = jnp.sum(
         pieces.reshape(y_count // 2, 4, quarter, local_width).astype(f32), axis=0

time: 210 us -> 203 us (0.967)
  Pallas kernels: 25.4 us -> 22.2 us
  local copies, waits for them, and re-layouts: 3.8 us -> 1.27 us
    pallas_call x2, Pallas kernels: 17.6 us -> 15 us  [the longest x1 8.17 us: shards(): parts = attend(place, held(gathered), *map(held, query_list))]
    unnamed x20 -> x8, local copies, waits for them, and re-layouts: 2.54 us -> 0.01 us
  transfers between devices with their start and end apart: 11 -> 11, of which waited for: 5 -> 5; matrix products, arithmetic and copies ran while one was open for 1% -> 1% of each run, Pallas kernels for 7% -> 6%
where the time goes in v6:
time: 203 us; the launch traced here: 202 us
  blocking collectives  69.3 us (34%)
  waiting for transfers between devices  58.1 us (29%)
  starting transfers between devices  48.5 us (24%)
  Pallas kernels  22.2 us (11%)
    all_to_all x1, blocking collectives, shards(): lax.all_to_all(copies.reshape(2 * y_count, quarter, local_width), TP, spl...  25.6 us
    all_to_all x1, blocking collectives, shards(): lax.all_to_all(out_rows, TP, split_axis=0, concat_axis=0, tiled=True)  22.6 us
    all_to_all x1, blocking collectives, shards(): lax.all_to_all(sent.reshape(sp_count, capacity, local_width), SP, split_a...  21.1 us
    ppermute x1, waiting for transfers between devices, shards(): near_set = lax.ppermute(own_set, TP, slice_moves)  19.7 us
    all_to_all x1, waiting for transfers between devices, shards(): lax.all_to_all(projected, 'y', split_axis=0, concat_axis=0, tiled=True)  16.4 us
    ppermute x3, starting transfers between devices, swapped(): return lax.ppermute(shard, 'c', [(0, 1), (1, 0)])  14.8 us
    all_to_all x1, waiting for transfers between devices, shards(): lax.all_to_all(expert_out.reshape(sp_count, capacity, local_width), SP, s...  11 us
    all_to_all x1, waiting for transfers between devices, shards(): lax.all_to_all(parts.reshape(2 * x_count, *part_shape[2:]), ('x', 'c'), s...  10.1 us
  transfers between devices with their start and end apart: 11, of which 5 were waited for; matrix products, arithmetic and copies ran while one was open for 1% of the time, Pallas kernels for 6%

profile of v6, /device:TPU:1, one launch (start us, length us, event | category | flops | bytes accessed | tf_op | source)
XLA Modules:
  0.0 202.2 jit_solution(13386792495831486060)
XLA Ops:
  0.0 3.0 %pack_weights.1.refs_0_ = bf16[3,2048,256]{2,1,0:T(8,128)(2,1)} custom-call(bf16[2048,256]{1,0:T(8,128)(2,1)} %bitcast.29, bf16[2048,256]{1,0:T(8,128)(2,1)} %bitcast.30, bf16[256,2048]{1,0:T(8,128)(2,1)} %bitcast.31), custom_call_target="tpu_custom_call" | custom-call | tf_op jit(solution)/shard_map/pack_weights/pallas_call | solution.py:284
  3.0 4.0 %collective-permute-start.5 = (bf16[3,2048,256]{2,1,0:T(8,128)(2,1)}, bf16[3,2048,256]{2,1,0:T(8,128)(2,1)}, u32[]{:S(2)}, u32[]{:S(2)}) collective-permute-start(bf16[3,2048,256]{2,1,0:T(8,128)(2,1)} %pack_weights.1.refs_0_), channel_id=1, source_target_pairs={{0,14},{1,3},{2,0},{3,5},{4,2},{5,7},{6,4},{7,9},{8,6},{9,11},{10,... | collective-permute-start | bytes 9437192 | tf_op jit(solution)/shard_map/ppermute | solution.py:297
  7.1 2.1 %pack.1 = (bf16[8,272,256]{2,1,0:T(8,128)(2,1)}, bf16[128,256]{1,0:T(8,128)(2,1)S(1)}) custom-call(bf16[128,256]{1,0:T(8,128)(2,1)} %keys_ref.1, bf16[128,256]{1,0:T(8,128)(2,1)} %values_ref.1, f32[2,256]{1,0:T(2,128)} %gates_ref.1, bf16[128,256]{1,0:T(8,128)(2,1)} %queries_ref.1), custom_call_target="tpu_custom_call" | custom-call | tf_op jit(solution)/shard_map/pack/pallas_call | solution.py:261
  9.2 10.0 %all-to-all-start = ((bf16[8,272,256]{2,1,0:T(8,128)(2,1)}), bf16[8,272,256]{2,1,0:T(8,128)(2,1)S(1)}, u32[]{:S(2)}, u32[]{:S(2)}) async-start(bf16[8,272,256]{2,1,0:T(8,128)(2,1)} %get-tuple-element.11), calls=%async_computation | async-start | bytes 2228224 | tf_op jit(solution)/shard_map/all_to_all | solution.py:272
  19.2 5.0 %collective-permute-start.4 = (bf16[3,2048,256]{2,1,0:T(8,128)(2,1)}, bf16[3,2048,256]{2,1,0:T(8,128)(2,1)}, u32[]{:S(2)}, u32[]{:S(2)}) collective-permute-start(bf16[3,2048,256]{2,1,0:T(8,128)(2,1)} %pack_weights.1.refs_0_), channel_id=1, source_target_pairs={{0,1},{1,0},{2,3},{3,2},{4,5},{5,4},{6,7},{7,6},{8,9},{9,8},{10,11... | collective-permute-start | bytes 9437192 | tf_op jit(solution)/shard_map/ppermute | solution.py:31
  24.2 19.7 %collective-permute-done.5.refs_2_ = bf16[3,2048,256]{2,1,0:T(8,128)(2,1)} collective-permute-done((bf16[3,2048,256]{2,1,0:T(8,128)(2,1)}, bf16[3,2048,256]{2,1,0:T(8,128)(2,1)}, u32[]{:S(2)}, u32[]{:S(2)}) %collective-permute-start.5) | collective-permute-done | bytes 3145760 | tf_op jit(solution)/shard_map/ppermute | solution.py:297
  43.9 7.3 %collective-permute-start.6 = (bf16[3,2048,256]{2,1,0:T(8,128)(2,1)}, bf16[3,2048,256]{2,1,0:T(8,128)(2,1)}, u32[]{:S(2)}, u32[]{:S(2)}) collective-permute-start(bf16[3,2048,256]{2,1,0:T(8,128)(2,1)} %collective-permute-done.5.refs_2_), channel_id=1, source_target_pairs={{0,1},{1,0},{2,3},{3,2},{4,5},{5,4},{6,7},{7,6},{8,9},{9,8},{10,11... | collective-permute-start | bytes 9437192 | tf_op jit(solution)/shard_map/ppermute | solution.py:31
  51.3 1.9 collective-permute-start.2
  53.2 1.9 collective-permute-start.1
  55.1 3.4 %collective-permute-start = (bf16[128,256]{1,0:T(8,128)(2,1)S(1)}, bf16[128,256]{1,0:T(8,128)(2,1)S(1)}, u32[]{:S(2)}, u32[]{:S(2)}) collective-permute-start(bf16[128,256]{1,0:T(8,128)(2,1)S(1)} %get-tuple-element.12.refs_0_), channel_id=1, source_target_pairs={{0,16},{16,32},{32,48},{48,0},{1,17},{17,33},{33,49},{49,1},{2,18}... | collective-permute-start | bytes 196616 | tf_op jit(solution)/shard_map/ppermute | solution.py:274
  58.5 0.0 collective-permute-done.2.refs_3_
  58.5 0.0 copy-done
  58.5 2.5 %collective-permute-start.3 = (bf16[128,2048]{1,0:T(8,128)(2,1)S(1)}, bf16[128,2048]{1,0:T(8,128)(2,1)S(1)}, u32[]{:S(2)}, u32[]{:S(2)}) collective-permute-start(bf16[128,2048]{1,0:T(8,128)(2,1)S(1)} %copy-done), channel_id=1, source_target_pairs={{0,1},{1,0},{2,3},{3,2},{4,5},{5,4},{6,7},{7,6},{8,9},{9,8},{10,11... | collective-permute-start | bytes 1572872 | tf_op jit(solution)/shard_map/ppermute | solution.py:31
  61.0 0.6 pad_add_fusion.place_ref
  61.6 0.0 collective-permute-done.1.refs_2_
  61.6 0.9 collective-permute-done.refs_1_
  62.5 0.0 all-to-all-done.kv_ref
  62.5 8.2 %attend.1 = bf16[4,2,144,256]{3,2,1,0:T(8,128)(2,1)} custom-call(s32[4]{0:T(128)} %pad_add_fusion.place_ref, bf16[8,272,256]{2,1,0:T(8,128)(2,1)S(1)} %all-to-all-done.kv_ref, bf16[128,256]{1,0:T(8,128)(2,1)S(1)} %get-tuple-element.12.refs_0_, bf16[128,256]{1,0:T(8,128)(2,1)S(1)} %collective-permute-done.refs_1_, ...), custom_call_target="tpu_custom_call" | custom-call | tf_op jit(solution)/shard_map/attend/pallas_call | solution.py:316
  70.7 4.9 %all-to-all-start.1 = ((bf16[8,144,256]{2,1,0:T(8,128)(2,1)}), bf16[8,144,256]{2,1,0:T(8,128)(2,1)S(1)}, u32[]{:S(2)}, u32[]{:S(2)}) async-start(bf16[8,144,256]{2,1,0:T(8,128)(2,1)} %bitcast.28), calls=%async_computation.1 | async-start | bytes 1179648 | tf_op jit(solution)/shard_map/all_to_all | solution.py:318
  75.6 0.0 collective-permute-done.3.far_weight_ref
  75.6 10.1 %all-to-all-done.1 = bf16[8,144,256]{2,1,0:T(8,128)(2,1)S(1)} async-done(((bf16[8,144,256]{2,1,0:T(8,128)(2,1)}), bf16[8,144,256]{2,1,0:T(8,128)(2,1)S(1)}, u32[]{:S(2)}, u32[]{:S(2)}) %all-to-all-start.1) | async-done | bytes 589856 | tf_op jit(solution)/shard_map/all_to_all | solution.py:318
  85.6 2.1 %project.1 = bf16[8,256,128]{2,1,0:T(8,128)(2,1)} custom-call(s32[4]{0:T(128)} %pad_add_fusion.place_ref, bf16[4,2,144,256]{3,2,1,0:T(8,128)(2,1)S(1)} %bitcast.25, bf16[128,2048]{1,0:T(8,128)(2,1)S(1)} %copy-done, bf16[128,2048]{1,0:T(8,128)(2,1)S(1)} %collective-permute-done.3.far_weight_ref), custom_call_target="tpu_custom_call" | custom-call | tf_op jit(solution)/shard_map/project/pallas_call | solution.py:342
  87.8 3.6 %all-to-all-start.2 = ((bf16[8,256,128]{2,1,0:T(8,128)(2,1)}), bf16[8,256,128]{2,1,0:T(8,128)(2,1)S(1)}, u32[]{:S(2)}, u32[]{:S(2)}) async-start(bf16[8,256,128]{2,1,0:T(8,128)(2,1)} %project.1), calls=%async_computation.2 | async-start | bytes 1048576 | tf_op jit(solution)/shard_map/all_to_all | solution.py:351
  91.4 0.1 eq.62
  91.5 0.0 copy-done.2
  91.6 0.1 and.15
  91.6 0.1 and.16
  91.7 0.2 convolution_convert_fusion.1
  91.9 0.1 eq.59
  92.0 0.1 eq.60
  92.1 0.0 collective-permute-done.4.refs_1_
  92.1 16.4 %all-to-all-done.2 = bf16[8,256,128]{2,1,0:T(8,128)(2,1)S(1)} async-done(((bf16[8,256,128]{2,1,0:T(8,128)(2,1)}), bf16[8,256,128]{2,1,0:T(8,128)(2,1)S(1)}, u32[]{:S(2)}, u32[]{:S(2)}) %all-to-all-start.2) | async-done | bytes 524320 | tf_op jit(solution)/shard_map/all_to_all | solution.py:351
  108.5 0.0 collective-permute-done.6.refs_3_
  108.5 0.1 convert_reduce_fusion
  108.5 0.0 copy-done.1
  108.5 0.3 convolution_convert_fusion
  108.9 21.1 %all_to_all.35 = bf16[32,20,128]{2,1,0:T(8,128)(2,1)S(1)} all-to-all(bf16[32,20,128]{2,1,0:T(8,128)(2,1)S(1)} %reshape.46), channel_id=1, replica_groups=mesh['z'=8,'x'=4,'y'=8,'c'=2] {'z','x'}, dimensions={0} | all-to-all | bytes 327680 | tf_op jit(solution)/shard_map/all_to_all | solution.py:360
  130.1 0.1 broadcast_in_dim.50
  130.1 25.6 %all_to_all.36.rows_in_ref = bf16[16,160,128]{2,1,0:T(8,128)(2,1)S(1)} all-to-all(bf16[16,160,128]{2,1,0:T(8,128)(2,1)S(1)} %bitcast.27), channel_id=1, replica_groups=mesh['z'=8,'x'=4,'y'=8,'c'=2] {'y','c'}, dimensions={0} | all-to-all | bytes 1310720 | tf_op jit(solution)/shard_map/all_to_all | solution.py:366
  155.8 6.8 %expert.1 = bf16[16,160,128]{2,1,0:T(8,128)(2,1)S(1)} custom-call(bf16[16,160,128]{2,1,0:T(8,128)(2,1)S(1)} %all_to_all.36.rows_in_ref, f32[16,1,128]{2,1,0:T(1,128)} %bitcast.34, bf16[3,2048,256]{2,1,0:T(8,128)(2,1)} %pack_weights.1.refs_0_, bf16[3,2048,256]{2,1,0:T(8,128)(2,1)} %collective-permute-done.4.refs_1_, ...), custom_call_target="tpu_custom_call" | custom-call | tf_op jit(solution)/shard_map/expert/pallas_call | solution.py:370
  162.6 22.6 %all_to_all.37 = bf16[16,160,128]{2,1,0:T(8,128)(2,1)S(1)} all-to-all(bf16[16,160,128]{2,1,0:T(8,128)(2,1)S(1)} %expert.1), channel_id=1, replica_groups=mesh['z'=8,'x'=4,'y'=8,'c'=2] {'y','c'}, dimensions={0} | all-to-all | bytes 1310720 | tf_op jit(solution)/shard_map/all_to_all | solution.py:384
  185.2 0.1 reduce_sum.32
  185.3 0.7 reshape.51
  186.0 3.9 %all-to-all-start.6 = ((bf16[32,20,128]{2,1,0:T(8,128)(2,1)}), bf16[32,20,128]{2,1,0:T(8,128)(2,1)S(1)}, u32[]{:S(2)}, u32[]{:S(2)}) async-start(bf16[32,20,128]{2,1,0:T(8,128)(2,1)} %reshape.51), calls=%async_computation.6 | async-start | bytes 393216 | tf_op jit(solution)/shard_map/all_to_all | solution.py:388
  189.9 0.0 copy-done.3
  189.9 11.0 %all-to-all-done.6 = bf16[32,20,128]{2,1,0:T(8,128)(2,1)S(1)} async-done(((bf16[32,20,128]{2,1,0:T(8,128)(2,1)}), bf16[32,20,128]{2,1,0:T(8,128)(2,1)S(1)}, u32[]{:S(2)}, u32[]{:S(2)}) %all-to-all-start.6) | async-done | bytes 163872 | tf_op jit(solution)/shard_map/all_to_all | solution.py:388
  201.0 0.3 convolution_bitcast_fusion
  201.3 0.9 fusion.2
  (10 shorter events, 0.1 us)
Async XLA Ops:
  0.0 58.5 %copy-start = (bf16[128,2048]{1,0:T(8,128)(2,1)S(1)}, bf16[128,2048]{1,0:T(8,128)(2,1)}, u32[]{:S(2)}) copy-start(bf16[128,2048]{1,0:T(8,128)(2,1)} %weight_ref.1) | copy-start | bytes 1572868
  3.0 40.9 %collective-permute-start.5 = (bf16[3,2048,256]{2,1,0:T(8,128)(2,1)}, bf16[3,2048,256]{2,1,0:T(8,128)(2,1)}, u32[]{:S(2)}, u32[]{:S(2)}) collective-permute-start(bf16[3,2048,256]{2,1,0:T(8,128)(2,1)} %pack_weights.1.refs_0_), channel_id=1, source_target_pairs={{0,14},{1,3},{2,0},{3,5},{4,2},{5,7},{6,4},{7,9},{8,6},{9,11},{10,... | collective-permute-start | bytes 9437192 | tf_op jit(solution)/shard_map/ppermute | solution.py:297
  9.2 53.4 %all-to-all-start = ((bf16[8,272,256]{2,1,0:T(8,128)(2,1)}), bf16[8,272,256]{2,1,0:T(8,128)(2,1)S(1)}, u32[]{:S(2)}, u32[]{:S(2)}) async-start(bf16[8,272,256]{2,1,0:T(8,128)(2,1)} %get-tuple-element.11), calls=%async_computation | async-start | bytes 2228224 | tf_op jit(solution)/shard_map/all_to_all | solution.py:272
  19.2 72.9 %collective-permute-start.4 = (bf16[3,2048,256]{2,1,0:T(8,128)(2,1)}, bf16[3,2048,256]{2,1,0:T(8,128)(2,1)}, u32[]{:S(2)}, u32[]{:S(2)}) collective-permute-start(bf16[3,2048,256]{2,1,0:T(8,128)(2,1)} %pack_weights.1.refs_0_), channel_id=1, source_target_pairs={{0,1},{1,0},{2,3},{3,2},{4,5},{5,4},{6,7},{7,6},{8,9},{9,8},{10,11... | collective-permute-start | bytes 9437192 | tf_op jit(solution)/shard_map/ppermute | solution.py:31
  43.9 64.5 %collective-permute-start.6 = (bf16[3,2048,256]{2,1,0:T(8,128)(2,1)}, bf16[3,2048,256]{2,1,0:T(8,128)(2,1)}, u32[]{:S(2)}, u32[]{:S(2)}) collective-permute-start(bf16[3,2048,256]{2,1,0:T(8,128)(2,1)} %collective-permute-done.5.refs_2_), channel_id=1, source_target_pairs={{0,1},{1,0},{2,3},{3,2},{4,5},{5,4},{6,7},{7,6},{8,9},{9,8},{10,11... | collective-permute-start | bytes 9437192 | tf_op jit(solution)/shard_map/ppermute | solution.py:31
  51.3 7.2 %collective-permute-start.2 = (bf16[128,256]{1,0:T(8,128)(2,1)S(1)}, bf16[128,256]{1,0:T(8,128)(2,1)S(1)}, u32[]{:S(2)}, u32[]{:S(2)}) collective-permute-start(bf16[128,256]{1,0:T(8,128)(2,1)S(1)} %get-tuple-element.12.refs_0_), channel_id=1, source_target_pairs={{0,48},{16,0},{32,16},{48,32},{1,49},{17,1},{33,17},{49,33},{2,50}... | collective-permute-start | bytes 196616 | tf_op jit(solution)/shard_map/ppermute | solution.py:274
  53.2 8.4 %collective-permute-start.1 = (bf16[128,256]{1,0:T(8,128)(2,1)S(1)}, bf16[128,256]{1,0:T(8,128)(2,1)S(1)}, u32[]{:S(2)}, u32[]{:S(2)}) collective-permute-start(bf16[128,256]{1,0:T(8,128)(2,1)S(1)} %get-tuple-element.12.refs_0_), channel_id=1, source_target_pairs={{0,32},{16,48},{32,0},{48,16},{1,33},{17,49},{33,1},{49,17},{2,34}... | collective-permute-start | bytes 196616 | tf_op jit(solution)/shard_map/ppermute | solution.py:274
  55.1 7.4 %collective-permute-start = (bf16[128,256]{1,0:T(8,128)(2,1)S(1)}, bf16[128,256]{1,0:T(8,128)(2,1)S(1)}, u32[]{:S(2)}, u32[]{:S(2)}) collective-permute-start(bf16[128,256]{1,0:T(8,128)(2,1)S(1)} %get-tuple-element.12.refs_0_), channel_id=1, source_target_pairs={{0,16},{16,32},{32,48},{48,0},{1,17},{17,33},{33,49},{49,1},{2,18}... | collective-permute-start | bytes 196616 | tf_op jit(solution)/shard_map/ppermute | solution.py:274
  58.5 17.0 %collective-permute-start.3 = (bf16[128,2048]{1,0:T(8,128)(2,1)S(1)}, bf16[128,2048]{1,0:T(8,128)(2,1)S(1)}, u32[]{:S(2)}, u32[]{:S(2)}) collective-permute-start(bf16[128,2048]{1,0:T(8,128)(2,1)S(1)} %copy-done), channel_id=1, source_target_pairs={{0,1},{1,0},{2,3},{3,2},{4,5},{5,4},{6,7},{7,6},{8,9},{9,8},{10,11... | collective-permute-start | bytes 1572872 | tf_op jit(solution)/shard_map/ppermute | solution.py:31
  61.6 29.9 %copy-start.2 = (s32[256,2]{0,1:T(2,128)S(1)}, s32[256,2]{0,1:T(2,128)}, u32[]{:S(2)}) copy-start(s32[256,2]{0,1:T(2,128)} %param.19) | copy-start | bytes 6148
  70.7 15.0 %all-to-all-start.1 = ((bf16[8,144,256]{2,1,0:T(8,128)(2,1)}), bf16[8,144,256]{2,1,0:T(8,128)(2,1)S(1)}, u32[]{:S(2)}, u32[]{:S(2)}) async-start(bf16[8,144,256]{2,1,0:T(8,128)(2,1)} %bitcast.28), calls=%async_computation.1 | async-start | bytes 1179648 | tf_op jit(solution)/shard_map/all_to_all | solution.py:318
  85.6 22.9 %copy-start.1 = (bf16[256,128]{1,0:T(8,128)(2,1)S(1)}, bf16[256,128]{1,0:T(8,128)(2,1)}, u32[]{:S(2)}) copy-start(bf16[256,128]{1,0:T(8,128)(2,1)} %param.12) | copy-start | bytes 196612
  87.8 20.7 %all-to-all-start.2 = ((bf16[8,256,128]{2,1,0:T(8,128)(2,1)}), bf16[8,256,128]{2,1,0:T(8,128)(2,1)S(1)}, u32[]{:S(2)}, u32[]{:S(2)}) async-start(bf16[8,256,128]{2,1,0:T(8,128)(2,1)} %project.1), calls=%async_computation.2 | async-start | bytes 1048576 | tf_op jit(solution)/shard_map/all_to_all | solution.py:351
  155.8 34.1 %copy-start.3 = (f32[256,2]{0,1:T(2,128)S(1)}, f32[256,2]{0,1:T(2,128)}, u32[]{:S(2)}) copy-start(f32[256,2]{0,1:T(2,128)} %param.20) | copy-start | bytes 6148
  186.0 14.9 %all-to-all-start.6 = ((bf16[32,20,128]{2,1,0:T(8,128)(2,1)}), bf16[32,20,128]{2,1,0:T(8,128)(2,1)S(1)}, u32[]{:S(2)}, u32[]{:S(2)}) async-start(bf16[32,20,128]{2,1,0:T(8,128)(2,1)} %reshape.51), calls=%async_computation.6 | async-start | bytes 393216 | tf_op jit(solution)/shard_map/all_to_all | solution.py:388

commit v7 on v6

--- a/solution.py
+++ b/solution.py
@@ -16,6 +16,7 @@
 norm_eps = 1e-06
 masked_score = -1e30
 extra_rows = 16
+gate_rows = 8
 lane = 128
 
 
@@ -49,7 +50,7 @@
         for place, part in enumerate(three_parts(gates_ref[head : head + 1])):
             gates = jnp.where(row == 3 * head + place, part, gates)
     message = jnp.concatenate(
-        [keys_ref[...], values_ref[...], gates.astype(jnp.bfloat16)], axis=0
+        [keys_ref[...], values_ref[...], gates[:gate_rows].astype(jnp.bfloat16)], axis=0
     )
     for copy in range(out_ref.shape[0]):
         out_ref[copy] = message
@@ -65,7 +66,7 @@
     row = lax.broadcasted_iota(jnp.int32, (extra_rows, tokens), 0)
     ones = jnp.ones((extra_rows, tokens), jnp.bfloat16)
     for head in range(head_count):
-        counted = ((row >= 3 * head) & (row < 3 * head + 3)) | (row == extra_rows - 1)
+        counted = ((row >= 3 * head) & (row < 3 * head + 3)) | (row == gate_rows - 1)
         minus = jnp.where(counted, -1.0, 0.0).astype(jnp.bfloat16)
         rows = slice(head * head_width, (head + 1) * head_width)
         for shift in range(x_count):
@@ -80,12 +81,12 @@
             later = jnp.where((block > 0) & (z_place + block < z_count), -2 * masked_score, 0.0)
             gates = kv_ref[source, 2 * head_count * head_width :]
             key_scratch[head, :head_width, columns] = kv_ref[source, rows]
-            key_scratch[head, head_width:, columns] = jnp.where(
-                row == extra_rows - 1, later, gates.astype(jnp.float32)
-            ).astype(jnp.bfloat16)
+            gates = jnp.where(row[:gate_rows] == gate_rows - 1, later, gates.astype(jnp.float32))
+            gates = jnp.concatenate([gates, jnp.zeros_like(gates)], axis=0)
+            key_scratch[head, head_width:, columns] = gates.astype(jnp.bfloat16)
             value_scratch[head, :head_width, columns] = kv_ref[source, first : first + head_width]
             value_scratch[head, head_width:, columns] = ones
-    wide = 2 * tokens if x_count % 2 == 0 else tokens
+    wide = x_count * tokens
     stats = [jnp.zeros((extra_rows, tokens), jnp.float32)] * x_count
     for head in range(head_count):
         rows = slice(head * head_width, (head + 1) * head_width)
@@ -100,10 +101,14 @@
             key_place = lax.broadcasted_iota(jnp.int32, near.shape, 0) + x_place * tokens
             query_place = lax.broadcasted_iota(jnp.int32, near.shape, 1) + first
             near = jnp.where(key_place <= query_place, near, 2 * masked_score)
-            scores = jnp.concatenate([near, scores[tokens:]], axis=0)
-            peak = jnp.maximum(jnp.max(scores, axis=0, keepdims=True), masked_score)
-            weights = jnp.exp(scores - peak).astype(jnp.bfloat16)
-            summed = jnp.dot(value_scratch[head], weights, preferred_element_type=jnp.float32)
+            rest = scores[tokens:]
+            peak = jnp.maximum(jnp.max(near, axis=0, keepdims=True), jnp.max(rest, axis=0, keepdims=True))
+            peak = jnp.maximum(peak, masked_score)
+            near_weights = jnp.exp(near - peak).astype(jnp.bfloat16)
+            rest_weights = jnp.exp(rest - peak).astype(jnp.bfloat16)
+            summed = jnp.dot(
+                value_scratch[head, :, :tokens], near_weights, preferred_element_type=jnp.float32
+            ) + jnp.dot(value_scratch[head, :, tokens:], rest_weights, preferred_element_type=jnp.float32)
             for block in range(first // tokens, (first + wide) // tokens):
                 columns = slice(block * tokens - first, (block + 1) * tokens - first)
                 part_sum = summed[:head_width, columns].astype(jnp.bfloat16)
@@ -257,7 +262,7 @@
     vmem = pl.BlockSpec(memory_space=pltpu.VMEM)
 
     deep = head_width + extra_rows
-    message_rows = 2 * head_count * head_width + extra_rows
+    message_rows = 2 * head_count * head_width + gate_rows
     message, scaled = pl.pallas_call(
         functools.partial(pack_kernel, head_width),
         out_shape=(
@@ -357,9 +362,7 @@
     stream = (residual.astype(f32) + head_sum).astype(bf16)
 
     sent = jnp.dot(taken, stream, preferred_element_type=f32).astype(bf16)
-    arrived = lax.all_to_all(
-        sent.reshape(sp_count, capacity, local_width), SP, split_axis=0, concat_axis=0, tiled=True
-    )
+    arrived = lax.all_to_all(sent.reshape(sp_count, capacity, local_width), SP, split_axis=0, concat_axis=0, tiled=True)
     quarter = slot_total // 4
     arrived = arrived.reshape(4, quarter, local_width)
     copies = jnp.broadcast_to(arrived, (y_count // 2, *arrived.shape))
@@ -414,6 +417,4 @@
         P(SP, None, TP),
         P(SP, TP, None),
     )
-    return jax.shard_map(
-        shards, mesh=finer, in_specs=in_specs, out_specs=P(SP, TP), check_vma=False
-    )
+    return jax.shard_map(shards, mesh=finer, in_specs=in_specs, out_specs=P(SP, TP), check_vma=False)

time: 203 us -> 202 us (level)
  no operation moved by 1% of the time
where the time goes in v7:
time: 202 us; the launch traced here: 201 us
  blocking collectives  69.3 us (34%)
  waiting for transfers between devices  58.1 us (29%)
  starting transfers between devices  48.5 us (24%)
  Pallas kernels  21.2 us (10%)
    all_to_all x1, blocking collectives, shards(): lax.all_to_all(copies.reshape(2 * y_count, quarter, local_width), TP, spl...  25.6 us
    all_to_all x1, blocking collectives, shards(): lax.all_to_all(out_rows, TP, split_axis=0, concat_axis=0, tiled=True)  22.6 us
    all_to_all x1, blocking collectives, shards(): lax.all_to_all(sent.reshape(sp_count, capacity, local_width), SP, split_a...  21.1 us
    ppermute x1, waiting for transfers between devices, shards(): near_set = lax.ppermute(own_set, TP, slice_moves)  19.7 us
    all_to_all x1, waiting for transfers between devices, shards(): lax.all_to_all(projected, 'y', split_axis=0, concat_axis=0, tiled=True)  16.4 us
    ppermute x3, starting transfers between devices, swapped(): return lax.ppermute(shard, 'c', [(0, 1), (1, 0)])  14.8 us
    all_to_all x1, waiting for transfers between devices, shards(): lax.all_to_all(expert_out.reshape(sp_count, capacity, local_width), SP, s...  11 us
    all_to_all x1, waiting for transfers between devices, shards(): lax.all_to_all(parts.reshape(2 * x_count, *part_shape[2:]), ('x', 'c'), s...  10.1 us
  transfers between devices with their start and end apart: 11, of which 5 were waited for; matrix products, arithmetic and copies ran while one was open for 1% of the time, Pallas kernels for 6%

profile of v7, /device:TPU:1, one launch (start us, length us, event | category | flops | bytes accessed | tf_op | source)
XLA Modules:
  0.0 201.2 jit_solution(16833938560948712221)
XLA Ops:
  0.0 3.0 %pack_weights.1.refs_0_ = bf16[3,2048,256]{2,1,0:T(8,128)(2,1)} custom-call(bf16[2048,256]{1,0:T(8,128)(2,1)} %bitcast.29, bf16[2048,256]{1,0:T(8,128)(2,1)} %bitcast.30, bf16[256,2048]{1,0:T(8,128)(2,1)} %bitcast.31), custom_call_target="tpu_custom_call" | custom-call | tf_op jit(solution)/shard_map/pack_weights/pallas_call | solution.py:289
  3.0 4.0 %collective-permute-start.5 = (bf16[3,2048,256]{2,1,0:T(8,128)(2,1)}, bf16[3,2048,256]{2,1,0:T(8,128)(2,1)}, u32[]{:S(2)}, u32[]{:S(2)}) collective-permute-start(bf16[3,2048,256]{2,1,0:T(8,128)(2,1)} %pack_weights.1.refs_0_), channel_id=1, source_target_pairs={{0,14},{1,3},{2,0},{3,5},{4,2},{5,7},{6,4},{7,9},{8,6},{9,11},{10,... | collective-permute-start | bytes 9437192 | tf_op jit(solution)/shard_map/ppermute | solution.py:302
  7.1 2.1 %pack.1 = (bf16[8,264,256]{2,1,0:T(8,128)(2,1)}, bf16[128,256]{1,0:T(8,128)(2,1)S(1)}) custom-call(bf16[128,256]{1,0:T(8,128)(2,1)} %keys_ref.1, bf16[128,256]{1,0:T(8,128)(2,1)} %values_ref.1, f32[2,256]{1,0:T(2,128)} %gates_ref.1, bf16[128,256]{1,0:T(8,128)(2,1)} %queries_ref.1), custom_call_target="tpu_custom_call" | custom-call | tf_op jit(solution)/shard_map/pack/pallas_call | solution.py:266
  9.1 10.0 %all-to-all-start = ((bf16[8,264,256]{2,1,0:T(8,128)(2,1)}), bf16[8,264,256]{2,1,0:T(8,128)(2,1)S(1)}, u32[]{:S(2)}, u32[]{:S(2)}) async-start(bf16[8,264,256]{2,1,0:T(8,128)(2,1)} %get-tuple-element.11), calls=%async_computation | async-start | bytes 2162688 | tf_op jit(solution)/shard_map/all_to_all | solution.py:277
  19.2 5.0 %collective-permute-start.4 = (bf16[3,2048,256]{2,1,0:T(8,128)(2,1)}, bf16[3,2048,256]{2,1,0:T(8,128)(2,1)}, u32[]{:S(2)}, u32[]{:S(2)}) collective-permute-start(bf16[3,2048,256]{2,1,0:T(8,128)(2,1)} %pack_weights.1.refs_0_), channel_id=1, source_target_pairs={{0,1},{1,0},{2,3},{3,2},{4,5},{5,4},{6,7},{7,6},{8,9},{9,8},{10,11... | collective-permute-start | bytes 9437192 | tf_op jit(solution)/shard_map/ppermute | solution.py:32
  24.2 19.7 %collective-permute-done.5.refs_2_ = bf16[3,2048,256]{2,1,0:T(8,128)(2,1)} collective-permute-done((bf16[3,2048,256]{2,1,0:T(8,128)(2,1)}, bf16[3,2048,256]{2,1,0:T(8,128)(2,1)}, u32[]{:S(2)}, u32[]{:S(2)}) %collective-permute-start.5) | collective-permute-done | bytes 3145760 | tf_op jit(solution)/shard_map/ppermute | solution.py:302
  43.9 7.3 %collective-permute-start.6 = (bf16[3,2048,256]{2,1,0:T(8,128)(2,1)}, bf16[3,2048,256]{2,1,0:T(8,128)(2,1)}, u32[]{:S(2)}, u32[]{:S(2)}) collective-permute-start(bf16[3,2048,256]{2,1,0:T(8,128)(2,1)} %collective-permute-done.5.refs_2_), channel_id=1, source_target_pairs={{0,1},{1,0},{2,3},{3,2},{4,5},{5,4},{6,7},{7,6},{8,9},{9,8},{10,11... | collective-permute-start | bytes 9437192 | tf_op jit(solution)/shard_map/ppermute | solution.py:32
  51.3 1.9 collective-permute-start.2
  53.2 1.9 collective-permute-start.1
  55.1 3.4 %collective-permute-start = (bf16[128,256]{1,0:T(8,128)(2,1)S(1)}, bf16[128,256]{1,0:T(8,128)(2,1)S(1)}, u32[]{:S(2)}, u32[]{:S(2)}) collective-permute-start(bf16[128,256]{1,0:T(8,128)(2,1)S(1)} %get-tuple-element.12.refs_0_), channel_id=1, source_target_pairs={{0,16},{16,32},{32,48},{48,0},{1,17},{17,33},{33,49},{49,1},{2,18}... | collective-permute-start | bytes 196616 | tf_op jit(solution)/shard_map/ppermute | solution.py:279
  58.5 0.0 collective-permute-done.2.refs_3_
  58.5 0.0 copy-done
  58.5 2.5 %collective-permute-start.3 = (bf16[128,2048]{1,0:T(8,128)(2,1)S(1)}, bf16[128,2048]{1,0:T(8,128)(2,1)S(1)}, u32[]{:S(2)}, u32[]{:S(2)}) collective-permute-start(bf16[128,2048]{1,0:T(8,128)(2,1)S(1)} %copy-done), channel_id=1, source_target_pairs={{0,1},{1,0},{2,3},{3,2},{4,5},{5,4},{6,7},{7,6},{8,9},{9,8},{10,11... | collective-permute-start | bytes 1572872 | tf_op jit(solution)/shard_map/ppermute | solution.py:32
  61.0 0.6 pad_add_fusion.place_ref
  61.6 0.0 collective-permute-done.1.refs_2_
  61.6 0.9 collective-permute-done.refs_1_
  62.5 0.0 all-to-all-done.kv_ref
  62.5 7.2 %attend.1 = bf16[4,2,144,256]{3,2,1,0:T(8,128)(2,1)} custom-call(s32[4]{0:T(128)} %pad_add_fusion.place_ref, bf16[8,264,256]{2,1,0:T(8,128)(2,1)S(1)} %all-to-all-done.kv_ref, bf16[128,256]{1,0:T(8,128)(2,1)S(1)} %get-tuple-element.12.refs_0_, bf16[128,256]{1,0:T(8,128)(2,1)S(1)} %collective-permute-done.refs_1_, ...), custom_call_target="tpu_custom_call" | custom-call | tf_op jit(solution)/shard_map/attend/pallas_call | solution.py:321
  69.7 4.9 %all-to-all-start.1 = ((bf16[8,144,256]{2,1,0:T(8,128)(2,1)}), bf16[8,144,256]{2,1,0:T(8,128)(2,1)S(1)}, u32[]{:S(2)}, u32[]{:S(2)}) async-start(bf16[8,144,256]{2,1,0:T(8,128)(2,1)} %bitcast.28), calls=%async_computation.1 | async-start | bytes 1179648 | tf_op jit(solution)/shard_map/all_to_all | solution.py:323
  74.6 0.0 collective-permute-done.3.far_weight_ref
  74.6 10.1 %all-to-all-done.1 = bf16[8,144,256]{2,1,0:T(8,128)(2,1)S(1)} async-done(((bf16[8,144,256]{2,1,0:T(8,128)(2,1)}), bf16[8,144,256]{2,1,0:T(8,128)(2,1)S(1)}, u32[]{:S(2)}, u32[]{:S(2)}) %all-to-all-start.1) | async-done | bytes 589856 | tf_op jit(solution)/shard_map/all_to_all | solution.py:323
  84.7 2.1 %project.1 = bf16[8,256,128]{2,1,0:T(8,128)(2,1)} custom-call(s32[4]{0:T(128)} %pad_add_fusion.place_ref, bf16[4,2,144,256]{3,2,1,0:T(8,128)(2,1)S(1)} %bitcast.25, bf16[128,2048]{1,0:T(8,128)(2,1)S(1)} %copy-done, bf16[128,2048]{1,0:T(8,128)(2,1)S(1)} %collective-permute-done.3.far_weight_ref), custom_call_target="tpu_custom_call" | custom-call | tf_op jit(solution)/shard_map/project/pallas_call | solution.py:347
  86.8 3.6 %all-to-all-start.2 = ((bf16[8,256,128]{2,1,0:T(8,128)(2,1)}), bf16[8,256,128]{2,1,0:T(8,128)(2,1)S(1)}, u32[]{:S(2)}, u32[]{:S(2)}) async-start(bf16[8,256,128]{2,1,0:T(8,128)(2,1)} %project.1), calls=%async_computation.2 | async-start | bytes 1048576 | tf_op jit(solution)/shard_map/all_to_all | solution.py:356
  90.5 0.1 eq.62
  90.6 0.0 copy-done.2
  90.6 0.1 and.15
  90.7 0.1 and.16
  90.8 0.2 convolution_convert_fusion.1
  90.9 0.1 eq.59
  91.0 0.1 eq.60
  91.1 0.0 collective-permute-done.4.refs_1_
  91.1 16.4 %all-to-all-done.2 = bf16[8,256,128]{2,1,0:T(8,128)(2,1)S(1)} async-done(((bf16[8,256,128]{2,1,0:T(8,128)(2,1)}), bf16[8,256,128]{2,1,0:T(8,128)(2,1)S(1)}, u32[]{:S(2)}, u32[]{:S(2)}) %all-to-all-start.2) | async-done | bytes 524320 | tf_op jit(solution)/shard_map/all_to_all | solution.py:356
  107.5 0.0 collective-permute-done.6.refs_3_
  107.5 0.1 convert_reduce_fusion
  107.6 0.0 copy-done.1
  107.6 0.3 convolution_convert_fusion
  107.9 21.1 %all_to_all.35 = bf16[32,20,128]{2,1,0:T(8,128)(2,1)S(1)} all-to-all(bf16[32,20,128]{2,1,0:T(8,128)(2,1)S(1)} %reshape.46), channel_id=1, replica_groups=mesh['z'=8,'x'=4,'y'=8,'c'=2] {'z','x'}, dimensions={0} | all-to-all | bytes 327680 | tf_op jit(solution)/shard_map/all_to_all | solution.py:365
  129.1 0.1 broadcast_in_dim.50
  129.2 25.6 %all_to_all.36.rows_in_ref = bf16[16,160,128]{2,1,0:T(8,128)(2,1)S(1)} all-to-all(bf16[16,160,128]{2,1,0:T(8,128)(2,1)S(1)} %bitcast.27), channel_id=1, replica_groups=mesh['z'=8,'x'=4,'y'=8,'c'=2] {'y','c'}, dimensions={0} | all-to-all | bytes 1310720 | tf_op jit(solution)/shard_map/all_to_all | solution.py:369
  154.8 6.8 %expert.1 = bf16[16,160,128]{2,1,0:T(8,128)(2,1)S(1)} custom-call(bf16[16,160,128]{2,1,0:T(8,128)(2,1)S(1)} %all_to_all.36.rows_in_ref, f32[16,1,128]{2,1,0:T(1,128)} %bitcast.34, bf16[3,2048,256]{2,1,0:T(8,128)(2,1)} %pack_weights.1.refs_0_, bf16[3,2048,256]{2,1,0:T(8,128)(2,1)} %collective-permute-done.4.refs_1_, ...), custom_call_target="tpu_custom_call" | custom-call | tf_op jit(solution)/shard_map/expert/pallas_call | solution.py:373
  161.6 22.6 %all_to_all.37 = bf16[16,160,128]{2,1,0:T(8,128)(2,1)S(1)} all-to-all(bf16[16,160,128]{2,1,0:T(8,128)(2,1)S(1)} %expert.1), channel_id=1, replica_groups=mesh['z'=8,'x'=4,'y'=8,'c'=2] {'y','c'}, dimensions={0} | all-to-all | bytes 1310720 | tf_op jit(solution)/shard_map/all_to_all | solution.py:387
  184.2 0.1 reduce_sum.32
  184.3 0.7 reshape.51
  185.0 3.9 %all-to-all-start.6 = ((bf16[32,20,128]{2,1,0:T(8,128)(2,1)}), bf16[32,20,128]{2,1,0:T(8,128)(2,1)S(1)}, u32[]{:S(2)}, u32[]{:S(2)}) async-start(bf16[32,20,128]{2,1,0:T(8,128)(2,1)} %reshape.51), calls=%async_computation.6 | async-start | bytes 393216 | tf_op jit(solution)/shard_map/all_to_all | solution.py:391
  188.9 0.0 copy-done.3
  189.0 11.0 %all-to-all-done.6 = bf16[32,20,128]{2,1,0:T(8,128)(2,1)S(1)} async-done(((bf16[32,20,128]{2,1,0:T(8,128)(2,1)}), bf16[32,20,128]{2,1,0:T(8,128)(2,1)S(1)}, u32[]{:S(2)}, u32[]{:S(2)}) %all-to-all-start.6) | async-done | bytes 163872 | tf_op jit(solution)/shard_map/all_to_all | solution.py:391
  200.0 0.3 convolution_bitcast_fusion
  200.3 0.9 fusion.2
  (10 shorter events, 0.1 us)
Async XLA Ops:
  0.0 58.5 %copy-start = (bf16[128,2048]{1,0:T(8,128)(2,1)S(1)}, bf16[128,2048]{1,0:T(8,128)(2,1)}, u32[]{:S(2)}) copy-start(bf16[128,2048]{1,0:T(8,128)(2,1)} %weight_ref.1) | copy-start | bytes 1572868
  3.0 40.9 %collective-permute-start.5 = (bf16[3,2048,256]{2,1,0:T(8,128)(2,1)}, bf16[3,2048,256]{2,1,0:T(8,128)(2,1)}, u32[]{:S(2)}, u32[]{:S(2)}) collective-permute-start(bf16[3,2048,256]{2,1,0:T(8,128)(2,1)} %pack_weights.1.refs_0_), channel_id=1, source_target_pairs={{0,14},{1,3},{2,0},{3,5},{4,2},{5,7},{6,4},{7,9},{8,6},{9,11},{10,... | collective-permute-start | bytes 9437192 | tf_op jit(solution)/shard_map/ppermute | solution.py:302
  9.1 53.4 %all-to-all-start = ((bf16[8,264,256]{2,1,0:T(8,128)(2,1)}), bf16[8,264,256]{2,1,0:T(8,128)(2,1)S(1)}, u32[]{:S(2)}, u32[]{:S(2)}) async-start(bf16[8,264,256]{2,1,0:T(8,128)(2,1)} %get-tuple-element.11), calls=%async_computation | async-start | bytes 2162688 | tf_op jit(solution)/shard_map/all_to_all | solution.py:277
  19.2 71.9 %collective-permute-start.4 = (bf16[3,2048,256]{2,1,0:T(8,128)(2,1)}, bf16[3,2048,256]{2,1,0:T(8,128)(2,1)}, u32[]{:S(2)}, u32[]{:S(2)}) collective-permute-start(bf16[3,2048,256]{2,1,0:T(8,128)(2,1)} %pack_weights.1.refs_0_), channel_id=1, source_target_pairs={{0,1},{1,0},{2,3},{3,2},{4,5},{5,4},{6,7},{7,6},{8,9},{9,8},{10,11... | collective-permute-start | bytes 9437192 | tf_op jit(solution)/shard_map/ppermute | solution.py:32
  43.9 63.6 %collective-permute-start.6 = (bf16[3,2048,256]{2,1,0:T(8,128)(2,1)}, bf16[3,2048,256]{2,1,0:T(8,128)(2,1)}, u32[]{:S(2)}, u32[]{:S(2)}) collective-permute-start(bf16[3,2048,256]{2,1,0:T(8,128)(2,1)} %collective-permute-done.5.refs_2_), channel_id=1, source_target_pairs={{0,1},{1,0},{2,3},{3,2},{4,5},{5,4},{6,7},{7,6},{8,9},{9,8},{10,11... | collective-permute-start | bytes 9437192 | tf_op jit(solution)/shard_map/ppermute | solution.py:32
  51.3 7.2 %collective-permute-start.2 = (bf16[128,256]{1,0:T(8,128)(2,1)S(1)}, bf16[128,256]{1,0:T(8,128)(2,1)S(1)}, u32[]{:S(2)}, u32[]{:S(2)}) collective-permute-start(bf16[128,256]{1,0:T(8,128)(2,1)S(1)} %get-tuple-element.12.refs_0_), channel_id=1, source_target_pairs={{0,48},{16,0},{32,16},{48,32},{1,49},{17,1},{33,17},{49,33},{2,50}... | collective-permute-start | bytes 196616 | tf_op jit(solution)/shard_map/ppermute | solution.py:279
  53.2 8.4 %collective-permute-start.1 = (bf16[128,256]{1,0:T(8,128)(2,1)S(1)}, bf16[128,256]{1,0:T(8,128)(2,1)S(1)}, u32[]{:S(2)}, u32[]{:S(2)}) collective-permute-start(bf16[128,256]{1,0:T(8,128)(2,1)S(1)} %get-tuple-element.12.refs_0_), channel_id=1, source_target_pairs={{0,32},{16,48},{32,0},{48,16},{1,33},{17,49},{33,1},{49,17},{2,34}... | collective-permute-start | bytes 196616 | tf_op jit(solution)/shard_map/ppermute | solution.py:279
  55.1 7.4 %collective-permute-start = (bf16[128,256]{1,0:T(8,128)(2,1)S(1)}, bf16[128,256]{1,0:T(8,128)(2,1)S(1)}, u32[]{:S(2)}, u32[]{:S(2)}) collective-permute-start(bf16[128,256]{1,0:T(8,128)(2,1)S(1)} %get-tuple-element.12.refs_0_), channel_id=1, source_target_pairs={{0,16},{16,32},{32,48},{48,0},{1,17},{17,33},{33,49},{49,1},{2,18}... | collective-permute-start | bytes 196616 | tf_op jit(solution)/shard_map/ppermute | solution.py:279
  58.5 16.1 %collective-permute-start.3 = (bf16[128,2048]{1,0:T(8,128)(2,1)S(1)}, bf16[128,2048]{1,0:T(8,128)(2,1)S(1)}, u32[]{:S(2)}, u32[]{:S(2)}) collective-permute-start(bf16[128,2048]{1,0:T(8,128)(2,1)S(1)} %copy-done), channel_id=1, source_target_pairs={{0,1},{1,0},{2,3},{3,2},{4,5},{5,4},{6,7},{7,6},{8,9},{9,8},{10,11... | collective-permute-start | bytes 1572872 | tf_op jit(solution)/shard_map/ppermute | solution.py:32
  61.6 29.0 %copy-start.2 = (s32[256,2]{0,1:T(2,128)S(1)}, s32[256,2]{0,1:T(2,128)}, u32[]{:S(2)}) copy-start(s32[256,2]{0,1:T(2,128)} %param.19) | copy-start | bytes 6148
  69.7 15.0 %all-to-all-start.1 = ((bf16[8,144,256]{2,1,0:T(8,128)(2,1)}), bf16[8,144,256]{2,1,0:T(8,128)(2,1)S(1)}, u32[]{:S(2)}, u32[]{:S(2)}) async-start(bf16[8,144,256]{2,1,0:T(8,128)(2,1)} %bitcast.28), calls=%async_computation.1 | async-start | bytes 1179648 | tf_op jit(solution)/shard_map/all_to_all | solution.py:323
  84.7 22.9 %copy-start.1 = (bf16[256,128]{1,0:T(8,128)(2,1)S(1)}, bf16[256,128]{1,0:T(8,128)(2,1)}, u32[]{:S(2)}) copy-start(bf16[256,128]{1,0:T(8,128)(2,1)} %param.12) | copy-start | bytes 196612
  86.8 20.6 %all-to-all-start.2 = ((bf16[8,256,128]{2,1,0:T(8,128)(2,1)}), bf16[8,256,128]{2,1,0:T(8,128)(2,1)S(1)}, u32[]{:S(2)}, u32[]{:S(2)}) async-start(bf16[8,256,128]{2,1,0:T(8,128)(2,1)} %project.1), calls=%async_computation.2 | async-start | bytes 1048576 | tf_op jit(solution)/shard_map/all_to_all | solution.py:356
  154.8 34.1 %copy-start.3 = (f32[256,2]{0,1:T(2,128)S(1)}, f32[256,2]{0,1:T(2,128)}, u32[]{:S(2)}) copy-start(f32[256,2]{0,1:T(2,128)} %param.20) | copy-start | bytes 6148
  185.0 14.9 %all-to-all-start.6 = ((bf16[32,20,128]{2,1,0:T(8,128)(2,1)}), bf16[32,20,128]{2,1,0:T(8,128)(2,1)S(1)}, u32[]{:S(2)}, u32[]{:S(2)}) async-start(bf16[32,20,128]{2,1,0:T(8,128)(2,1)} %reshape.51), calls=%async_computation.6 | async-start | bytes 393216 | tf_op jit(solution)/shard_map/all_to_all | solution.py:391

commit v8 on v7

--- a/solution.py
+++ b/solution.py
@@ -303,6 +303,20 @@
     own_swapped = swapped(own_set)
     far_out_weight = swapped(out_weight)
     near_swapped = swapped(near_set)
+    expert_ids = jnp.arange(sp_count, dtype=jnp.int32)
+    chosen = routes[:, :, None] == expert_ids
+    named = jnp.any(chosen, axis=1)
+    token_ids = jnp.arange(token_count, dtype=jnp.int32)
+    before = (token_ids[None, :] < token_ids[:, None]).astype(bf16)
+    rank = jnp.dot(before, named.astype(bf16), preferred_element_type=f32).astype(jnp.int32)
+    slot_ids = jnp.arange(capacity, dtype=jnp.int32)
+    taken = (named.T[:, None, :] & (rank.T[:, None, :] == slot_ids[:, None])).astype(bf16)
+    taken = taken.reshape(slot_total, token_count)
+    share = jnp.sum(jnp.where(chosen, route_weight[:, :, None], 0.0), axis=1)
+    share_first = lax.reduce_precision(share, 8, 7)
+    share_rest = (share - share_first).astype(bf16)
+
+    gathered, taken = lax.optimization_barrier((gathered, taken))
     attend = pl.pallas_call(
         functools.partial(attend_kernel, head_count, head_width),
         out_shape=jax.ShapeDtypeStruct(
@@ -323,19 +337,7 @@
     received = lax.all_to_all(
         parts.reshape(2 * x_count, *part_shape[2:]), ("x", "c"), split_axis=0, concat_axis=0, tiled=True
     ).reshape(part_shape)
-
-    expert_ids = jnp.arange(sp_count, dtype=jnp.int32)
-    chosen = routes[:, :, None] == expert_ids
-    named = jnp.any(chosen, axis=1)
-    token_ids = jnp.arange(token_count, dtype=jnp.int32)
-    before = (token_ids[None, :] < token_ids[:, None]).astype(bf16)
-    rank = jnp.dot(before, named.astype(bf16), preferred_element_type=f32).astype(jnp.int32)
-    slot_ids = jnp.arange(capacity, dtype=jnp.int32)
-    taken = (named.T[:, None, :] & (rank.T[:, None, :] == slot_ids[:, None])).astype(bf16)
-    taken = taken.reshape(slot_total, token_count)
-    share = jnp.sum(jnp.where(chosen, route_weight[:, :, None], 0.0), axis=1)
-    share_first = lax.reduce_precision(share, 8, 7)
-    share_rest = (share - share_first).astype(bf16)
+    received, own_swapped = lax.optimization_barrier((received, own_swapped))
 
     def spread(weights):
         return jnp.where(
@@ -346,7 +348,7 @@
 
     projected = pl.pallas_call(
         functools.partial(project_kernel, head_count, head_width),
-        out_shape=jax.ShapeDtypeStruct((y_count, token_count, local_width), bf16),
+        out_shape=kept((y_count, token_count, local_width), bf16),
         in_specs=[smem, vmem, vmem, vmem],
         out_specs=vmem,
         scratch_shapes=[pltpu.VMEM((2 * head_count * head_width, y_count * local_width), bf16)],
@@ -354,9 +356,6 @@
         interpret=INTERPRET,
     )(place, held(received), held(out_weight), held(far_out_weight))
     pieces = lax.all_to_all(projected, "y", split_axis=0, concat_axis=0, tiled=True)
-    pieces, own_swapped, near_set, near_swapped = lax.optimization_barrier(
-        (pieces, own_swapped, near_set, near_swapped)
-    )
     weight_sets = [own_set, own_swapped, near_set, near_swapped]
     head_sum = jnp.sum(pieces.astype(f32), axis=0)
     stream = (residual.astype(f32) + head_sum).astype(bf16)

time: 202 us -> 184 us (0.911)
  waiting for transfers between devices: 58.1 us -> 34.1 us
  blocking collectives: 69.3 us -> 81.7 us
  starting transfers between devices: 48.5 us -> 43.1 us
    ppermute x1, waiting for transfers between devices: 19.7 us -> 0.01 us  [shards(): near_set = lax.ppermute(own_set, TP, slice_moves)]
    all_to_all x0 -> x1, blocking collectives: none -> 19.5 us  [shards(): lax.all_to_all(projected, 'y', split_axis=0, concat_axis=0, tiled=True)]
    all_to_all x1 -> x0, waiting for transfers between devices: 16.4 us -> none  [shards(): lax.all_to_all(projected, 'y', split_axis=0, concat_axis=0, tiled=True)]
    all_to_all x1, waiting for transfers between devices: 0.01 us -> 14.9 us  [shards(): lax.all_to_all(message, 'z', split_axis=0, concat_axis=0, tiled=True)]
    all_to_all x1, blocking collectives: 21.1 us -> 13 us  [shards(): lax.all_to_all(sent.reshape(sp_count, capacity, local_width), SP, split_a...]
    all_to_all x1 -> x0, starting transfers between devices: 3.62 us -> none  [shards(): lax.all_to_all(projected, 'y', split_axis=0, concat_axis=0, tiled=True)]
    ppermute x3, starting transfers between devices: 7.2 us -> 10.5 us  [shards(): lax.ppermute(scaled, 'x', [(i, (i + shift) % x_count) for i in range(x_co...]
    ppermute x3, starting transfers between devices: 14.8 us -> 11.6 us  [swapped(): return lax.ppermute(shard, 'c', [(0, 1), (1, 0)])]
  transfers between devices with their start and end apart: 11 -> 10, of which waited for: 5 -> 3; matrix products, arithmetic and copies ran while one was open for 1% -> 1% of each run, Pallas kernels for 6% -> 6%
where the time goes in v8:
time: 184 us; the launch traced here: 183 us
  blocking collectives  81.7 us (44%)
  starting transfers between devices  43.1 us (23%)
  waiting for transfers between devices  34.1 us (19%)
  Pallas kernels  20.2 us (11%)
    all_to_all x1, blocking collectives, shards(): lax.all_to_all(copies.reshape(2 * y_count, quarter, local_width), TP, spl...  26.6 us
    all_to_all x1, blocking collectives, shards(): lax.all_to_all(out_rows, TP, split_axis=0, concat_axis=0, tiled=True)  22.6 us
    all_to_all x1, blocking collectives, shards(): lax.all_to_all(projected, 'y', split_axis=0, concat_axis=0, tiled=True)  19.5 us
    all_to_all x1, waiting for transfers between devices, shards(): lax.all_to_all(message, 'z', split_axis=0, concat_axis=0, tiled=True)  14.9 us
    all_to_all x1, blocking collectives, shards(): lax.all_to_all(sent.reshape(sp_count, capacity, local_width), SP, split_a...  13 us
    ppermute x3, starting transfers between devices, swapped(): return lax.ppermute(shard, 'c', [(0, 1), (1, 0)])  11.6 us
    all_to_all x1, waiting for transfers between devices, shards(): lax.all_to_all(expert_out.reshape(sp_count, capacity, local_width), SP, s...  11 us
    ppermute x3, starting transfers between devices, shards(): lax.ppermute(scaled, 'x', [(i, (i + shift) % x_count) for i in range(x_co...  10.5 us
  transfers between devices with their start and end apart: 10, of which 3 were waited for; matrix products, arithmetic and copies ran while one was open for 1% of the time, Pallas kernels for 6%

profile of v8, /device:TPU:1, one launch (start us, length us, event | category | flops | bytes accessed | tf_op | source)
XLA Modules:
  0.0 183.2 jit_solution(10539273552167005653)
XLA Ops:
  0.0 3.0 %pack_weights.1.refs_0_ = bf16[3,2048,256]{2,1,0:T(8,128)(2,1)} custom-call(bf16[2048,256]{1,0:T(8,128)(2,1)} %bitcast.30, bf16[2048,256]{1,0:T(8,128)(2,1)} %bitcast.31, bf16[256,2048]{1,0:T(8,128)(2,1)} %bitcast.32), custom_call_target="tpu_custom_call" | custom-call | tf_op jit(solution)/shard_map/pack_weights/pallas_call | solution.py:289
  3.0 4.0 %collective-permute-start.5 = (bf16[3,2048,256]{2,1,0:T(8,128)(2,1)}, bf16[3,2048,256]{2,1,0:T(8,128)(2,1)}, u32[]{:S(2)}, u32[]{:S(2)}) collective-permute-start(bf16[3,2048,256]{2,1,0:T(8,128)(2,1)} %pack_weights.1.refs_0_), channel_id=1, source_target_pairs={{0,14},{1,3},{2,0},{3,5},{4,2},{5,7},{6,4},{7,9},{8,6},{9,11},{10,... | collective-permute-start | bytes 9437192 | tf_op jit(solution)/shard_map/ppermute | solution.py:302
  7.0 6.6 %collective-permute-start.3 = (bf16[3,2048,256]{2,1,0:T(8,128)(2,1)}, bf16[3,2048,256]{2,1,0:T(8,128)(2,1)}, u32[]{:S(2)}, u32[]{:S(2)}) collective-permute-start(bf16[3,2048,256]{2,1,0:T(8,128)(2,1)} %pack_weights.1.refs_0_), channel_id=1, source_target_pairs={{0,1},{1,0},{2,3},{3,2},{4,5},{5,4},{6,7},{7,6},{8,9},{9,8},{10,11... | collective-permute-start | bytes 9437192 | tf_op jit(solution)/shard_map/ppermute | solution.py:32
  13.7 2.0 %pack.1 = (bf16[8,264,256]{2,1,0:T(8,128)(2,1)}, bf16[128,256]{1,0:T(8,128)(2,1)S(1)}) custom-call(bf16[128,256]{1,0:T(8,128)(2,1)} %keys_ref.1, bf16[128,256]{1,0:T(8,128)(2,1)} %values_ref.1, f32[2,256]{1,0:T(2,128)} %gates_ref.1, bf16[128,256]{1,0:T(8,128)(2,1)} %queries_ref.1), custom_call_target="tpu_custom_call" | custom-call | tf_op jit(solution)/shard_map/pack/pallas_call | solution.py:266
  15.7 8.3 %all-to-all-start = ((bf16[8,264,256]{2,1,0:T(8,128)(2,1)}), bf16[8,264,256]{2,1,0:T(8,128)(2,1)S(1)}, u32[]{:S(2)}, u32[]{:S(2)}) async-start(bf16[8,264,256]{2,1,0:T(8,128)(2,1)} %get-tuple-element.11), calls=%async_computation | async-start | bytes 2162688 | tf_op jit(solution)/shard_map/all_to_all | solution.py:277
  24.0 3.1 %collective-permute-start = (bf16[128,256]{1,0:T(8,128)(2,1)S(1)}, bf16[128,256]{1,0:T(8,128)(2,1)S(1)}, u32[]{:S(2)}, u32[]{:S(2)}) collective-permute-start(bf16[128,256]{1,0:T(8,128)(2,1)S(1)} %get-tuple-element.13.refs_0_), channel_id=1, source_target_pairs={{0,16},{16,32},{32,48},{48,0},{1,17},{17,33},{33,49},{49,1},{2,18}... | collective-permute-start | bytes 196616 | tf_op jit(solution)/shard_map/ppermute | solution.py:279
  27.1 4.4 %collective-permute-start.1 = (bf16[128,256]{1,0:T(8,128)(2,1)S(1)}, bf16[128,256]{1,0:T(8,128)(2,1)S(1)}, u32[]{:S(2)}, u32[]{:S(2)}) collective-permute-start(bf16[128,256]{1,0:T(8,128)(2,1)S(1)} %get-tuple-element.13.refs_0_), channel_id=1, source_target_pairs={{0,32},{16,48},{32,0},{48,16},{1,33},{17,49},{33,1},{49,17},{2,34}... | collective-permute-start | bytes 196616 | tf_op jit(solution)/shard_map/ppermute | solution.py:279
  31.4 3.1 %collective-permute-start.2 = (bf16[128,256]{1,0:T(8,128)(2,1)S(1)}, bf16[128,256]{1,0:T(8,128)(2,1)S(1)}, u32[]{:S(2)}, u32[]{:S(2)}) collective-permute-start(bf16[128,256]{1,0:T(8,128)(2,1)S(1)} %get-tuple-element.13.refs_0_), channel_id=1, source_target_pairs={{0,48},{16,0},{32,16},{48,32},{1,49},{17,1},{33,17},{49,33},{2,50}... | collective-permute-start | bytes 196616 | tf_op jit(solution)/shard_map/ppermute | solution.py:279
  34.5 0.0 copy-done.2
  34.5 0.2 convolution_convert_fusion.1
  34.7 0.1 eq.56
  34.8 0.1 eq.57
  34.9 0.1 and.15
  34.9 0.1 and.16
  35.0 0.1 eq.59
  35.1 0.2 and_convert_fusion
  35.3 0.0 collective-permute-done.refs_1_
  35.3 0.0 copy-done
  35.3 3.0 %collective-permute-start.4 = (bf16[128,2048]{1,0:T(8,128)(2,1)S(1)}, bf16[128,2048]{1,0:T(8,128)(2,1)S(1)}, u32[]{:S(2)}, u32[]{:S(2)}) collective-permute-start(bf16[128,2048]{1,0:T(8,128)(2,1)S(1)} %copy-done), channel_id=1, source_target_pairs={{0,1},{1,0},{2,3},{3,2},{4,5},{5,4},{6,7},{7,6},{8,9},{9,8},{10,11... | collective-permute-start | bytes 1572872 | tf_op jit(solution)/shard_map/ppermute | solution.py:32
  38.4 0.6 pad_add_fusion.place_ref
  39.0 14.9 %all-to-all-done.kv_ref = bf16[8,264,256]{2,1,0:T(8,128)(2,1)S(1)} async-done(((bf16[8,264,256]{2,1,0:T(8,128)(2,1)}), bf16[8,264,256]{2,1,0:T(8,128)(2,1)S(1)}, u32[]{:S(2)}, u32[]{:S(2)}) %all-to-all-start) | async-done | bytes 1081376 | tf_op jit(solution)/shard_map/all_to_all | solution.py:277
  53.9 0.0 collective-permute-done.1.refs_2_
  53.9 0.0 collective-permute-done.2.refs_3_
  53.9 7.2 %attend.1 = bf16[4,2,144,256]{3,2,1,0:T(8,128)(2,1)} custom-call(s32[4]{0:T(128)} %pad_add_fusion.place_ref, bf16[8,264,256]{2,1,0:T(8,128)(2,1)S(1)} %all-to-all-done.kv_ref, bf16[128,256]{1,0:T(8,128)(2,1)S(1)} %get-tuple-element.13.refs_0_, bf16[128,256]{1,0:T(8,128)(2,1)S(1)} %collective-permute-done.refs_1_, ...), custom_call_target="tpu_custom_call" | custom-call | tf_op jit(solution)/shard_map/attend/pallas_call | solution.py:335
  61.1 4.8 %all-to-all-start.1 = ((bf16[8,144,256]{2,1,0:T(8,128)(2,1)}), bf16[8,144,256]{2,1,0:T(8,128)(2,1)S(1)}, u32[]{:S(2)}, u32[]{:S(2)}) async-start(bf16[8,144,256]{2,1,0:T(8,128)(2,1)} %bitcast.29), calls=%async_computation.1 | async-start | bytes 1179648 | tf_op jit(solution)/shard_map/all_to_all | solution.py:337
  65.9 0.0 collective-permute-done.5.refs_2_
  65.9 1.9 %collective-permute-start.6 = (bf16[3,2048,256]{2,1,0:T(8,128)(2,1)}, bf16[3,2048,256]{2,1,0:T(8,128)(2,1)}, u32[]{:S(2)}, u32[]{:S(2)}) collective-permute-start(bf16[3,2048,256]{2,1,0:T(8,128)(2,1)} %collective-permute-done.5.refs_2_), channel_id=1, source_target_pairs={{0,1},{1,0},{2,3},{3,2},{4,5},{5,4},{6,7},{7,6},{8,9},{9,8},{10,11... | collective-permute-start | bytes 9437192 | tf_op jit(solution)/shard_map/ppermute | solution.py:32
  67.8 8.1 %all-to-all-done.1 = bf16[8,144,256]{2,1,0:T(8,128)(2,1)S(1)} async-done(((bf16[8,144,256]{2,1,0:T(8,128)(2,1)}), bf16[8,144,256]{2,1,0:T(8,128)(2,1)S(1)}, u32[]{:S(2)}, u32[]{:S(2)}) %all-to-all-start.1) | async-done | bytes 589856 | tf_op jit(solution)/shard_map/all_to_all | solution.py:337
  75.9 0.0 collective-permute-done.3.refs_1_
  75.9 0.0 collective-permute-done.4.far_weight_ref
  75.9 1.2 project.1
  77.1 19.5 %all_to_all.35 = bf16[8,256,128]{2,1,0:T(8,128)(2,1)S(1)} all-to-all(bf16[8,256,128]{2,1,0:T(8,128)(2,1)S(1)} %project.1), channel_id=1, replica_groups=mesh['z'=8,'x'=4,'y'=8,'c'=2] {'y'}, dimensions={0} | all-to-all | bytes 1048576 | tf_op jit(solution)/shard_map/all_to_all | solution.py:358
  96.7 0.1 convert_reduce_fusion
  96.7 0.0 copy-done.1
  96.7 0.2 convolution_convert_fusion
  97.0 13.0 %all_to_all.36 = bf16[32,20,128]{2,1,0:T(8,128)(2,1)S(1)} all-to-all(bf16[32,20,128]{2,1,0:T(8,128)(2,1)S(1)} %reshape.46), channel_id=1, replica_groups=mesh['z'=8,'x'=4,'y'=8,'c'=2] {'z','x'}, dimensions={0} | all-to-all | bytes 327680 | tf_op jit(solution)/shard_map/all_to_all | solution.py:364
  110.0 0.1 broadcast_in_dim.50
  110.1 26.6 %all_to_all.37.rows_in_ref = bf16[16,160,128]{2,1,0:T(8,128)(2,1)S(1)} all-to-all(bf16[16,160,128]{2,1,0:T(8,128)(2,1)S(1)} %bitcast.28), channel_id=1, replica_groups=mesh['z'=8,'x'=4,'y'=8,'c'=2] {'y','c'}, dimensions={0} | all-to-all | bytes 1310720 | tf_op jit(solution)/shard_map/all_to_all | solution.py:368
  136.8 0.0 collective-permute-done.6.refs_3_
  136.8 6.8 %expert.1 = bf16[16,160,128]{2,1,0:T(8,128)(2,1)S(1)} custom-call(bf16[16,160,128]{2,1,0:T(8,128)(2,1)S(1)} %all_to_all.37.rows_in_ref, f32[16,1,128]{2,1,0:T(1,128)} %bitcast.35, bf16[3,2048,256]{2,1,0:T(8,128)(2,1)} %pack_weights.1.refs_0_, bf16[3,2048,256]{2,1,0:T(8,128)(2,1)} %collective-permute-done.3.refs_1_, ...), custom_call_target="tpu_custom_call" | custom-call | tf_op jit(solution)/shard_map/expert/pallas_call | solution.py:372
  143.6 22.6 %all_to_all.38 = bf16[16,160,128]{2,1,0:T(8,128)(2,1)S(1)} all-to-all(bf16[16,160,128]{2,1,0:T(8,128)(2,1)S(1)} %expert.1), channel_id=1, replica_groups=mesh['z'=8,'x'=4,'y'=8,'c'=2] {'y','c'}, dimensions={0} | all-to-all | bytes 1310720 | tf_op jit(solution)/shard_map/all_to_all | solution.py:386
  166.2 0.1 reduce_sum.32
  166.3 0.7 reshape.51
  167.0 3.9 %all-to-all-start.6 = ((bf16[32,20,128]{2,1,0:T(8,128)(2,1)}), bf16[32,20,128]{2,1,0:T(8,128)(2,1)S(1)}, u32[]{:S(2)}, u32[]{:S(2)}) async-start(bf16[32,20,128]{2,1,0:T(8,128)(2,1)} %reshape.51), calls=%async_computation.6 | async-start | bytes 393216 | tf_op jit(solution)/shard_map/all_to_all | solution.py:390
  170.9 0.0 copy-done.3
  170.9 11.0 %all-to-all-done.6 = bf16[32,20,128]{2,1,0:T(8,128)(2,1)S(1)} async-done(((bf16[32,20,128]{2,1,0:T(8,128)(2,1)}), bf16[32,20,128]{2,1,0:T(8,128)(2,1)S(1)}, u32[]{:S(2)}, u32[]{:S(2)}) %all-to-all-start.6) | async-done | bytes 163872 | tf_op jit(solution)/shard_map/all_to_all | solution.py:390
  182.0 0.3 convolution_bitcast_fusion
  182.3 0.9 fusion.2
  (10 shorter events, 0.1 us)
Async XLA Ops:
  0.0 34.5 %copy-start.2 = (s32[256,2]{0,1:T(2,128)S(1)}, s32[256,2]{0,1:T(2,128)}, u32[]{:S(2)}) copy-start(s32[256,2]{0,1:T(2,128)} %param.19) | copy-start | bytes 6148
  3.0 62.9 %collective-permute-start.5 = (bf16[3,2048,256]{2,1,0:T(8,128)(2,1)}, bf16[3,2048,256]{2,1,0:T(8,128)(2,1)}, u32[]{:S(2)}, u32[]{:S(2)}) collective-permute-start(bf16[3,2048,256]{2,1,0:T(8,128)(2,1)} %pack_weights.1.refs_0_), channel_id=1, source_target_pairs={{0,14},{1,3},{2,0},{3,5},{4,2},{5,7},{6,4},{7,9},{8,6},{9,11},{10,... | collective-permute-start | bytes 9437192 | tf_op jit(solution)/shard_map/ppermute | solution.py:302
  7.0 68.9 %collective-permute-start.3 = (bf16[3,2048,256]{2,1,0:T(8,128)(2,1)}, bf16[3,2048,256]{2,1,0:T(8,128)(2,1)}, u32[]{:S(2)}, u32[]{:S(2)}) collective-permute-start(bf16[3,2048,256]{2,1,0:T(8,128)(2,1)} %pack_weights.1.refs_0_), channel_id=1, source_target_pairs={{0,1},{1,0},{2,3},{3,2},{4,5},{5,4},{6,7},{7,6},{8,9},{9,8},{10,11... | collective-permute-start | bytes 9437192 | tf_op jit(solution)/shard_map/ppermute | solution.py:32
  15.7 19.7 %copy-start = (bf16[128,2048]{1,0:T(8,128)(2,1)S(1)}, bf16[128,2048]{1,0:T(8,128)(2,1)}, u32[]{:S(2)}) copy-start(bf16[128,2048]{1,0:T(8,128)(2,1)} %weight_ref.1) | copy-start | bytes 1572868
  15.7 38.2 %all-to-all-start = ((bf16[8,264,256]{2,1,0:T(8,128)(2,1)}), bf16[8,264,256]{2,1,0:T(8,128)(2,1)S(1)}, u32[]{:S(2)}, u32[]{:S(2)}) async-start(bf16[8,264,256]{2,1,0:T(8,128)(2,1)} %get-tuple-element.11), calls=%async_computation | async-start | bytes 2162688 | tf_op jit(solution)/shard_map/all_to_all | solution.py:277
  24.0 11.4 %collective-permute-start = (bf16[128,256]{1,0:T(8,128)(2,1)S(1)}, bf16[128,256]{1,0:T(8,128)(2,1)S(1)}, u32[]{:S(2)}, u32[]{:S(2)}) collective-permute-start(bf16[128,256]{1,0:T(8,128)(2,1)S(1)} %get-tuple-element.13.refs_0_), channel_id=1, source_target_pairs={{0,16},{16,32},{32,48},{48,0},{1,17},{17,33},{33,49},{49,1},{2,18}... | collective-permute-start | bytes 196616 | tf_op jit(solution)/shard_map/ppermute | solution.py:279
  27.1 26.9 %collective-permute-start.1 = (bf16[128,256]{1,0:T(8,128)(2,1)S(1)}, bf16[128,256]{1,0:T(8,128)(2,1)S(1)}, u32[]{:S(2)}, u32[]{:S(2)}) collective-permute-start(bf16[128,256]{1,0:T(8,128)(2,1)S(1)} %get-tuple-element.13.refs_0_), channel_id=1, source_target_pairs={{0,32},{16,48},{32,0},{48,16},{1,33},{17,49},{33,1},{49,17},{2,34}... | collective-permute-start | bytes 196616 | tf_op jit(solution)/shard_map/ppermute | solution.py:279
  31.4 22.5 %collective-permute-start.2 = (bf16[128,256]{1,0:T(8,128)(2,1)S(1)}, bf16[128,256]{1,0:T(8,128)(2,1)S(1)}, u32[]{:S(2)}, u32[]{:S(2)}) collective-permute-start(bf16[128,256]{1,0:T(8,128)(2,1)S(1)} %get-tuple-element.13.refs_0_), channel_id=1, source_target_pairs={{0,48},{16,0},{32,16},{48,32},{1,49},{17,1},{33,17},{49,33},{2,50}... | collective-permute-start | bytes 196616 | tf_op jit(solution)/shard_map/ppermute | solution.py:279
  35.3 40.6 %collective-permute-start.4 = (bf16[128,2048]{1,0:T(8,128)(2,1)S(1)}, bf16[128,2048]{1,0:T(8,128)(2,1)S(1)}, u32[]{:S(2)}, u32[]{:S(2)}) collective-permute-start(bf16[128,2048]{1,0:T(8,128)(2,1)S(1)} %copy-done), channel_id=1, source_target_pairs={{0,1},{1,0},{2,3},{3,2},{4,5},{5,4},{6,7},{7,6},{8,9},{9,8},{10,11... | collective-permute-start | bytes 1572872 | tf_op jit(solution)/shard_map/ppermute | solution.py:32
  39.0 57.7 %copy-start.1 = (bf16[256,128]{1,0:T(8,128)(2,1)S(1)}, bf16[256,128]{1,0:T(8,128)(2,1)}, u32[]{:S(2)}) copy-start(bf16[256,128]{1,0:T(8,128)(2,1)} %param.12) | copy-start | bytes 196612
  61.1 14.8 %all-to-all-start.1 = ((bf16[8,144,256]{2,1,0:T(8,128)(2,1)}), bf16[8,144,256]{2,1,0:T(8,128)(2,1)S(1)}, u32[]{:S(2)}, u32[]{:S(2)}) async-start(bf16[8,144,256]{2,1,0:T(8,128)(2,1)} %bitcast.29), calls=%async_computation.1 | async-start | bytes 1179648 | tf_op jit(solution)/shard_map/all_to_all | solution.py:337
  65.9 70.9 %collective-permute-start.6 = (bf16[3,2048,256]{2,1,0:T(8,128)(2,1)}, bf16[3,2048,256]{2,1,0:T(8,128)(2,1)}, u32[]{:S(2)}, u32[]{:S(2)}) collective-permute-start(bf16[3,2048,256]{2,1,0:T(8,128)(2,1)} %collective-permute-done.5.refs_2_), channel_id=1, source_target_pairs={{0,1},{1,0},{2,3},{3,2},{4,5},{5,4},{6,7},{7,6},{8,9},{9,8},{10,11... | collective-permute-start | bytes 9437192 | tf_op jit(solution)/shard_map/ppermute | solution.py:32
  136.8 34.1 %copy-start.3 = (f32[256,2]{0,1:T(2,128)S(1)}, f32[256,2]{0,1:T(2,128)}, u32[]{:S(2)}) copy-start(f32[256,2]{0,1:T(2,128)} %param.20) | copy-start | bytes 6148
  167.0 14.9 %all-to-all-start.6 = ((bf16[32,20,128]{2,1,0:T(8,128)(2,1)}), bf16[32,20,128]{2,1,0:T(8,128)(2,1)S(1)}, u32[]{:S(2)}, u32[]{:S(2)}) async-start(bf16[32,20,128]{2,1,0:T(8,128)(2,1)} %reshape.51), calls=%async_computation.6 | async-start | bytes 393216 | tf_op jit(solution)/shard_map/all_to_all | solution.py:390

commit v9 on v7

--- a/solution.py
+++ b/solution.py
@@ -211,8 +211,9 @@
         squares = squares + values * values
     scale = lax.rsqrt(jnp.sum(squares, axis=1, keepdims=True) / width + norm_eps)
     for block in range(blocks):
-        values = rows_in_ref[block].astype(jnp.float32) * scale * gain_ref[block]
-        rows_ref[:, block * lane : (block + 1) * lane] = values.astype(jnp.bfloat16)
+        place = block % (blocks // 2) * 2 + block // (blocks // 2)
+        values = rows_in_ref[block].astype(jnp.float32) * scale * gain_ref[place]
+        rows_ref[:, place * lane : (place + 1) * lane] = values.astype(jnp.bfloat16)
     for part in range(sets):
         copies[part][0].wait()
         gate = jnp.dot(rows_ref[...], kinds[part, 0], preferred_element_type=jnp.float32)
@@ -228,7 +229,8 @@
             for part in range(sets)
         ).astype(jnp.bfloat16)
         for piece in range(units // lane):
-            out_ref[block * (units // lane) + piece] = total[:, piece * lane : (piece + 1) * lane]
+            place = block * (units // lane) + piece
+            out_ref[place % 2 * (blocks // 2) + place // 2] = total[:, piece * lane : (piece + 1) * lane]
 
 
 def shards(
@@ -365,9 +367,14 @@
     arrived = lax.all_to_all(sent.reshape(sp_count, capacity, local_width), SP, split_axis=0, concat_axis=0, tiled=True)
     quarter = slot_total // 4
     arrived = arrived.reshape(4, quarter, local_width)
-    copies = jnp.broadcast_to(arrived, (y_count // 2, *arrived.shape))
+    by_core = arrived.reshape(2, 2, quarter, local_width).swapaxes(0, 1)
+    copies = jnp.broadcast_to(by_core[:, None], (2, y_count // 2, 2, quarter, local_width))
     rows = lax.all_to_all(
-        copies.reshape(2 * y_count, quarter, local_width), TP, split_axis=0, concat_axis=0, tiled=True
+        copies.reshape(2 * y_count, quarter, local_width),
+        ("c", "y"),
+        split_axis=0,
+        concat_axis=0,
+        tiled=True,
     )
     sets = len(weight_sets)
     out_rows = pl.pallas_call(
@@ -384,10 +391,10 @@
         name="expert",
         interpret=INTERPRET,
     )(held(rows), norm_gain.reshape(2 * y_count, 1, lane), *weight_sets)
-    pieces = lax.all_to_all(out_rows, TP, split_axis=0, concat_axis=0, tiled=True)
+    pieces = lax.all_to_all(out_rows, ("c", "y"), split_axis=0, concat_axis=0, tiled=True)
     expert_out = jnp.sum(
-        pieces.reshape(y_count // 2, 4, quarter, local_width).astype(f32), axis=0
-    ).astype(bf16)
+        pieces.reshape(2, y_count // 2, 2, quarter, local_width).astype(f32), axis=1
+    ).astype(bf16).swapaxes(0, 1)
     back = lax.all_to_all(
         expert_out.reshape(sp_count, capacity, local_width), SP, split_axis=0, concat_axis=0, tiled=True
     ).reshape(slot_total, local_width)

time: 202 us -> 201 us (level)
  no operation moved by 1% of the time
where the time goes in v9:
time: 201 us; the launch traced here: 199 us
  blocking collectives  68.1 us (34%)
  waiting for transfers between devices  57.1 us (28%)
  starting transfers between devices  48.5 us (24%)
  Pallas kernels  21.2 us (11%)
    all_to_all x1, blocking collectives, shards(): lax.all_to_all(copies.reshape(2 * y_count, quarter, local_width), ('c', '...  24.1 us
    all_to_all x1, blocking collectives, shards(): lax.all_to_all(out_rows, ('c', 'y'), split_axis=0, concat_axis=0, tiled=T...  23 us
    all_to_all x1, blocking collectives, shards(): lax.all_to_all(sent.reshape(sp_count, capacity, local_width), SP, split_a...  21.1 us
    ppermute x1, waiting for transfers between devices, shards(): near_set = lax.ppermute(own_set, TP, slice_moves)  19.7 us
    all_to_all x1, waiting for transfers between devices, shards(): lax.all_to_all(projected, 'y', split_axis=0, concat_axis=0, tiled=True)  16.4 us
    ppermute x3, starting transfers between devices, swapped(): return lax.ppermute(shard, 'c', [(0, 1), (1, 0)])  14.8 us
    all_to_all x1, waiting for transfers between devices, shards(): lax.all_to_all(parts.reshape(2 * x_count, *part_shape[2:]), ('x', 'c'), s...  10.1 us
    all_to_all x1, starting transfers between devices, shards(): lax.all_to_all(message, 'z', split_axis=0, concat_axis=0, tiled=True)  10 us
  transfers between devices with their start and end apart: 11, of which 5 were waited for; matrix products, arithmetic and copies ran while one was open for 1% of the time, Pallas kernels for 6%

profile of v9, /device:TPU:1, one launch (start us, length us, event | category | flops | bytes accessed | tf_op | source)
XLA Modules:
  0.0 199.0 jit_solution(12776699843516834398)
XLA Ops:
  0.0 3.0 %pack_weights.1.refs_0_ = bf16[3,2048,256]{2,1,0:T(8,128)(2,1)} custom-call(bf16[2048,256]{1,0:T(8,128)(2,1)} %bitcast.33, bf16[2048,256]{1,0:T(8,128)(2,1)} %bitcast.34, bf16[256,2048]{1,0:T(8,128)(2,1)} %bitcast.35), custom_call_target="tpu_custom_call" | custom-call | tf_op jit(solution)/shard_map/pack_weights/pallas_call | solution.py:291
  3.0 4.0 %collective-permute-start.5 = (bf16[3,2048,256]{2,1,0:T(8,128)(2,1)}, bf16[3,2048,256]{2,1,0:T(8,128)(2,1)}, u32[]{:S(2)}, u32[]{:S(2)}) collective-permute-start(bf16[3,2048,256]{2,1,0:T(8,128)(2,1)} %pack_weights.1.refs_0_), channel_id=1, source_target_pairs={{0,14},{1,3},{2,0},{3,5},{4,2},{5,7},{6,4},{7,9},{8,6},{9,11},{10,... | collective-permute-start | bytes 9437192 | tf_op jit(solution)/shard_map/ppermute | solution.py:304
  7.1 2.1 %pack.1 = (bf16[8,264,256]{2,1,0:T(8,128)(2,1)}, bf16[128,256]{1,0:T(8,128)(2,1)S(1)}) custom-call(bf16[128,256]{1,0:T(8,128)(2,1)} %keys_ref.1, bf16[128,256]{1,0:T(8,128)(2,1)} %values_ref.1, f32[2,256]{1,0:T(2,128)} %gates_ref.1, bf16[128,256]{1,0:T(8,128)(2,1)} %queries_ref.1), custom_call_target="tpu_custom_call" | custom-call | tf_op jit(solution)/shard_map/pack/pallas_call | solution.py:268
  9.1 10.0 %all-to-all-start = ((bf16[8,264,256]{2,1,0:T(8,128)(2,1)}), bf16[8,264,256]{2,1,0:T(8,128)(2,1)S(1)}, u32[]{:S(2)}, u32[]{:S(2)}) async-start(bf16[8,264,256]{2,1,0:T(8,128)(2,1)} %get-tuple-element.11), calls=%async_computation | async-start | bytes 2162688 | tf_op jit(solution)/shard_map/all_to_all | solution.py:279
  19.2 5.0 %collective-permute-start.4 = (bf16[3,2048,256]{2,1,0:T(8,128)(2,1)}, bf16[3,2048,256]{2,1,0:T(8,128)(2,1)}, u32[]{:S(2)}, u32[]{:S(2)}) collective-permute-start(bf16[3,2048,256]{2,1,0:T(8,128)(2,1)} %pack_weights.1.refs_0_), channel_id=1, source_target_pairs={{0,1},{1,0},{2,3},{3,2},{4,5},{5,4},{6,7},{7,6},{8,9},{9,8},{10,11... | collective-permute-start | bytes 9437192 | tf_op jit(solution)/shard_map/ppermute | solution.py:32
  24.2 19.7 %collective-permute-done.5.refs_2_ = bf16[3,2048,256]{2,1,0:T(8,128)(2,1)} collective-permute-done((bf16[3,2048,256]{2,1,0:T(8,128)(2,1)}, bf16[3,2048,256]{2,1,0:T(8,128)(2,1)}, u32[]{:S(2)}, u32[]{:S(2)}) %collective-permute-start.5) | collective-permute-done | bytes 3145760 | tf_op jit(solution)/shard_map/ppermute | solution.py:304
  43.9 7.3 %collective-permute-start.6 = (bf16[3,2048,256]{2,1,0:T(8,128)(2,1)}, bf16[3,2048,256]{2,1,0:T(8,128)(2,1)}, u32[]{:S(2)}, u32[]{:S(2)}) collective-permute-start(bf16[3,2048,256]{2,1,0:T(8,128)(2,1)} %collective-permute-done.5.refs_2_), channel_id=1, source_target_pairs={{0,1},{1,0},{2,3},{3,2},{4,5},{5,4},{6,7},{7,6},{8,9},{9,8},{10,11... | collective-permute-start | bytes 9437192 | tf_op jit(solution)/shard_map/ppermute | solution.py:32
  51.3 1.9 collective-permute-start.2
  53.2 1.9 collective-permute-start.1
  55.1 3.4 %collective-permute-start = (bf16[128,256]{1,0:T(8,128)(2,1)S(1)}, bf16[128,256]{1,0:T(8,128)(2,1)S(1)}, u32[]{:S(2)}, u32[]{:S(2)}) collective-permute-start(bf16[128,256]{1,0:T(8,128)(2,1)S(1)} %get-tuple-element.12.refs_0_), channel_id=1, source_target_pairs={{0,16},{16,32},{32,48},{48,0},{1,17},{17,33},{33,49},{49,1},{2,18}... | collective-permute-start | bytes 196616 | tf_op jit(solution)/shard_map/ppermute | solution.py:281
  58.5 0.0 collective-permute-done.2.refs_3_
  58.5 0.0 copy-done
  58.5 2.5 %collective-permute-start.3 = (bf16[128,2048]{1,0:T(8,128)(2,1)S(1)}, bf16[128,2048]{1,0:T(8,128)(2,1)S(1)}, u32[]{:S(2)}, u32[]{:S(2)}) collective-permute-start(bf16[128,2048]{1,0:T(8,128)(2,1)S(1)} %copy-done), channel_id=1, source_target_pairs={{0,1},{1,0},{2,3},{3,2},{4,5},{5,4},{6,7},{7,6},{8,9},{9,8},{10,11... | collective-permute-start | bytes 1572872 | tf_op jit(solution)/shard_map/ppermute | solution.py:32
  61.0 0.6 pad_add_fusion.place_ref
  61.6 0.0 collective-permute-done.1.refs_2_
  61.6 0.9 collective-permute-done.refs_1_
  62.5 0.0 all-to-all-done.kv_ref
  62.5 7.2 %attend.1 = bf16[4,2,144,256]{3,2,1,0:T(8,128)(2,1)} custom-call(s32[4]{0:T(128)} %pad_add_fusion.place_ref, bf16[8,264,256]{2,1,0:T(8,128)(2,1)S(1)} %all-to-all-done.kv_ref, bf16[128,256]{1,0:T(8,128)(2,1)S(1)} %get-tuple-element.12.refs_0_, bf16[128,256]{1,0:T(8,128)(2,1)S(1)} %collective-permute-done.refs_1_, ...), custom_call_target="tpu_custom_call" | custom-call | tf_op jit(solution)/shard_map/attend/pallas_call | solution.py:323
  69.7 4.9 %all-to-all-start.1 = ((bf16[8,144,256]{2,1,0:T(8,128)(2,1)}), bf16[8,144,256]{2,1,0:T(8,128)(2,1)S(1)}, u32[]{:S(2)}, u32[]{:S(2)}) async-start(bf16[8,144,256]{2,1,0:T(8,128)(2,1)} %bitcast.32), calls=%async_computation.1 | async-start | bytes 1179648 | tf_op jit(solution)/shard_map/all_to_all | solution.py:325
  74.6 0.0 collective-permute-done.3.far_weight_ref
  74.6 10.1 %all-to-all-done.1 = bf16[8,144,256]{2,1,0:T(8,128)(2,1)S(1)} async-done(((bf16[8,144,256]{2,1,0:T(8,128)(2,1)}), bf16[8,144,256]{2,1,0:T(8,128)(2,1)S(1)}, u32[]{:S(2)}, u32[]{:S(2)}) %all-to-all-start.1) | async-done | bytes 589856 | tf_op jit(solution)/shard_map/all_to_all | solution.py:325
  84.7 2.1 %project.1 = bf16[8,256,128]{2,1,0:T(8,128)(2,1)} custom-call(s32[4]{0:T(128)} %pad_add_fusion.place_ref, bf16[4,2,144,256]{3,2,1,0:T(8,128)(2,1)S(1)} %bitcast.29, bf16[128,2048]{1,0:T(8,128)(2,1)S(1)} %copy-done, bf16[128,2048]{1,0:T(8,128)(2,1)S(1)} %collective-permute-done.3.far_weight_ref), custom_call_target="tpu_custom_call" | custom-call | tf_op jit(solution)/shard_map/project/pallas_call | solution.py:349
  86.8 3.6 %all-to-all-start.2 = ((bf16[8,256,128]{2,1,0:T(8,128)(2,1)}), bf16[8,256,128]{2,1,0:T(8,128)(2,1)S(1)}, u32[]{:S(2)}, u32[]{:S(2)}) async-start(bf16[8,256,128]{2,1,0:T(8,128)(2,1)} %project.1), calls=%async_computation.2 | async-start | bytes 1048576 | tf_op jit(solution)/shard_map/all_to_all | solution.py:358
  90.5 0.1 eq.62
  90.6 0.1 and.15
  90.7 0.1 and.16
  90.8 0.2 convolution_convert_fusion.1
  90.9 0.1 eq.59
  91.0 0.1 eq.60
  91.1 0.0 collective-permute-done.4.refs_1_
  91.1 16.4 %all-to-all-done.2 = bf16[8,256,128]{2,1,0:T(8,128)(2,1)S(1)} async-done(((bf16[8,256,128]{2,1,0:T(8,128)(2,1)}), bf16[8,256,128]{2,1,0:T(8,128)(2,1)S(1)}, u32[]{:S(2)}, u32[]{:S(2)}) %all-to-all-start.2) | async-done | bytes 524320 | tf_op jit(solution)/shard_map/all_to_all | solution.py:358
  107.5 0.0 collective-permute-done.6.refs_3_
  107.5 0.1 convert_reduce_fusion
  107.6 0.0 copy-done.1
  107.6 0.3 convolution_convert_fusion
  107.9 21.1 %all_to_all.35 = bf16[32,20,128]{2,1,0:T(8,128)(2,1)S(1)} all-to-all(bf16[32,20,128]{2,1,0:T(8,128)(2,1)S(1)} %reshape.44), channel_id=1, replica_groups=mesh['z'=8,'x'=4,'y'=8,'c'=2] {'z','x'}, dimensions={0} | all-to-all | bytes 327680 | tf_op jit(solution)/shard_map/all_to_all | solution.py:367
  129.1 0.1 broadcast_in_dim.53
  129.2 24.1 %all_to_all.36.rows_in_ref = bf16[16,160,128]{2,1,0:T(8,128)(2,1)S(1)} all-to-all(bf16[16,160,128]{2,1,0:T(8,128)(2,1)S(1)} %bitcast.31), channel_id=1, replica_groups=mesh['z'=8,'x'=4,'y'=8,'c'=2] {'c','y'}, dimensions={0} | all-to-all | bytes 1310720 | tf_op jit(solution)/shard_map/all_to_all | solution.py:372
  153.2 6.8 %expert.1 = bf16[16,160,128]{2,1,0:T(8,128)(2,1)S(1)} custom-call(bf16[16,160,128]{2,1,0:T(8,128)(2,1)S(1)} %all_to_all.36.rows_in_ref, f32[16,1,128]{2,1,0:T(1,128)} %bitcast.40, bf16[3,2048,256]{2,1,0:T(8,128)(2,1)} %pack_weights.1.refs_0_, bf16[3,2048,256]{2,1,0:T(8,128)(2,1)} %collective-permute-done.4.refs_1_, ...), custom_call_target="tpu_custom_call" | custom-call | tf_op jit(solution)/shard_map/expert/pallas_call | solution.py:380
  160.0 0.0 copy-start.3
  160.0 23.0 %all_to_all.37 = bf16[16,160,128]{2,1,0:T(8,128)(2,1)S(1)} all-to-all(bf16[16,160,128]{2,1,0:T(8,128)(2,1)S(1)} %expert.1), channel_id=1, replica_groups=mesh['z'=8,'x'=4,'y'=8,'c'=2] {'c','y'}, dimensions={0} | all-to-all | bytes 1310720 | tf_op jit(solution)/shard_map/all_to_all | solution.py:394
  183.0 0.1 reduce_sum.32
  183.2 0.7 reshape.48
  183.9 3.9 %all-to-all-start.6 = ((bf16[32,20,128]{2,1,0:T(8,128)(2,1)}), bf16[32,20,128]{2,1,0:T(8,128)(2,1)S(1)}, u32[]{:S(2)}, u32[]{:S(2)}) async-start(bf16[32,20,128]{2,1,0:T(8,128)(2,1)} %reshape.48), calls=%async_computation.6 | async-start | bytes 393216 | tf_op jit(solution)/shard_map/all_to_all | solution.py:398
  187.7 0.0 copy-done.3
  187.8 10.0 %all-to-all-done.6 = bf16[32,20,128]{2,1,0:T(8,128)(2,1)S(1)} async-done(((bf16[32,20,128]{2,1,0:T(8,128)(2,1)}), bf16[32,20,128]{2,1,0:T(8,128)(2,1)S(1)}, u32[]{:S(2)}, u32[]{:S(2)}) %all-to-all-start.6) | async-done | bytes 163872 | tf_op jit(solution)/shard_map/all_to_all | solution.py:398
  197.8 0.3 convolution_bitcast_fusion
  198.1 0.9 fusion.2
  (12 shorter events, 0.1 us)
Async XLA Ops:
  0.0 58.5 %copy-start = (bf16[128,2048]{1,0:T(8,128)(2,1)S(1)}, bf16[128,2048]{1,0:T(8,128)(2,1)}, u32[]{:S(2)}) copy-start(bf16[128,2048]{1,0:T(8,128)(2,1)} %weight_ref.1) | copy-start | bytes 1572868
  3.0 40.9 %collective-permute-start.5 = (bf16[3,2048,256]{2,1,0:T(8,128)(2,1)}, bf16[3,2048,256]{2,1,0:T(8,128)(2,1)}, u32[]{:S(2)}, u32[]{:S(2)}) collective-permute-start(bf16[3,2048,256]{2,1,0:T(8,128)(2,1)} %pack_weights.1.refs_0_), channel_id=1, source_target_pairs={{0,14},{1,3},{2,0},{3,5},{4,2},{5,7},{6,4},{7,9},{8,6},{9,11},{10,... | collective-permute-start | bytes 9437192 | tf_op jit(solution)/shard_map/ppermute | solution.py:304
  9.1 53.4 %all-to-all-start = ((bf16[8,264,256]{2,1,0:T(8,128)(2,1)}), bf16[8,264,256]{2,1,0:T(8,128)(2,1)S(1)}, u32[]{:S(2)}, u32[]{:S(2)}) async-start(bf16[8,264,256]{2,1,0:T(8,128)(2,1)} %get-tuple-element.11), calls=%async_computation | async-start | bytes 2162688 | tf_op jit(solution)/shard_map/all_to_all | solution.py:279
  19.2 71.9 %collective-permute-start.4 = (bf16[3,2048,256]{2,1,0:T(8,128)(2,1)}, bf16[3,2048,256]{2,1,0:T(8,128)(2,1)}, u32[]{:S(2)}, u32[]{:S(2)}) collective-permute-start(bf16[3,2048,256]{2,1,0:T(8,128)(2,1)} %pack_weights.1.refs_0_), channel_id=1, source_target_pairs={{0,1},{1,0},{2,3},{3,2},{4,5},{5,4},{6,7},{7,6},{8,9},{9,8},{10,11... | collective-permute-start | bytes 9437192 | tf_op jit(solution)/shard_map/ppermute | solution.py:32
  43.9 63.6 %collective-permute-start.6 = (bf16[3,2048,256]{2,1,0:T(8,128)(2,1)}, bf16[3,2048,256]{2,1,0:T(8,128)(2,1)}, u32[]{:S(2)}, u32[]{:S(2)}) collective-permute-start(bf16[3,2048,256]{2,1,0:T(8,128)(2,1)} %collective-permute-done.5.refs_2_), channel_id=1, source_target_pairs={{0,1},{1,0},{2,3},{3,2},{4,5},{5,4},{6,7},{7,6},{8,9},{9,8},{10,11... | collective-permute-start | bytes 9437192 | tf_op jit(solution)/shard_map/ppermute | solution.py:32
  51.3 7.2 %collective-permute-start.2 = (bf16[128,256]{1,0:T(8,128)(2,1)S(1)}, bf16[128,256]{1,0:T(8,128)(2,1)S(1)}, u32[]{:S(2)}, u32[]{:S(2)}) collective-permute-start(bf16[128,256]{1,0:T(8,128)(2,1)S(1)} %get-tuple-element.12.refs_0_), channel_id=1, source_target_pairs={{0,48},{16,0},{32,16},{48,32},{1,49},{17,1},{33,17},{49,33},{2,50}... | collective-permute-start | bytes 196616 | tf_op jit(solution)/shard_map/ppermute | solution.py:281
  53.2 8.4 %collective-permute-start.1 = (bf16[128,256]{1,0:T(8,128)(2,1)S(1)}, bf16[128,256]{1,0:T(8,128)(2,1)S(1)}, u32[]{:S(2)}, u32[]{:S(2)}) collective-permute-start(bf16[128,256]{1,0:T(8,128)(2,1)S(1)} %get-tuple-element.12.refs_0_), channel_id=1, source_target_pairs={{0,32},{16,48},{32,0},{48,16},{1,33},{17,49},{33,1},{49,17},{2,34}... | collective-permute-start | bytes 196616 | tf_op jit(solution)/shard_map/ppermute | solution.py:281
  55.1 7.4 %collective-permute-start = (bf16[128,256]{1,0:T(8,128)(2,1)S(1)}, bf16[128,256]{1,0:T(8,128)(2,1)S(1)}, u32[]{:S(2)}, u32[]{:S(2)}) collective-permute-start(bf16[128,256]{1,0:T(8,128)(2,1)S(1)} %get-tuple-element.12.refs_0_), channel_id=1, source_target_pairs={{0,16},{16,32},{32,48},{48,0},{1,17},{17,33},{33,49},{49,1},{2,18}... | collective-permute-start | bytes 196616 | tf_op jit(solution)/shard_map/ppermute | solution.py:281
  58.5 16.1 %collective-permute-start.3 = (bf16[128,2048]{1,0:T(8,128)(2,1)S(1)}, bf16[128,2048]{1,0:T(8,128)(2,1)S(1)}, u32[]{:S(2)}, u32[]{:S(2)}) collective-permute-start(bf16[128,2048]{1,0:T(8,128)(2,1)S(1)} %copy-done), channel_id=1, source_target_pairs={{0,1},{1,0},{2,3},{3,2},{4,5},{5,4},{6,7},{7,6},{8,9},{9,8},{10,11... | collective-permute-start | bytes 1572872 | tf_op jit(solution)/shard_map/ppermute | solution.py:32
  61.6 29.0 %copy-start.2 = (s32[256,2]{0,1:T(2,128)S(1)}, s32[256,2]{0,1:T(2,128)}, u32[]{:S(2)}) copy-start(s32[256,2]{0,1:T(2,128)} %param.19) | copy-start | bytes 6148
  69.7 15.0 %all-to-all-start.1 = ((bf16[8,144,256]{2,1,0:T(8,128)(2,1)}), bf16[8,144,256]{2,1,0:T(8,128)(2,1)S(1)}, u32[]{:S(2)}, u32[]{:S(2)}) async-start(bf16[8,144,256]{2,1,0:T(8,128)(2,1)} %bitcast.32), calls=%async_computation.1 | async-start | bytes 1179648 | tf_op jit(solution)/shard_map/all_to_all | solution.py:325
  84.7 22.9 %copy-start.1 = (bf16[256,128]{1,0:T(8,128)(2,1)S(1)}, bf16[256,128]{1,0:T(8,128)(2,1)}, u32[]{:S(2)}) copy-start(bf16[256,128]{1,0:T(8,128)(2,1)} %param.12) | copy-start | bytes 196612
  86.8 20.6 %all-to-all-start.2 = ((bf16[8,256,128]{2,1,0:T(8,128)(2,1)}), bf16[8,256,128]{2,1,0:T(8,128)(2,1)S(1)}, u32[]{:S(2)}, u32[]{:S(2)}) async-start(bf16[8,256,128]{2,1,0:T(8,128)(2,1)} %project.1), calls=%async_computation.2 | async-start | bytes 1048576 | tf_op jit(solution)/shard_map/all_to_all | solution.py:358
  160.0 27.7 %copy-start.3 = (f32[256,2]{0,1:T(2,128)S(1)}, f32[256,2]{0,1:T(2,128)}, u32[]{:S(2)}) copy-start(f32[256,2]{0,1:T(2,128)} %param.20) | copy-start | bytes 6148
  183.9 13.9 %all-to-all-start.6 = ((bf16[32,20,128]{2,1,0:T(8,128)(2,1)}), bf16[32,20,128]{2,1,0:T(8,128)(2,1)S(1)}, u32[]{:S(2)}, u32[]{:S(2)}) async-start(bf16[32,20,128]{2,1,0:T(8,128)(2,1)} %reshape.48), calls=%async_computation.6 | async-start | bytes 393216 | tf_op jit(solution)/shard_map/all_to_all | solution.py:398
